TPU v7x, 512 devices: a 8x2x16 block of a 8x16x16 slice. The times are simulated.
512 devices in a mesh: grp: 2 (over y), tp: 16 (over z), dp: 16 (over x, core).
Axes of the slice: x: 8, y: 2, z: 16, core: 2. Of those that a mesh axis runs over, the one named last changes fastest.
The devices are a block of a 8x16x16 slice.
Arguments:
- tokens: bfloat16 [1024, 4096], P(('grp', 'tp'), 'dp'), parts along dimension 0, may hold values from -6 to 6
- lengths: int32 [256], P(('grp', 'dp')), parts along dimension 0, may hold values from 1 to 4, as said below
- norm_gain: float32 [2, 4096], P(None, 'dp'), may hold values from 0.1 to 1.9
- w_recept: bfloat16 [2, 4096, 2048], P(None, 'dp', 'tp'), may hold values from -0.09375 to 0.09375
- w_keys: bfloat16 [2, 4096, 2048], P(None, 'dp', 'tp'), may hold values from -0.09375 to 0.09375
- w_values: bfloat16 [2, 4096, 2048], P(None, 'dp', 'tp'), may hold values from -0.09375 to 0.09375
- w_decay: bfloat16 [2, 4096, 2048], P(None, 'dp', 'tp'), may hold values from -0.09375 to 0.09375
- w_rate: bfloat16 [2, 4096, 2048], P(None, 'dp', 'tp'), may hold values from -0.09375 to 0.09375
- w_gate: bfloat16 [2, 4096, 2048], P(None, 'dp', 'tp'), may hold values from -0.09375 to 0.09375
- decay_base: float32 [2, 2048], P(None, 'tp'), may hold values from -3 to 1
- group_gain: float32 [2, 2048], P(None, 'tp'), may hold values from 0.1 to 1.9
- w_out: bfloat16 [2, 2048, 4096], P(None, 'tp', 'dp'), may hold values from -0.125 to 0.125
- states: float32 [2, 256, 32, 4096], P(None, ('grp', 'dp'), 'tp'), parts along dimension 1, may hold values from -2 to 2
Outputs:
- tokens_out: bfloat16 [1024, 4096], P(('grp', 'tp'), 'dp'), parts along dimension 0
- states_out: float32 [2, 256, 32, 4096], P(None, ('grp', 'dp'), 'tp'), parts along dimension 1
There are 2 independent parts, one for each index of `grp`. A program takes and returns all parts, laid end to end along the dimension named above; an argument that names none is the same for every part. Nothing has to cross between parts.
Inputs may be any that keep to these rules, and one draw needn't show every extreme that they name: Sequence s has its first lengths[s] of its 4 slots live; in every draw all 8 sequences of some index of dp have 4 live slots.
All inputs are finite; a program needn't handle non-finite values.
Results may differ from a plain program's by a relative error of at most 0.029.
Values may be sent and summed in bfloat16 or wider, within the bound.
No kernel may reach another device: no remote copies, remote signals or barrier semaphores. Data moves between devices by JAX's collectives and lax.ppermute only.
A program may use at most 64 MiB of HBM per device.

v0:
```python
import jax
import jax.numpy as jnp
from jax import lax
from jax.sharding import PartitionSpec as P

D = 4096
HEAD = 64
NEW = 4


norm_epsilon = 1e-06
unit_epsilon = 0.00064
group_epsilon = 0.00064


def laid_out(blocks, dim):
    blocks = jnp.moveaxis(blocks, 0, dim)
    dims = blocks.shape
    return blocks.reshape(*dims[:dim], dims[dim] * dims[dim + 1], *dims[dim + 2 :])


def copy_for_each(x, axis):
    copies = jnp.broadcast_to(x, (lax.axis_size(axis), *x.shape))
    return lax.all_to_all(copies, axis, split_axis=0, concat_axis=0, tiled=True)


def gather_directly(x, axis, dim):
    return laid_out(copy_for_each(x, axis), dim)


def of_everyone(x, axis):
    return copy_for_each(x, axis).sum(axis=0)


def cut_along(x, dim, size):
    dims = x.shape
    blocks = x.reshape(*dims[:dim], size, dims[dim] // size, *dims[dim + 1 :])
    return jnp.moveaxis(blocks, dim, 0)


def summed_on_arrival(x, axis, dim):
    blocks = cut_along(x, dim, lax.axis_size(axis))
    arrived = lax.all_to_all(blocks, axis, split_axis=0, concat_axis=0, tiled=True)
    return arrived.sum(axis=0)


def sent_and_summed(x, axis, dim):
    size = lax.axis_size(axis)
    blocks = lax.all_to_all(cut_along(x, dim, size), axis, 0, 0, tiled=True)
    return jnp.sum(blocks.astype(jnp.float32), axis=0)


def advance(state_in, pieces, lengths, base_log, gain_vec):
    seq_count = state_in.shape[0]
    head_count = state_in.shape[1]
    head_shape = (seq_count, NEW, head_count, HEAD)
    recept, keys, values, decay_pre, rate_pre, gate_pre = [
        piece.astype(jnp.float32).reshape(head_shape) for piece in pieces
    ]
    decays = jnp.exp(
        -jnp.exp(-jax.nn.softplus(-(base_log.reshape(head_count, HEAD) + decay_pre)) - 0.5)
    )
    rates = jax.nn.sigmoid(rate_pre)
    unit_keys = keys * lax.rsqrt(jnp.sum(keys * keys, -1, keepdims=True) + unit_epsilon)
    memory = state_in.reshape(seq_count, head_count, HEAD, HEAD)
    live_mask = jnp.arange(NEW)[None, :] < lengths[:, None]
    readings = []
    for position in range(NEW):
        unit_now = unit_keys[:, position]
        removed = jnp.einsum("shvk,shk->shv", memory, unit_now)
        updated = (
            memory * decays[:, position][:, :, None, :]
            - removed[..., None] * (unit_now * rates[:, position])[:, :, None, :]
            + values[:, position][..., None] * keys[:, position][:, :, None, :]
        )
        live_now = live_mask[:, position][:, None, None, None]
        memory = jnp.where(live_now, updated, memory)
        readings.append(jnp.einsum("shvk,shk->shv", memory, recept[:, position]))
    outputs_h = jnp.stack(readings, 1)
    head_mean = jnp.mean(outputs_h, -1, keepdims=True)
    head_var = jnp.mean(jnp.square(outputs_h - head_mean), -1, keepdims=True)
    normed = (
        (outputs_h - head_mean)
        * lax.rsqrt(head_var + group_epsilon)
        * gain_vec.reshape(head_count, HEAD)
    )
    mixed_out = normed * jax.nn.sigmoid(gate_pre) * live_mask[:, :, None, None].astype(jnp.float32)
    return (
        memory.reshape(state_in.shape),
        mixed_out.reshape(seq_count * NEW, head_count * HEAD).astype(jnp.bfloat16),
    )


def per_device(
    tokens,
    lengths,
    norm_gain,
    w_recept,
    w_keys,
    w_values,
    w_decay,
    w_rate,
    w_gate,
    decay_base,
    group_gain,
    w_out,
    states,
):
    gathered = gather_directly(tokens, "tp", 0)
    own_count = gathered.shape[0] // lax.axis_size("dp")
    row_start = lax.axis_index("dp") * own_count
    width_dev = w_recept.shape[2]
    own_rows = tokens
    new_states = []
    for layer_id in range(2):
        wide_rows = gathered.astype(jnp.float32)
        square = of_everyone(jnp.sum(wide_rows * wide_rows, -1), "dp")
        inv_rms = lax.rsqrt(
            lax.dynamic_slice_in_dim(square, row_start, own_count, 0) / D + norm_epsilon
        )[:, None]
        scaled = (wide_rows * norm_gain[layer_id]).astype(jnp.bfloat16)
        matrices = [
            matrix[layer_id] for matrix in (w_recept, w_keys, w_values, w_decay, w_rate, w_gate)
        ]

        def project():
            return jnp.concatenate(
                [
                    jnp.dot(scaled, matrix, preferred_element_type=jnp.float32)
                    for matrix in matrices
                ],
                1,
            )

        summed = summed_on_arrival(project(), "dp", 0)
        pieces = [
            (inv_rms * summed[:, role_id * width_dev : (role_id + 1) * width_dev]).astype(
                jnp.bfloat16
            )
            for role_id in range(6)
        ]
        memory, mixed_out = advance(
            states[layer_id], pieces, lengths, decay_base[layer_id], group_gain[layer_id]
        )
        new_states.append(memory)
        out_weight = w_out[layer_id]
        partial_value = jnp.dot(
            gather_directly(mixed_out, "dp", 0), out_weight, preferred_element_type=jnp.float32
        )
        shared_sum = sent_and_summed(partial_value.astype(jnp.bfloat16), "tp", 0)
        own_rows = (own_rows.astype(jnp.float32) + shared_sum).astype(jnp.bfloat16)
        if layer_id == 0:
            gathered = gather_directly(own_rows, "tp", 0)
    return (own_rows, jnp.stack(new_states))


def solution(mesh):
    placed = (
        P(("grp", "tp"), "dp"),
        P(("grp", "dp")),
        P(None, "dp"),
        P(None, "dp", "tp"),
        P(None, "dp", "tp"),
        P(None, "dp", "tp"),
        P(None, "dp", "tp"),
        P(None, "dp", "tp"),
        P(None, "dp", "tp"),
        P(None, "tp"),
        P(None, "tp"),
        P(None, "tp", "dp"),
        P(None, ("grp", "dp"), "tp", None),
    )
    return jax.shard_map(
        per_device,
        mesh=mesh,
        in_specs=placed,
        out_specs=(P(("grp", "tp"), "dp"), P(None, ("grp", "dp"), "tp", None)),
        check_vma=False,
    )
```

profile of v0, /device:TPU:80, one launch (start us, length us, event | category | flops | bytes accessed | tf_op | source)
XLA Modules:
  0.0 308.3 jit_solution(11342835664175332296)
XLA Ops:
  0.7 1.5 broadcast_in_dim.105
  2.2 43.7 %all-to-all-start = ((bf16[16,32,256]{2,1,0:T(8,128)(2,1)}), bf16[16,32,256]{2,1,0:T(8,128)(2,1)S(1)}, u32[]{:S(2)}, u32[]{:S(2)}) async-start(bf16[16,32,256]{2,1,0:T(8,128)(2,1)} %broadcast_in_dim.105), calls=%async_computation | async-start | bytes 524288 | tf_op jit(solution)/shard_map/all_to_all | solution.py:24
  45.9 1.3 fusion.97
  47.2 16.8 %all-to-all-done = bf16[16,32,256]{2,1,0:T(8,128)(2,1)S(1)} async-done(((bf16[16,32,256]{2,1,0:T(8,128)(2,1)}), bf16[16,32,256]{2,1,0:T(8,128)(2,1)S(1)}, u32[]{:S(2)}, u32[]{:S(2)}) %all-to-all-start) | async-done | bytes 262176 | tf_op jit(solution)/shard_map/all_to_all | solution.py:24
  64.9 7.6 %all-to-all-start.1 = ((f32[16,1,512]{2,1,0:T(1,128)}), f32[16,1,512]{2,1,0:T(1,128)S(1)}, u32[]{:S(2)}, u32[]{:S(2)}) async-start(f32[16,1,512]{2,1,0:T(1,128)} %broadcast_in_dim.107), calls=%async_computation.1 | async-start | bytes 65536 | tf_op jit(solution)/shard_map/all_to_all | solution.py:24
  72.5 1.1 convolution_dynamic-update-slice_fusion.11
  74.8 1.6 copy.40
  76.4 3.6 %all-to-all-done.1 = f32[16,1,512]{2,1,0:T(1,128)S(1)} async-done(((f32[16,1,512]{2,1,0:T(1,128)}), f32[16,1,512]{2,1,0:T(1,128)S(1)}, u32[]{:S(2)}, u32[]{:S(2)}) %all-to-all-start.1) | async-done | bytes 32800 | tf_op jit(solution)/shard_map/all_to_all | solution.py:24
  80.6 4.1 %all-to-all-start.2 = ((f32[16,32,768]{2,1,0:T(8,128)}), f32[16,32,768]{2,1,0:T(8,128)S(1)}, u32[]{:S(2)}, u32[]{:S(2)}) async-start(f32[16,32,768]{2,1,0:T(8,128)} %bitcast.8), calls=%async_computation.2 | async-start | bytes 3145728 | tf_op jit(solution)/shard_map/all_to_all | solution.py:43
  87.7 34.6 %all-to-all-done.2 = f32[16,32,768]{2,1,0:T(8,128)S(1)} async-done(((f32[16,32,768]{2,1,0:T(8,128)}), f32[16,32,768]{2,1,0:T(8,128)S(1)}, u32[]{:S(2)}, u32[]{:S(2)}) %all-to-all-start.2) | async-done | bytes 1572896 | tf_op jit(solution)/shard_map/all_to_all | solution.py:43
  124.6 1.3 broadcast_multiply_fusion.13
  126.4 1.4 broadcast_multiply_fusion.11
  129.6 13.3 %all_to_all.52 = bf16[16,32,128]{2,1,0:T(8,128)(2,1)S(1)} all-to-all(bf16[16,32,128]{2,1,0:T(8,128)(2,1)S(1)} %broadcast_in_dim.114), channel_id=1, replica_groups=mesh['grp'=2,'tp'=16,'dp'=16] {'dp'}, dimensions={0} | all-to-all | bytes 262144 | tf_op jit(solution)/shard_map/all_to_all | solution.py:24
  143.1 24.7 %all_to_all.53 = bf16[16,32,256]{2,1,0:T(8,128)(2,1)S(1)} all-to-all(bf16[16,32,256]{2,1,0:T(8,128)(2,1)S(1)} %bitcast.352), channel_id=1, replica_groups=mesh['grp'=2,'tp'=16,'dp'=16] {'tp'}, dimensions={0} | all-to-all | bytes 524288 | tf_op jit(solution)/shard_map/all_to_all | solution.py:49
  167.9 24.3 %all_to_all.54 = bf16[16,32,256]{2,1,0:T(8,128)(2,1)S(1)} all-to-all(bf16[16,32,256]{2,1,0:T(8,128)(2,1)S(1)} %broadcast_in_dim.115), channel_id=1, replica_groups=mesh['grp'=2,'tp'=16,'dp'=16] {'tp'}, dimensions={0} | all-to-all | bytes 524288 | tf_op jit(solution)/shard_map/all_to_all | solution.py:24
  193.1 4.5 %all-to-all-start.6 = ((f32[16,1,512]{2,1,0:T(1,128)}), f32[16,1,512]{2,1,0:T(1,128)}, u32[]{:S(2)}, u32[]{:S(2)}) async-start(f32[16,1,512]{2,1,0:T(1,128)} %broadcast_in_dim.117), calls=%async_computation.6 | async-start | bytes 65536 | tf_op jit(solution)/shard_map/all_to_all | solution.py:24
  198.8 1.1 convolution_dynamic-update-slice_fusion
  199.8 1.6 copy.46
  201.5 3.6 %all-to-all-done.6 = f32[16,1,512]{2,1,0:T(1,128)} async-done(((f32[16,1,512]{2,1,0:T(1,128)}), f32[16,1,512]{2,1,0:T(1,128)}, u32[]{:S(2)}, u32[]{:S(2)}) %all-to-all-start.6) | async-done | bytes 32800 | tf_op jit(solution)/shard_map/all_to_all | solution.py:24
  205.1 4.5 %all-to-all-start.7 = ((f32[16,32,768]{2,1,0:T(8,128)}), f32[16,32,768]{2,1,0:T(8,128)S(1)}, u32[]{:S(2)}, u32[]{:S(2)}) async-start(f32[16,32,768]{2,1,0:T(8,128)} %bitcast.77), calls=%async_computation.7 | async-start | bytes 3145728 | tf_op jit(solution)/shard_map/all_to_all | solution.py:43
  210.0 1.0 mul.937
  211.0 1.0 mul.933
  212.1 1.0 mul.929
  213.0 1.0 broadcast_multiply_fusion.8
  214.0 2.1 mul.944
  218.0 2.1 mul.935
  220.1 1.0 mul.936
  223.6 3.7 %add_select_fusion.7 = (f32[1,8,2,4096]{3,2,1,0:T(2,128)}, f32[1,8,2,4096]{3,2,1,0:T(2,128)S(1)}) fusion(f32[1,8,2,4096]{3,2,1,0:T(2,128)} %mul.944, f32[1,8,2,4096]{3,2,1,0:T(2,128)S(1)} %mul.943, f32[1,8,2,4096]{3,2,1,0:T(2,128)S(1)} %mul.941, f32[1,8,2,4096]{3,2,1,0:T(2,128)} %mul.940, f32[1,8,2,4096]{3,2,1,0:T(2,128)} %mul.939, ...), kind=kLoop, calls=%fused_computation.42 | loop fusion | flops 1048576 | bytes 4194336 | tf_op jit(solution)/shard_map/jit(_where)/select_n | solution.py:77
  228.5 18.3 %all-to-all-done.7 = f32[16,32,768]{2,1,0:T(8,128)S(1)} async-done(((f32[16,32,768]{2,1,0:T(8,128)}), f32[16,32,768]{2,1,0:T(8,128)S(1)}, u32[]{:S(2)}, u32[]{:S(2)}) %all-to-all-start.7) | async-done | bytes 1572896 | tf_op jit(solution)/shard_map/all_to_all | solution.py:43
  252.8 5.0 %all-to-all-start.8 = ((bf16[16,32,128]{2,1,0:T(8,128)(2,1)}), bf16[16,32,128]{2,1,0:T(8,128)(2,1)S(1)}, u32[]{:S(2)}, u32[]{:S(2)}) async-start(bf16[16,32,128]{2,1,0:T(8,128)(2,1)} %broadcast_in_dim.118), calls=%async_computation.8 | async-start | bytes 262144 | tf_op jit(solution)/shard_map/all_to_all | solution.py:24
  257.8 1.0 broadcast_multiply_fusion
  259.7 1.3 mul.957
  261.0 1.5 mul.897
  262.5 2.0 mul.953
  264.5 1.5 mul.885
  266.1 2.0 mul.949
  268.1 1.5 mul.866
  269.6 2.0 mul.945
  271.6 2.0 mul.960
  273.6 1.0 mul.947
  277.5 1.0 mul.955
  279.4 1.0 broadcast_multiply_fusion.1
  280.4 1.0 mul.959
  281.4 1.8 convolution_convert_fusion
  283.1 6.2 %all-to-all-start.9 = ((bf16[16,32,256]{2,1,0:T(8,128)(2,1)}), bf16[16,32,256]{2,1,0:T(8,128)(2,1)S(1)}, u32[]{:S(2)}, u32[]{:S(2)}) async-start(bf16[16,32,256]{2,1,0:T(8,128)(2,1)} %bitcast.137), calls=%async_computation.9 | async-start | bytes 524288 | tf_op jit(solution)/shard_map/all_to_all | solution.py:49
  289.4 2.4 add_select_fusion.6
  291.8 1.0 pad_maximum_fusion
  292.9 14.8 %all-to-all-done.9 = bf16[16,32,256]{2,1,0:T(8,128)(2,1)S(1)} async-done(((bf16[16,32,256]{2,1,0:T(8,128)(2,1)}), bf16[16,32,256]{2,1,0:T(8,128)(2,1)S(1)}, u32[]{:S(2)}, u32[]{:S(2)}) %all-to-all-start.9) | async-done | bytes 262176 | tf_op jit(solution)/shard_map/all_to_all | solution.py:49
  (255 shorter events, 29.2 us)
Async XLA Ops:
  0.6 72.9 %copy-start.15 = (bf16[2,256,128]{2,1,0:T(8,128)(2,1)S(1)}, bf16[2,256,128]{2,1,0:T(8,128)(2,1)}, u32[]{:S(2)}) copy-start(bf16[2,256,128]{2,1,0:T(8,128)(2,1)} %param.17) | copy-start | bytes 393220
  0.6 73.2 %copy-start.16 = (bf16[2,256,128]{2,1,0:T(8,128)(2,1)S(1)}, bf16[2,256,128]{2,1,0:T(8,128)(2,1)}, u32[]{:S(2)}) copy-start(bf16[2,256,128]{2,1,0:T(8,128)(2,1)} %param.18) | copy-start | bytes 393220
  0.7 73.4 %copy-start.18 = (bf16[2,256,128]{2,1,0:T(8,128)(2,1)S(1)}, bf16[2,256,128]{2,1,0:T(8,128)(2,1)}, u32[]{:S(2)}) copy-start(bf16[2,256,128]{2,1,0:T(8,128)(2,1)} %param.19) | copy-start | bytes 393220
  2.2 61.8 %all-to-all-start = ((bf16[16,32,256]{2,1,0:T(8,128)(2,1)}), bf16[16,32,256]{2,1,0:T(8,128)(2,1)S(1)}, u32[]{:S(2)}, u32[]{:S(2)}) async-start(bf16[16,32,256]{2,1,0:T(8,128)(2,1)} %broadcast_in_dim.105), calls=%async_computation | async-start | bytes 524288 | tf_op jit(solution)/shard_map/all_to_all | solution.py:24
  45.9 28.4 %copy-start.20 = (bf16[2,256,128]{2,1,0:T(8,128)(2,1)S(1)}, bf16[2,256,128]{2,1,0:T(8,128)(2,1)}, u32[]{:S(2)}) copy-start(bf16[2,256,128]{2,1,0:T(8,128)(2,1)} %param.20) | copy-start | bytes 393220
  64.1 10.4 %copy-start.22 = (bf16[2,256,128]{2,1,0:T(8,128)(2,1)S(1)}, bf16[2,256,128]{2,1,0:T(8,128)(2,1)}, u32[]{:S(2)}) copy-start(bf16[2,256,128]{2,1,0:T(8,128)(2,1)} %param.21) | copy-start | bytes 393220
  64.9 15.1 %all-to-all-start.1 = ((f32[16,1,512]{2,1,0:T(1,128)}), f32[16,1,512]{2,1,0:T(1,128)S(1)}, u32[]{:S(2)}, u32[]{:S(2)}) async-start(f32[16,1,512]{2,1,0:T(1,128)} %broadcast_in_dim.107), calls=%async_computation.1 | async-start | bytes 65536 | tf_op jit(solution)/shard_map/all_to_all | solution.py:24
  80.0 4.8 %copy-start.62 = (f32[2,128]{1,0:T(2,128)S(1)}, f32[2,128]{1,0:T(2,128)}, u32[]{:S(2)}) copy-start(f32[2,128]{1,0:T(2,128)} %param.22) | copy-start | bytes 3076
  80.0 5.5 %copy-start.65 = (s32[8]{0:T(128)S(1)}, s32[8]{0:T(128)}, u32[]{:S(2)}) copy-start(s32[8]{0:T(128)} %param.14) | copy-start | bytes 100
  80.0 5.6 %slice-start = ((f32[2,8,2,4096]{3,2,1,0:T(2,128)}), f32[1,8,2,4096]{3,2,1,0:T(2,128)S(1)}, s32[]{:S(2)}) async-start(f32[2,8,2,4096]{3,2,1,0:T(2,128)} %param.25), calls=%async_computation.10 | async-start | bytes 524288 | tf_op jit(solution)/shard_map/slice | solution.py:143
  80.0 6.2 %copy-start.63 = (f32[2,128]{1,0:T(2,128)S(1)}, f32[2,128]{1,0:T(2,128)}, u32[]{:S(2)}) copy-start(f32[2,128]{1,0:T(2,128)} %param.23) | copy-start | bytes 3076
  80.6 41.7 %all-to-all-start.2 = ((f32[16,32,768]{2,1,0:T(8,128)}), f32[16,32,768]{2,1,0:T(8,128)S(1)}, u32[]{:S(2)}, u32[]{:S(2)}) async-start(f32[16,32,768]{2,1,0:T(8,128)} %bitcast.8), calls=%async_computation.2 | async-start | bytes 3145728 | tf_op jit(solution)/shard_map/all_to_all | solution.py:43
  85.6 43.8 %copy-start.53 = (f32[32]{0:T(128)}, f32[32]{0:T(128)S(1)}, u32[]{:S(2)}) copy-start(f32[32]{0:T(128)S(1)} %reshape.764) | copy-start | bytes 388
  86.2 37.5 %copy-start.51 = (pred[8]{0:T(512)(128)(4,1)}, pred[8]{0:T(512)(128)(4,1)S(1)}, u32[]{:S(2)}) copy-start(pred[8]{0:T(512)(128)(4,1)S(1)} %get-tuple-element.7) | copy-start | bytes 28
  86.2 38.4 %copy-start.49 = (pred[8]{0:T(512)(128)(4,1)}, pred[8]{0:T(512)(128)(4,1)S(1)}, u32[]{:S(2)}) copy-start(pred[8]{0:T(512)(128)(4,1)S(1)} %get-tuple-element.6) | copy-start | bytes 28
  86.2 40.3 %copy-start.47 = (pred[8]{0:T(512)(128)(4,1)}, pred[8]{0:T(512)(128)(4,1)S(1)}, u32[]{:S(2)}) copy-start(pred[8]{0:T(512)(128)(4,1)S(1)} %get-tuple-element.5) | copy-start | bytes 28
  86.2 42.1 %copy-start.55 = (pred[8]{0:T(512)(128)(4,1)}, pred[8]{0:T(512)(128)(4,1)S(1)}, u32[]{:S(2)}) copy-start(pred[8]{0:T(512)(128)(4,1)S(1)} %get-tuple-element.4) | copy-start | bytes 28
  87.7 34.8 %copy-start.58 = (f32[32]{0:T(128)}, f32[32]{0:T(128)S(1)}, u32[]{:S(2)}) copy-start(f32[32]{0:T(128)S(1)} %add_rsqrt_fusion.5) | copy-start | bytes 388
  123.0 5.2 %copy-start.40 = (f32[8,2,64]{2,1,0:T(2,128)}, f32[8,2,64]{2,1,0:T(2,128)S(1)}, u32[]{:S(2)}) copy-start(f32[8,2,64]{2,1,0:T(2,128)S(1)} %get-tuple-element.56) | copy-start | bytes 12292
  123.1 5.2 %copy-start.42 = (f32[8,2,64]{2,1,0:T(2,128)}, f32[8,2,64]{2,1,0:T(2,128)S(1)}, u32[]{:S(2)}) copy-start(f32[8,2,64]{2,1,0:T(2,128)S(1)} %get-tuple-element.103) | copy-start | bytes 12292
  123.2 5.1 %copy-start.38 = (f32[8,2,64]{2,1,0:T(2,128)}, f32[8,2,64]{2,1,0:T(2,128)S(1)}, u32[]{:S(2)}) copy-start(f32[8,2,64]{2,1,0:T(2,128)S(1)} %get-tuple-element.32) | copy-start | bytes 12292
  123.5 4.8 %copy-start.45 = (f32[8,2,64]{2,1,0:T(2,128)}, f32[8,2,64]{2,1,0:T(2,128)S(1)}, u32[]{:S(2)}) copy-start(f32[8,2,64]{2,1,0:T(2,128)S(1)} %get-tuple-element.64) | copy-start | bytes 12292
  127.8 15.1 %copy-start.23 = (bf16[2,128,256]{2,1,0:T(8,128)(2,1)S(1)}, bf16[2,128,256]{2,1,0:T(8,128)(2,1)}, u32[]{:S(2)}) copy-start(bf16[2,128,256]{2,1,0:T(8,128)(2,1)} %param.24) | copy-start | bytes 393220
  128.3 39.5 %copy-start.34 = (bf16[32,256]{1,0:T(8,128)(2,1)S(1)}, bf16[32,256]{1,0:T(8,128)(2,1)}, u32[]{:S(2)}) copy-start(bf16[32,256]{1,0:T(8,128)(2,1)} %param.13) | copy-start | bytes 49156
  128.8 63.4 %copy-start.57 = (f32[1,256]{1,0:T(1,128)S(1)}, f32[1,256]{1,0:T(1,128)}, u32[]{:S(2)}) copy-start(f32[1,256]{1,0:T(1,128)} %get-tuple-element.94) | copy-start | bytes 3076
  129.5 68.0 %copy-start.14 = (bf16[2,256,128]{2,1,0:T(8,128)(2,1)S(1)}, bf16[2,256,128]{2,1,0:T(8,128)(2,1)}, u32[]{:S(2)}) copy-start(bf16[2,256,128]{2,1,0:T(8,128)(2,1)} %param.16) | copy-start | bytes 393220
  167.8 30.3 %copy-start.17 = (bf16[2,256,128]{2,1,0:T(8,128)(2,1)S(1)}, bf16[2,256,128]{2,1,0:T(8,128)(2,1)}, u32[]{:S(2)}) copy-start(bf16[2,256,128]{2,1,0:T(8,128)(2,1)} %param.18) | copy-start | bytes 393220
  167.8 30.5 %copy-start.19 = (bf16[2,256,128]{2,1,0:T(8,128)(2,1)S(1)}, bf16[2,256,128]{2,1,0:T(8,128)(2,1)}, u32[]{:S(2)}) copy-start(bf16[2,256,128]{2,1,0:T(8,128)(2,1)} %param.19) | copy-start | bytes 393220
  192.2 6.3 %copy-start.21 = (bf16[2,256,128]{2,1,0:T(8,128)(2,1)S(1)}, bf16[2,256,128]{2,1,0:T(8,128)(2,1)}, u32[]{:S(2)}) copy-start(bf16[2,256,128]{2,1,0:T(8,128)(2,1)} %param.20) | copy-start | bytes 393220
  193.1 12.0 %all-to-all-start.6 = ((f32[16,1,512]{2,1,0:T(1,128)}), f32[16,1,512]{2,1,0:T(1,128)}, u32[]{:S(2)}, u32[]{:S(2)}) async-start(f32[16,1,512]{2,1,0:T(1,128)} %broadcast_in_dim.117), calls=%async_computation.6 | async-start | bytes 65536 | tf_op jit(solution)/shard_map/all_to_all | solution.py:24
  205.1 4.6 %copy-start.46 = (f32[8,2,64]{2,1,0:T(2,128)S(1)}, f32[8,2,64]{2,1,0:T(2,128)}, u32[]{:S(2)}) copy-start(f32[8,2,64]{2,1,0:T(2,128)} %copy-done.45) | copy-start | bytes 12292
  205.1 4.9 %copy-start.30 = (f32[8,2,64]{2,1,0:T(2,128)S(1)}, f32[8,2,64]{2,1,0:T(2,128)}, u32[]{:S(2)}) copy-start(f32[8,2,64]{2,1,0:T(2,128)} %copy-done.29) | copy-start | bytes 12292
  205.1 41.7 %all-to-all-start.7 = ((f32[16,32,768]{2,1,0:T(8,128)}), f32[16,32,768]{2,1,0:T(8,128)S(1)}, u32[]{:S(2)}, u32[]{:S(2)}) async-start(f32[16,32,768]{2,1,0:T(8,128)} %bitcast.77), calls=%async_computation.7 | async-start | bytes 3145728 | tf_op jit(solution)/shard_map/all_to_all | solution.py:43
  214.0 6.1 %copy-start = (f32[8,2,64,64]{3,2,1,0:T(8,128)S(1)}, f32[8,2,64,64]{3,2,1,0:T(8,128)}, u32[]{:S(2)}) copy-start(f32[8,2,64,64]{3,2,1,0:T(8,128)} %get-tuple-element.73) | copy-start | bytes 786436
  217.1 5.0 %copy-start.1 = (f32[8,2,64,64]{3,2,1,0:T(8,128)S(1)}, f32[8,2,64,64]{3,2,1,0:T(8,128)}, u32[]{:S(2)}) copy-start(f32[8,2,64,64]{3,2,1,0:T(8,128)} %get-tuple-element.76) | copy-start | bytes 786436
  218.0 5.0 %copy-start.36 = (f32[8,2,1,64]{3,2,1,0:T(1,128)S(1)}, f32[8,2,1,64]{3,2,1,0:T(1,128)}, u32[]{:S(2)}) copy-start(f32[8,2,1,64]{3,2,1,0:T(1,128)} %copy-done.35) | copy-start | bytes 12292
  218.0 5.0 %copy-start.39 = (f32[8,2,64]{2,1,0:T(2,128)S(1)}, f32[8,2,64]{2,1,0:T(2,128)}, u32[]{:S(2)}) copy-start(f32[8,2,64]{2,1,0:T(2,128)} %copy-done.38) | copy-start | bytes 12292
  252.8 28.6 %all-to-all-start.8 = ((bf16[16,32,128]{2,1,0:T(8,128)(2,1)}), bf16[16,32,128]{2,1,0:T(8,128)(2,1)S(1)}, u32[]{:S(2)}, u32[]{:S(2)}) async-start(bf16[16,32,128]{2,1,0:T(8,128)(2,1)} %broadcast_in_dim.118), calls=%async_computation.8 | async-start | bytes 262144 | tf_op jit(solution)/shard_map/all_to_all | solution.py:24
  278.4 10.9 %copy-start.4 = (f32[2,8,2,4096]{3,2,1,0:T(2,128)S(1)}, f32[2,8,2,4096]{3,2,1,0:T(2,128)}, u32[]{:S(2)}) copy-start(f32[2,8,2,4096]{3,2,1,0:T(2,128)} %param.25) | copy-start | bytes 1572868
  278.4 10.9 %copy-start.5 = (f32[1,8,2,4096]{3,2,1,0:T(2,128)S(1)}, f32[1,8,2,4096]{3,2,1,0:T(2,128)}, u32[]{:S(2)}) copy-start(f32[1,8,2,4096]{3,2,1,0:T(2,128)} %mul.953) | copy-start | bytes 786436
  278.4 10.9 %copy-start.6 = (f32[1,8,2,4096]{3,2,1,0:T(2,128)S(1)}, f32[1,8,2,4096]{3,2,1,0:T(2,128)}, u32[]{:S(2)}) copy-start(f32[1,8,2,4096]{3,2,1,0:T(2,128)} %mul.949) | copy-start | bytes 786436
  278.4 10.9 %copy-start.7 = (f32[1,8,2,4096]{3,2,1,0:T(2,128)S(1)}, f32[1,8,2,4096]{3,2,1,0:T(2,128)}, u32[]{:S(2)}) copy-start(f32[1,8,2,4096]{3,2,1,0:T(2,128)} %mul.945) | copy-start | bytes 786436
  278.4 10.9 %copy-start.8 = (f32[1,8,2,4096]{3,2,1,0:T(2,128)S(1)}, f32[1,8,2,4096]{3,2,1,0:T(2,128)}, u32[]{:S(2)}) copy-start(f32[1,8,2,4096]{3,2,1,0:T(2,128)} %mul.960) | copy-start | bytes 786436
  278.5 10.9 %copy-start.9 = (f32[1,8,2,4096]{3,2,1,0:T(2,128)S(1)}, f32[1,8,2,4096]{3,2,1,0:T(2,128)}, u32[]{:S(2)}) copy-start(f32[1,8,2,4096]{3,2,1,0:T(2,128)} %mul.947) | copy-start | bytes 786436
  278.5 10.9 %copy-start.10 = (f32[1,8,2,4096]{3,2,1,0:T(2,128)S(1)}, f32[1,8,2,4096]{3,2,1,0:T(2,128)}, u32[]{:S(2)}) copy-start(f32[1,8,2,4096]{3,2,1,0:T(2,128)} %mul.948) | copy-start | bytes 786436
  279.4 10.0 %copy-start.11 = (f32[1,8,2,4096]{3,2,1,0:T(2,128)S(1)}, f32[1,8,2,4096]{3,2,1,0:T(2,128)}, u32[]{:S(2)}) copy-start(f32[1,8,2,4096]{3,2,1,0:T(2,128)} %mul.955) | copy-start | bytes 786436
  279.4 10.0 %copy-start.12 = (f32[1,8,2,4096]{3,2,1,0:T(2,128)S(1)}, f32[1,8,2,4096]{3,2,1,0:T(2,128)}, u32[]{:S(2)}) copy-start(f32[1,8,2,4096]{3,2,1,0:T(2,128)} %mul.956) | copy-start | bytes 786436
  283.1 24.5 %all-to-all-start.9 = ((bf16[16,32,256]{2,1,0:T(8,128)(2,1)}), bf16[16,32,256]{2,1,0:T(8,128)(2,1)S(1)}, u32[]{:S(2)}, u32[]{:S(2)}) async-start(bf16[16,32,256]{2,1,0:T(8,128)(2,1)} %bitcast.137), calls=%async_computation.9 | async-start | bytes 524288 | tf_op jit(solution)/shard_map/all_to_all | solution.py:49
  (26 other events, 53.1 us)
where the time goes:
time: 310 us; the launch traced here: 308 us
  waiting for transfers between devices  91.7 us (30%)
  starting transfers between devices  75.6 us (24%)
  blocking collectives  62.3 us (20%)
  local copies, waits for them, and re-layouts  46.6 us (15%)
  other arithmetic  19.7 us (6%)
  matrix products  10.6 us (3%)
    all_to_all x4, starting transfers between devices, copy_for_each(): return lax.all_to_all(copies, axis, split_axis=0, concat_axis=0, tiled=True)  60.9 us
    all_to_all x2, waiting for transfers between devices, summed_on_arrival(): lax.all_to_all(blocks, axis, split_axis=0, concat_axis=0, tiled=True)  53 us
    all_to_all x2, blocking collectives, copy_for_each(): return lax.all_to_all(copies, axis, split_axis=0, concat_axis=0, tiled=True)  37.6 us
    all_to_all x1, blocking collectives, sent_and_summed(): blocks = lax.all_to_all(cut_along(x, dim, size), axis, 0, 0, tiled=True)  24.7 us
    all_to_all x4, waiting for transfers between devices, copy_for_each(): return lax.all_to_all(copies, axis, split_axis=0, concat_axis=0, tiled=True)  23.9 us
    mul x18, local copies, waits for them, and re-layouts, advance(): memory * decays[:, position][:, :, None, :]  16.1 us
    all_to_all x1, waiting for transfers between devices, sent_and_summed(): blocks = lax.all_to_all(cut_along(x, dim, size), axis, 0, 0, tiled=True)  14.8 us
    mul x11, local copies, waits for them, and re-layouts, advance(): values[:, position][..., None] * keys[:, position][:, :, None, :]  9.89 us
  transfers between devices with their start and end apart: 7, of which 6 were waited for; matrix products, arithmetic and copies ran while one was open for 19% of the time, Pallas kernels for 0%

commit v1 on v0

v1 whole, which is shorter than its diff:
```python
import functools

import jax
import jax.numpy as jnp
from jax import lax
from jax.experimental import pallas as pl
from jax.experimental.pallas import tpu as pltpu
from jax.sharding import PartitionSpec as P

HEAD = 64
NEW = 4
LANES = 128

norm_epsilon = 1e-06
unit_epsilon = 0.00064
group_epsilon = 0.00064

VMEM = pl.BlockSpec(memory_space=pltpu.VMEM)
SMEM = pl.BlockSpec(memory_space=pltpu.SMEM)


def iota(shape, dim):
    return lax.broadcasted_iota(jnp.int32, shape, dim)


def split_dot(x, ones):
    high = x.astype(jnp.bfloat16)
    low = (x - high.astype(jnp.float32)).astype(jnp.bfloat16)
    return jnp.dot(high, ones, preferred_element_type=jnp.float32) + jnp.dot(
        low, ones, preferred_element_type=jnp.float32
    )


def project_kernel(layer, rows, x_ref, gain_ref, *refs):
    *weight_refs, out_ref = refs
    owners, _, depth = x_ref.shape
    x = x_ref[...].reshape(owners * rows, depth).astype(jnp.float32)
    scaled = (x * gain_ref[layer : layer + 1, :]).astype(jnp.bfloat16)
    for first in range(0, 6, 2):
        pair = jnp.concatenate([weight_refs[first][layer], weight_refs[first + 1][layer]], 1)
        product = jnp.dot(scaled, pair, preferred_element_type=jnp.float32).astype(jnp.bfloat16)
        for half in range(2):
            out_ref[:, pl.ds((first + half) * rows, rows), :] = product[
                :, half * LANES : (half + 1) * LANES
            ].reshape(owners, rows, LANES)
    squares = jnp.sum(x * x, -1, keepdims=True)
    eye = iota((rows, LANES), 0) == iota((rows, LANES), 1)
    pick = iota((8, LANES), 0)
    for owner in range(owners):
        row = jnp.sum(
            jnp.where(eye, squares[owner * rows : (owner + 1) * rows], 0.0), 0, keepdims=True
        )
        high = row.astype(jnp.bfloat16).astype(jnp.float32)
        tail = jnp.where(pick == 0, high, jnp.where(pick == 1, row - high, 0.0))
        out_ref[owner, pl.ds(6 * rows, 8), :] = tail.astype(jnp.bfloat16)


def advance_kernel(layer, rows, width, arrived_ref, lengths_ref, base_ref, gain_ref, state_ref, *refs):
    mixed_ref, new_ref, line_ref, read_ref = refs[-4:]
    seqs = rows // NEW
    total = jnp.sum(arrived_ref[...].astype(jnp.float32), 0)
    eye = iota((rows, LANES), 0) == iota((rows, LANES), 1)
    square = total[6 * rows : 6 * rows + 1] + total[6 * rows + 1 : 6 * rows + 2]
    square = jnp.sum(jnp.where(eye, square, 0.0), 1, keepdims=True)
    inv_rms = lax.rsqrt(square / width + norm_epsilon)
    recept, keys, values, decay_pre, rate_pre, gate_pre = [
        (inv_rms * total[role * rows : (role + 1) * rows]).astype(jnp.bfloat16).astype(jnp.float32)
        for role in range(6)
    ]
    same_head = (iota((LANES, LANES), 0) // HEAD == iota((LANES, LANES), 1) // HEAD).astype(
        jnp.float32
    ).astype(jnp.bfloat16)
    log_rate = base_ref[layer : layer + 1, :] + decay_pre
    decays = jnp.exp(jax.nn.sigmoid(log_rate) * (-0.6065306597126334))
    rates = jax.nn.sigmoid(rate_pre)
    unit = keys * lax.rsqrt(split_dot(keys * keys, same_head) + unit_epsilon)
    slot = iota((rows, LANES), 0)
    limit = jnp.zeros((rows, LANES), jnp.int32)
    for seq in range(seqs):
        limit = jnp.where(slot // NEW == seq, lengths_ref[seq], limit)
    live = slot % NEW < limit
    decays = jnp.where(live, decays, 1.0)
    unit = jnp.where(live, unit, 0.0)
    keys = jnp.where(live, keys, 0.0)
    lane = iota((rows, LANES), 1)
    for place, line in enumerate((decays, unit, unit * rates, keys, recept)):
        turned = pltpu.roll(line, HEAD, 1)
        line_ref[2 * place] = jnp.where(lane < HEAD, line, turned)
        line_ref[2 * place + 1] = jnp.where(lane < HEAD, turned, line)
    line_ref[10] = values
    even = iota((8, LANES), 0) % 2 == 0
    block_row, block_lane = iota((HEAD, LANES), 0), iota((HEAD, LANES), 1)
    place_mask = (block_row % 2 == block_lane // HEAD) & (block_row // 2 == block_lane % HEAD // 2)
    parity = (iota((LANES, LANES), 0) % 2 == iota((LANES, LANES), 1) // HEAD).astype(
        jnp.float32
    ).astype(jnp.bfloat16)
    parity_back = (iota((LANES, LANES), 1) % 2 == iota((LANES, LANES), 0) // HEAD).astype(
        jnp.float32
    ).astype(jnp.bfloat16)

    def spread(place, token):
        return jnp.where(
            even, line_ref[2 * place, pl.ds(token, 1), :], line_ref[2 * place + 1, pl.ds(token, 1), :]
        )[None]

    state = [
        state_ref[pl.ds(seq * HEAD, HEAD), :].reshape(8, 8, LANES) for seq in range(seqs)
    ]
    for position in range(NEW):
        tokens = [seq * NEW + position for seq in range(seqs)]
        against = jnp.concatenate(
            [(s * spread(1, t)).reshape(HEAD, LANES) for s, t in zip(state, tokens)], 0
        )
        removed = split_dot(against, same_head)
        written = jnp.concatenate(
            [jnp.where(place_mask, line_ref[10, pl.ds(t, 1), :], 0.0) for t in tokens], 0
        ).astype(jnp.bfloat16)
        written = jnp.dot(written, parity, preferred_element_type=jnp.float32)
        for seq, t in enumerate(tokens):
            part = slice(seq * HEAD, (seq + 1) * HEAD)
            state[seq] = (
                state[seq] * spread(0, t)
                - removed[part].reshape(8, 8, LANES) * spread(2, t)
                + written[part].reshape(8, 8, LANES) * spread(3, t)
            )
        read = jnp.concatenate(
            [(s * spread(4, t)).reshape(HEAD, LANES) for s, t in zip(state, tokens)], 0
        )
        read = split_dot(read, parity_back)
        for seq, t in enumerate(tokens):
            part = slice(seq * HEAD, (seq + 1) * HEAD)
            read_ref[pl.ds(t, 1), :] = jnp.sum(
                jnp.where(place_mask, read[part], 0.0), 0, keepdims=True
            )
    for seq in range(seqs):
        new_ref[0, pl.ds(seq * HEAD, HEAD), :] = state[seq].reshape(HEAD, LANES)
    read = read_ref[...]
    centred = read - split_dot(read, same_head) / HEAD
    variance = split_dot(centred * centred, same_head) / HEAD
    normed = centred * lax.rsqrt(variance + group_epsilon) * gain_ref[layer : layer + 1, :]
    mixed_ref[...] = jnp.where(live, normed * jax.nn.sigmoid(gate_pre), 0.0).astype(jnp.bfloat16)


def project(layer, x, gain, weights):
    owners, rows, _ = x.shape
    return pl.pallas_call(
        functools.partial(project_kernel, layer, rows),
        out_shape=jax.ShapeDtypeStruct((owners, 6 * rows + 8, LANES), jnp.bfloat16),
        in_specs=[VMEM] * 8,
        out_specs=VMEM,
        compiler_params=pltpu.CompilerParams(vmem_limit_bytes=24 * 2**20),
        cost_estimate=pl.CostEstimate(flops=2 * 10**8, bytes_accessed=2 * 10**6, transcendentals=0),
    )(x, gain, *weights)


def advance(layer, width, arrived, lengths, base, gain, states, held):
    rows = lengths.shape[0] * NEW
    state_rows = states.shape[1]
    block = pl.BlockSpec((1, state_rows, LANES), lambda i: (layer, 0, 0))
    in_block = pl.BlockSpec((None, state_rows, LANES), lambda i: (layer, 0, 0))
    operands = [arrived, lengths, base, gain, states]
    in_specs = [VMEM, SMEM, VMEM, VMEM, in_block]
    aliases = {}
    if held is not None:
        aliases = {len(operands): 1}
        operands.append(held)
        in_specs.append(pl.BlockSpec(memory_space=pl.ANY))
    return pl.pallas_call(
        functools.partial(advance_kernel, layer, rows, width),
        grid=(1,),
        out_shape=(
            jax.ShapeDtypeStruct((rows, LANES), jnp.bfloat16),
            jax.ShapeDtypeStruct(states.shape, jnp.float32),
        ),
        in_specs=in_specs,
        out_specs=(pl.BlockSpec((rows, LANES), lambda i: (0, 0)), block),
        scratch_shapes=[
            pltpu.VMEM((11, rows, LANES), jnp.float32),
            pltpu.VMEM((rows, LANES), jnp.float32),
        ],
        input_output_aliases=aliases,
        compiler_params=pltpu.CompilerParams(vmem_limit_bytes=24 * 2**20),
        cost_estimate=pl.CostEstimate(flops=2 * 10**8, bytes_accessed=2 * 10**6, transcendentals=0),
    )(*operands)


def gather_blocks(x, axis):
    copies = jnp.broadcast_to(x, (lax.axis_size(axis), *x.shape))
    return lax.all_to_all(copies, axis, split_axis=0, concat_axis=0, tiled=True)


def per_device(
    tokens,
    lengths,
    norm_gain,
    w_recept,
    w_keys,
    w_values,
    w_decay,
    w_rate,
    w_gate,
    decay_base,
    group_gain,
    w_out,
    states,
):
    weights = (w_recept, w_keys, w_values, w_decay, w_rate, w_gate)
    own_count, depth = tokens.shape
    width = depth * lax.axis_size("dp")
    blocks, seqs, heads, _ = states.shape
    folded = states.reshape(blocks, seqs, heads, HEAD // 2, LANES)
    folded = jnp.swapaxes(folded, 2, 3).reshape(blocks, seqs * HEAD, LANES)
    own_rows = tokens
    held = None
    for layer in range(2):
        gathered = gather_blocks(own_rows, "tp")
        partial_sums = project(layer, gathered, norm_gain, weights)
        arrived = lax.all_to_all(partial_sums, "dp", 0, 0, tiled=True)
        mixed, held = advance(
            layer, width, arrived, lengths, decay_base, group_gain, folded, held
        )
        everyone = gather_blocks(mixed, "dp")
        product = jnp.dot(
            everyone.reshape(-1, LANES), w_out[layer], preferred_element_type=jnp.float32
        )
        product = product.astype(jnp.bfloat16).reshape(-1, own_count, depth)
        summed = lax.all_to_all(product, "tp", 0, 0, tiled=True)
        own_rows = (
            own_rows.astype(jnp.float32) + jnp.sum(summed.astype(jnp.float32), 0)
        ).astype(jnp.bfloat16)
    new_states = jnp.swapaxes(held.reshape(blocks, seqs, HEAD // 2, heads, LANES), 2, 3)
    return (own_rows, new_states.reshape(states.shape))


def solution(mesh):
    placed = (
        P(("grp", "tp"), "dp"),
        P(("grp", "dp")),
        P(None, "dp"),
        P(None, "dp", "tp"),
        P(None, "dp", "tp"),
        P(None, "dp", "tp"),
        P(None, "dp", "tp"),
        P(None, "dp", "tp"),
        P(None, "dp", "tp"),
        P(None, "tp"),
        P(None, "tp"),
        P(None, "tp", "dp"),
        P(None, ("grp", "dp"), "tp", None),
    )
    return jax.shard_map(
        per_device,
        mesh=mesh,
        in_specs=placed,
        out_specs=(P(("grp", "tp"), "dp"), P(None, ("grp", "dp"), "tp", None)),
        check_vma=False,
    )
```

time: 310 us -> 226 us (0.73)
  blocking collectives: 62.3 us -> 215 us
  waiting for transfers between devices: 91.7 us -> 0 us
  starting transfers between devices: 75.6 us -> 0 us
  local copies, waits for them, and re-layouts: 46.6 us -> 2.24 us
  other arithmetic: 19.7 us -> 0.7 us
  matrix products: 10.6 us -> 0.41 us
  Pallas kernels: 0 us -> 6.31 us
    all_to_all x3 -> x8, blocking collectives: 62.3 us -> 215 us  [the longest x4 110 us: gather_blocks(): return lax.all_to_all(copies, axis, split_axis=0, concat_axis=0, tiled=True)]
    all_to_all x7 -> x0, waiting for transfers between devices: 91.7 us -> none  [the longest x2 53 us: summed_on_arrival(): lax.all_to_all(blocks, axis, split_axis=0, concat_axis=0, tiled=True)]
    all_to_all x7 -> x0, starting transfers between devices: 75.6 us -> none  [the longest x4 60.9 us: copy_for_each(): return lax.all_to_all(copies, axis, split_axis=0, concat_axis=0, tiled=True)]
    mul x40 -> x0, local copies, waits for them, and re-layouts: 34.9 us -> none  [the longest x18 16.1 us: advance(): memory * decays[:, position][:, :, None, :]]
    dot_general x30 -> x2, matrix products: 10.6 us -> 0.41 us  [per_device(): jnp.dot(everyone.reshape(-1, LANES), w_out[layer], preferred_element_type...]
    mul x16 -> x0, other arithmetic: 7.97 us -> none  [the longest x8 5.48 us: advance(): removed[..., None] * (unit_now * rates[:, position])[:, :, None, :]]
    pallas_call x0 -> x4, Pallas kernels: none -> 6.31 us  [the longest x2 5.54 us: advance(): pl.pallas_call(functools.partial(advance_kernel, layer, rows, width), gri...]
    select_n x2 -> x0, other arithmetic: 6.09 us -> none  [advance(): memory = jnp.where(live_now, updated, memory)]
  transfers between devices with their start and end apart: 7 -> 0, of which waited for: 6 -> 0; matrix products, arithmetic and copies ran while one was open for 19% -> 0% of each run, Pallas kernels for 0% -> 0%
where the time goes in v1:
time: 226 us
  blocking collectives  215 us (95%)
  Pallas kernels  6.31 us (3%)
    all_to_all x4, blocking collectives, gather_blocks(): return lax.all_to_all(copies, axis, split_axis=0, concat_axis=0, tiled=True)  110 us
    all_to_all x2, blocking collectives, per_device(): arrived = lax.all_to_all(partial_sums, 'dp', 0, 0, tiled=True)  56 us
    all_to_all x2, blocking collectives, per_device(): summed = lax.all_to_all(product, 'tp', 0, 0, tiled=True)  49.4 us
    pallas_call x2, Pallas kernels, advance(): pl.pallas_call(functools.partial(advance_kernel, layer, rows, width), gri...  5.54 us

profile of v1, /device:TPU:80, one launch (start us, length us, event | category | flops | bytes accessed | tf_op | source)
XLA Modules:
  0.0 225.9 jit_solution(3580625944452431898)
XLA Ops:
  0.6 0.0 copy-start.5
  0.6 0.0 copy-start.6
  0.7 0.0 copy-start.7
  0.7 0.8 broadcast_in_dim.12
  1.4 0.0 copy-start.1
  1.5 0.0 copy-start.2
  1.5 0.0 copy-start.3
  1.5 0.0 copy-start.4
  1.5 61.7 %all_to_all.40.x_ref = bf16[16,32,256]{2,1,0:T(8,128)(2,1)S(1)} all-to-all(bf16[16,32,256]{2,1,0:T(8,128)(2,1)S(1)} %broadcast_in_dim.12), channel_id=1, replica_groups=mesh['grp'=2,'tp'=16,'dp'=16] {'tp'}, dimensions={0} | all-to-all | bytes 524288 | tf_op jit(solution)/shard_map/all_to_all | solution.py:189
  63.2 0.0 copy-done.5
  63.2 0.0 copy-done.6
  63.2 0.0 copy-done.7
  63.2 0.0 copy-done.1
  63.3 0.0 copy-done.2
  63.3 0.0 copy-done.3
  63.3 0.0 copy-done.4
  63.3 0.4 shard_map.140
  63.7 0.0 copy-start
  63.7 0.0 copy-start.9
  63.7 30.3 %all_to_all.41.arrived_ref = bf16[16,200,128]{2,1,0:T(8,128)(2,1)S(1)} all-to-all(bf16[16,200,128]{2,1,0:T(8,128)(2,1)S(1)} %shard_map.140), channel_id=1, replica_groups=mesh['grp'=2,'tp'=16,'dp'=16] {'dp'}, dimensions={0} | all-to-all | bytes 1638400 | tf_op jit(solution)/shard_map/all_to_all | solution.py:218
  94.0 0.0 copy-start.8
  94.0 0.0 copy-start.10
  94.0 0.0 copy-done
  94.0 0.0 copy-done.9
  94.0 0.7 copy-done.8
  94.7 0.0 copy-done.10
  94.7 2.8 %shard_map.141 = (bf16[32,128]{1,0:T(8,128)(2,1)S(1)}, f32[2,512,128]{2,1,0:T(8,128)}) custom-call(bf16[16,200,128]{2,1,0:T(8,128)(2,1)S(1)} %all_to_all.41.arrived_ref, s32[8]{0:T(128)S(1)} %copy-done.10, f32[2,128]{1,0:T(2,128)S(1)} %copy-done.8, f32[2,128]{1,0:T(2,128)S(1)} %copy-done.9, f32[2,512,128]{2,1,0:T(8,128)S(1)} %bitcast.22), custom_call_target="tpu_custom_call" | custom-call | flops 200000000 | bytes 2000000 | tf_op jit(solution)/shard_map/pallas_call | solution.py:168
  97.5 0.0 copy-start.11
  97.5 12.2 %all_to_all.42 = bf16[16,32,128]{2,1,0:T(8,128)(2,1)S(1)} all-to-all(bf16[16,32,128]{2,1,0:T(8,128)(2,1)S(1)} %broadcast_in_dim.13), channel_id=1, replica_groups=mesh['grp'=2,'tp'=16,'dp'=16] {'dp'}, dimensions={0} | all-to-all | bytes 262144 | tf_op jit(solution)/shard_map/all_to_all | solution.py:189
  109.6 0.0 copy-done.11
  109.6 0.2 convolution_convert_fusion.1
  109.8 24.7 %all_to_all.43 = bf16[16,32,256]{2,1,0:T(8,128)(2,1)S(1)} all-to-all(bf16[16,32,256]{2,1,0:T(8,128)(2,1)S(1)} %bitcast.24), channel_id=1, replica_groups=mesh['grp'=2,'tp'=16,'dp'=16] {'tp'}, dimensions={0} | all-to-all | bytes 524288 | tf_op jit(solution)/shard_map/all_to_all | solution.py:227
  134.5 0.0 copy-start.12
  134.6 0.7 copy-done.12
  135.3 24.2 %all_to_all.44.x_ref = bf16[16,32,256]{2,1,0:T(8,128)(2,1)S(1)} all-to-all(bf16[16,32,256]{2,1,0:T(8,128)(2,1)S(1)} %broadcast_in_dim.14), channel_id=1, replica_groups=mesh['grp'=2,'tp'=16,'dp'=16] {'tp'}, dimensions={0} | all-to-all | bytes 524288 | tf_op jit(solution)/shard_map/all_to_all | solution.py:189
  159.5 0.4 shard_map.142
  159.9 25.7 %all_to_all.45.arrived_ref = bf16[16,200,128]{2,1,0:T(8,128)(2,1)S(1)} all-to-all(bf16[16,200,128]{2,1,0:T(8,128)(2,1)S(1)} %shard_map.142), channel_id=1, replica_groups=mesh['grp'=2,'tp'=16,'dp'=16] {'dp'}, dimensions={0} | all-to-all | bytes 1638400 | tf_op jit(solution)/shard_map/all_to_all | solution.py:218
  185.5 2.8 %shard_map.143 = (bf16[32,128]{1,0:T(8,128)(2,1)S(1)}, f32[2,512,128]{2,1,0:T(8,128)}) custom-call(bf16[16,200,128]{2,1,0:T(8,128)(2,1)S(1)} %all_to_all.45.arrived_ref, s32[8]{0:T(128)S(1)} %copy-done.10, f32[2,128]{1,0:T(2,128)S(1)} %copy-done.8, f32[2,128]{1,0:T(2,128)S(1)} %copy-done.9, ...), custom_call_target="tpu_custom_call", output_to_operand_aliasing={{1}: (5, {})} | custom-call | flops 200000000 | bytes 2000000 | tf_op jit(solution)/shard_map/pallas_call | solution.py:168
  188.3 12.0 %all_to_all.46 = bf16[16,32,128]{2,1,0:T(8,128)(2,1)S(1)} all-to-all(bf16[16,32,128]{2,1,0:T(8,128)(2,1)S(1)} %broadcast_in_dim.15), channel_id=1, replica_groups=mesh['grp'=2,'tp'=16,'dp'=16] {'dp'}, dimensions={0} | all-to-all | bytes 262144 | tf_op jit(solution)/shard_map/all_to_all | solution.py:189
  200.3 0.2 convolution_convert_fusion
  200.5 24.7 %all_to_all.47 = bf16[16,32,256]{2,1,0:T(8,128)(2,1)S(1)} all-to-all(bf16[16,32,256]{2,1,0:T(8,128)(2,1)S(1)} %bitcast.25), channel_id=1, replica_groups=mesh['grp'=2,'tp'=16,'dp'=16] {'tp'}, dimensions={0} | all-to-all | bytes 524288 | tf_op jit(solution)/shard_map/all_to_all | solution.py:227
  225.3 0.6 add_convert_fusion
  (6 shorter events, 0.1 us)
Async XLA Ops:
  0.6 62.6 %copy-start.5 = (bf16[2,256,128]{2,1,0:T(8,128)(2,1)S(1)}, bf16[2,256,128]{2,1,0:T(8,128)(2,1)}, u32[]{:S(2)}) copy-start(bf16[2,256,128]{2,1,0:T(8,128)(2,1)} %refs_4_.3) | copy-start | bytes 393220
  0.6 62.6 %copy-start.6 = (bf16[2,256,128]{2,1,0:T(8,128)(2,1)S(1)}, bf16[2,256,128]{2,1,0:T(8,128)(2,1)}, u32[]{:S(2)}) copy-start(bf16[2,256,128]{2,1,0:T(8,128)(2,1)} %refs_5_.3) | copy-start | bytes 393220
  0.7 62.6 %copy-start.7 = (f32[2,256]{1,0:T(2,128)S(1)}, f32[2,256]{1,0:T(2,128)}, u32[]{:S(2)}) copy-start(f32[2,256]{1,0:T(2,128)} %gain_ref.6) | copy-start | bytes 6148
  1.4 61.8 %copy-start.1 = (bf16[2,256,128]{2,1,0:T(8,128)(2,1)S(1)}, bf16[2,256,128]{2,1,0:T(8,128)(2,1)}, u32[]{:S(2)}) copy-start(bf16[2,256,128]{2,1,0:T(8,128)(2,1)} %refs_0_.3) | copy-start | bytes 393220
  1.5 61.8 %copy-start.2 = (bf16[2,256,128]{2,1,0:T(8,128)(2,1)S(1)}, bf16[2,256,128]{2,1,0:T(8,128)(2,1)}, u32[]{:S(2)}) copy-start(bf16[2,256,128]{2,1,0:T(8,128)(2,1)} %refs_1_.3) | copy-start | bytes 393220
  1.5 61.8 %copy-start.3 = (bf16[2,256,128]{2,1,0:T(8,128)(2,1)S(1)}, bf16[2,256,128]{2,1,0:T(8,128)(2,1)}, u32[]{:S(2)}) copy-start(bf16[2,256,128]{2,1,0:T(8,128)(2,1)} %refs_2_.3) | copy-start | bytes 393220
  1.5 61.8 %copy-start.4 = (bf16[2,256,128]{2,1,0:T(8,128)(2,1)S(1)}, bf16[2,256,128]{2,1,0:T(8,128)(2,1)}, u32[]{:S(2)}) copy-start(bf16[2,256,128]{2,1,0:T(8,128)(2,1)} %refs_3_.3) | copy-start | bytes 393220
  63.7 30.3 %copy-start = (f32[2,8,2,4096]{3,2,1,0:T(2,128)S(1)}, f32[2,8,2,4096]{3,2,1,0:T(2,128)}, u32[]{:S(2)}) copy-start(f32[2,8,2,4096]{3,2,1,0:T(2,128)} %param.25) | copy-start | bytes 1572868
  63.7 30.3 %copy-start.9 = (f32[2,128]{1,0:T(2,128)S(1)}, f32[2,128]{1,0:T(2,128)}, u32[]{:S(2)}) copy-start(f32[2,128]{1,0:T(2,128)} %gain_ref.7) | copy-start | bytes 3076
  94.0 0.7 copy-start.8
  94.0 0.7 copy-start.10
  97.5 12.2 %copy-start.11 = (bf16[2,128,256]{2,1,0:T(8,128)(2,1)S(1)}, bf16[2,128,256]{2,1,0:T(8,128)(2,1)}, u32[]{:S(2)}) copy-start(bf16[2,128,256]{2,1,0:T(8,128)(2,1)} %param.24) | copy-start | bytes 393220
  134.5 0.7 copy-start.12

commit v2 on v1

--- a/solution.py
+++ b/solution.py
@@ -31,40 +31,66 @@
     )
 
 
-def project_kernel(layer, rows, x_ref, gain_ref, *refs):
-    *weight_refs, out_ref = refs
-    owners, _, depth = x_ref.shape
-    x = x_ref[...].reshape(owners * rows, depth).astype(jnp.float32)
+def project_kernel(layer, far, groups, place_ref, x_ref, gain_ref, *refs):
+    out_ref = refs[-1]
+    core, column = place_ref[0], place_ref[1]
+    blocks, rows, depth = x_ref.shape
+    half = rows // 2
+    first_half = core == (1 if far else 0)
+    x = x_ref[...].astype(jnp.float32)
+    x = jnp.where(first_half, x[:, :half], x[:, half:]).reshape(blocks * half, depth)
     scaled = (x * gain_ref[layer : layer + 1, :]).astype(jnp.bfloat16)
-    for first in range(0, 6, 2):
-        pair = jnp.concatenate([weight_refs[first][layer], weight_refs[first + 1][layer]], 1)
-        product = jnp.dot(scaled, pair, preferred_element_type=jnp.float32).astype(jnp.bfloat16)
-        for half in range(2):
-            out_ref[:, pl.ds((first + half) * rows, rows), :] = product[
-                :, half * LANES : (half + 1) * LANES
-            ].reshape(owners, rows, LANES)
     squares = jnp.sum(x * x, -1, keepdims=True)
-    eye = iota((rows, LANES), 0) == iota((rows, LANES), 1)
+    eye = iota((half, LANES), 0) == iota((half, LANES), 1)
     pick = iota((8, LANES), 0)
-    for owner in range(owners):
-        row = jnp.sum(
-            jnp.where(eye, squares[owner * rows : (owner + 1) * rows], 0.0), 0, keepdims=True
-        )
-        high = row.astype(jnp.bfloat16).astype(jnp.float32)
-        tail = jnp.where(pick == 0, high, jnp.where(pick == 1, row - high, 0.0))
-        out_ref[owner, pl.ds(6 * rows, 8), :] = tail.astype(jnp.bfloat16)
+    for group in range(groups):
+        owner = jnp.bitwise_xor(column, group) if groups > 1 else 0
+        for first in range(0, 6, 2):
+            if group:
+                pair = [refs[6][first], refs[6][first + 1]]
+            else:
+                pair = [refs[first][layer], refs[first + 1][layer]]
+            product = jnp.dot(
+                scaled, jnp.concatenate(pair, 1), preferred_element_type=jnp.float32
+            )
+            for side in range(2):
+                part = product[:, side * LANES : (side + 1) * LANES].reshape(blocks, half, LANES)
+                where = pl.ds((first + side) * half, half)
+                if not far:
+                    part = part + refs[-2][owner, :, where, :].astype(jnp.float32)
+                out_ref[owner, :, where, :] = part.astype(jnp.bfloat16)
+        for block in range(blocks):
+            row = jnp.sum(
+                jnp.where(eye, squares[block * half : (block + 1) * half], 0.0), 0, keepdims=True
+            )
+            if not far:
+                came = refs[-2][owner, block, pl.ds(6 * half, 8), :].astype(jnp.float32)
+                row = row + came[0:1] + came[1:2]
+            high = row.astype(jnp.bfloat16).astype(jnp.float32)
+            tail = jnp.where(pick == 0, high, jnp.where(pick == 1, row - high, 0.0))
+            out_ref[owner, block, pl.ds(6 * half, 8), :] = tail.astype(jnp.bfloat16)
 
 
 def advance_kernel(layer, rows, width, arrived_ref, lengths_ref, base_ref, gain_ref, state_ref, *refs):
     mixed_ref, new_ref, line_ref, read_ref = refs[-4:]
     seqs = rows // NEW
-    total = jnp.sum(arrived_ref[...].astype(jnp.float32), 0)
-    eye = iota((rows, LANES), 0) == iota((rows, LANES), 1)
-    square = total[6 * rows : 6 * rows + 1] + total[6 * rows + 1 : 6 * rows + 2]
-    square = jnp.sum(jnp.where(eye, square, 0.0), 1, keepdims=True)
-    inv_rms = lax.rsqrt(square / width + norm_epsilon)
+    parts, part_rows = arrived_ref.shape[0], (arrived_ref.shape[1] - 8) // 6
+    eye = iota((part_rows, LANES), 0) == iota((part_rows, LANES), 1)
+    scaled = []
+    for part in range(rows // part_rows):
+        outer, core = part // 2, part % 2
+        chips = parts * part_rows // rows
+        total = arrived_ref[outer * chips * 2 + core].astype(jnp.float32)
+        for chip in range(1, chips):
+            total += arrived_ref[(outer * chips + chip) * 2 + core].astype(jnp.float32)
+        square = total[6 * part_rows : 6 * part_rows + 1] + total[6 * part_rows + 1 : 6 * part_rows + 2]
+        square = jnp.sum(jnp.where(eye, square, 0.0), 1, keepdims=True)
+        inv_rms = lax.rsqrt(square / width + norm_epsilon)
+        scaled.append(
+            [inv_rms * total[role * part_rows : (role + 1) * part_rows] for role in range(6)]
+        )
     recept, keys, values, decay_pre, rate_pre, gate_pre = [
-        (inv_rms * total[role * rows : (role + 1) * rows]).astype(jnp.bfloat16).astype(jnp.float32)
+        jnp.concatenate([part[role] for part in scaled], 0).astype(jnp.bfloat16).astype(jnp.float32)
         for role in range(6)
     ]
     same_head = (iota((LANES, LANES), 0) // HEAD == iota((LANES, LANES), 1) // HEAD).astype(
@@ -141,19 +167,56 @@
     mixed_ref[...] = jnp.where(live, normed * jax.nn.sigmoid(gate_pre), 0.0).astype(jnp.bfloat16)
 
 
-def project(layer, x, gain, weights):
-    owners, rows, _ = x.shape
+def out_kernel(layer, place_ref, mixed_ref, own_ref, other_ref, out_ref):
+    pair, blocks, rows, _ = mixed_ref.shape
+    first = place_ref[1] == 0
+    own, other = own_ref[layer], other_ref[layer]
+    total = 0.0
+    for member, matrix in enumerate(
+        (jnp.where(first, own, other), jnp.where(first, other, own))
+    ):
+        total += jnp.dot(
+            mixed_ref[member].reshape(blocks * rows, LANES),
+            matrix,
+            preferred_element_type=jnp.float32,
+        )
+    out_ref[...] = total.astype(jnp.bfloat16).reshape(out_ref.shape)
+
+
+def params():
+    return {
+        "compiler_params": pltpu.CompilerParams(vmem_limit_bytes=24 * 2**20),
+        "cost_estimate": pl.CostEstimate(
+            flops=10**8, bytes_accessed=2 * 10**6, transcendentals=0
+        ),
+    }
+
+
+def project(layer, far, place, x, gain, weights, others, came):
+    blocks, rows, _ = x.shape
+    groups = 1 if others is None else 2
+    extra = ([] if others is None else [others]) + ([] if came is None else [came])
     return pl.pallas_call(
-        functools.partial(project_kernel, layer, rows),
-        out_shape=jax.ShapeDtypeStruct((owners, 6 * rows + 8, LANES), jnp.bfloat16),
-        in_specs=[VMEM] * 8,
+        functools.partial(project_kernel, layer, far, groups),
+        out_shape=jax.ShapeDtypeStruct((groups, blocks, 3 * rows + 8, LANES), jnp.bfloat16),
+        in_specs=[SMEM] + [VMEM] * (8 + len(extra)),
         out_specs=VMEM,
-        compiler_params=pltpu.CompilerParams(vmem_limit_bytes=24 * 2**20),
-        cost_estimate=pl.CostEstimate(flops=2 * 10**8, bytes_accessed=2 * 10**6, transcendentals=0),
-    )(x, gain, *weights)
-
-
-def advance(layer, width, arrived, lengths, base, gain, states, held):
+        **params(),
+    )(place, x, gain, *weights, *extra)
+
+
+def project_out(layer, place, mixed, own, other):
+    _, blocks, rows, _ = mixed.shape
+    return pl.pallas_call(
+        functools.partial(out_kernel, layer),
+        out_shape=jax.ShapeDtypeStruct((blocks, rows, own.shape[2]), jnp.bfloat16),
+        in_specs=[SMEM] + [VMEM] * 3,
+        out_specs=VMEM,
+        **params(),
+    )(place, mixed, own, other)
+
+
+def advance(layer, width, arrived, lengths, base, gain, states, held, awaited):
     rows = lengths.shape[0] * NEW
     state_rows = states.shape[1]
     block = pl.BlockSpec((1, state_rows, LANES), lambda i: (layer, 0, 0))
@@ -165,6 +228,8 @@
         aliases = {len(operands): 1}
         operands.append(held)
         in_specs.append(pl.BlockSpec(memory_space=pl.ANY))
+    operands.extend(awaited)
+    in_specs.extend([pl.BlockSpec(memory_space=pl.ANY)] * len(awaited))
     return pl.pallas_call(
         functools.partial(advance_kernel, layer, rows, width),
         grid=(1,),
@@ -179,14 +244,16 @@
             pltpu.VMEM((rows, LANES), jnp.float32),
         ],
         input_output_aliases=aliases,
-        compiler_params=pltpu.CompilerParams(vmem_limit_bytes=24 * 2**20),
-        cost_estimate=pl.CostEstimate(flops=2 * 10**8, bytes_accessed=2 * 10**6, transcendentals=0),
+        **params(),
     )(*operands)
 
 
-def gather_blocks(x, axis):
-    copies = jnp.broadcast_to(x, (lax.axis_size(axis), *x.shape))
-    return lax.all_to_all(copies, axis, split_axis=0, concat_axis=0, tiled=True)
+def exchange(x, axis, groups=None):
+    return lax.all_to_all(x, axis, 0, 0, tiled=True, axis_index_groups=groups)
+
+
+def from_partner(x, axis):
+    return lax.ppermute(x, axis, [(i, i ^ 1) for i in range(lax.axis_size(axis))])
 
 
 def per_device(
@@ -210,23 +277,46 @@
     blocks, seqs, heads, _ = states.shape
     folded = states.reshape(blocks, seqs, heads, HEAD // 2, LANES)
     folded = jnp.swapaxes(folded, 2, 3).reshape(blocks, seqs * HEAD, LANES)
+    columns, owners = lax.axis_size("tp"), lax.axis_size("dp")
+    place = jnp.stack([lax.axis_index("dp") % 2, lax.axis_index("tp") % 2])
+    both = ("tp", "dp")
+    pairs = [
+        [column * owners + owner for column in (first, first + 1) for owner in range(owners)]
+        for first in range(0, columns, 2)
+    ]
+    half = own_count // 2
+    other_out = from_partner(w_out, "tp")
+    other_weights = from_partner(jnp.stack([weight[1] for weight in weights]), "tp")
     own_rows = tokens
     held = None
     for layer in range(2):
-        gathered = gather_blocks(own_rows, "tp")
-        partial_sums = project(layer, gathered, norm_gain, weights)
-        arrived = lax.all_to_all(partial_sums, "dp", 0, 0, tiled=True)
+        if layer == 0:
+            spread = jnp.broadcast_to(own_rows, (columns, own_count, depth))
+            others = None
+        else:
+            spread = jnp.broadcast_to(
+                own_rows.reshape(2, half, depth), (columns // 2, 2, half, depth)
+            ).reshape(columns, half, depth)
+            others = other_weights
+        gathered = exchange(spread, "tp")
+        far = project(layer, True, place, gathered, norm_gain, weights, others, None)
+        came = from_partner(far, "dp")
+        near = project(layer, False, place, gathered, norm_gain, weights, others, came)
+        near = near.reshape(-1, *near.shape[2:])
+        arrived = exchange(near, "dp") if layer == 0 else exchange(near, both, pairs)
         mixed, held = advance(
-            layer, width, arrived, lengths, decay_base, group_gain, folded, held
-        )
-        everyone = gather_blocks(mixed, "dp")
-        product = jnp.dot(
-            everyone.reshape(-1, LANES), w_out[layer], preferred_element_type=jnp.float32
-        )
-        product = product.astype(jnp.bfloat16).reshape(-1, own_count, depth)
-        summed = lax.all_to_all(product, "tp", 0, 0, tiled=True)
+            layer, width, arrived, lengths, decay_base, group_gain, folded, held,
+            [] if layer else [other_out, other_weights],
+        )
+        shared = jnp.broadcast_to(mixed.reshape(2, 1, half, LANES), (2, owners, half, LANES))
+        shared = exchange(shared.reshape(2 * owners, half, LANES), both, pairs)
+        product = project_out(
+            layer, place, shared.reshape(2, owners, half, LANES), w_out, other_out
+        )
+        summed = exchange(product, "tp").astype(jnp.float32)
+        summed = jnp.sum(summed.reshape(columns // 2, 2, half, depth), 0)
         own_rows = (
-            own_rows.astype(jnp.float32) + jnp.sum(summed.astype(jnp.float32), 0)
+            own_rows.astype(jnp.float32) + summed.reshape(own_count, depth)
         ).astype(jnp.bfloat16)
     new_states = jnp.swapaxes(held.reshape(blocks, seqs, HEAD // 2, heads, LANES), 2, 3)
     return (own_rows, new_states.reshape(states.shape))

time: 226 us -> 215 us (0.951)
  blocking collectives: 215 us -> 107 us
  starting transfers between devices: 0 us -> 61.5 us
  waiting for transfers between devices: 0 us -> 30.7 us
  Pallas kernels: 6.31 us -> 11.1 us
    all_to_all x8 -> x6, blocking collectives: 215 us -> 107 us  [exchange(): return lax.all_to_all(x, axis, 0, 0, tiled=True, axis_index_groups=groups)]
    all_to_all x0 -> x2, starting transfers between devices: none -> 51.6 us  [exchange(): return lax.all_to_all(x, axis, 0, 0, tiled=True, axis_index_groups=groups)]
    all_to_all x0 -> x2, waiting for transfers between devices: none -> 17.2 us  [exchange(): return lax.all_to_all(x, axis, 0, 0, tiled=True, axis_index_groups=groups)]
    ppermute x0 -> x4, waiting for transfers between devices: none -> 13.5 us  [from_partner(): lax.ppermute(x, axis, [(i, i ^ 1) for i in range(lax.axis_size(axis))])]
    ppermute x0 -> x4, starting transfers between devices: none -> 9.94 us  [from_partner(): lax.ppermute(x, axis, [(i, i ^ 1) for i in range(lax.axis_size(axis))])]
    pallas_call x2 -> x6, Pallas kernels: 0.77 us -> 5.55 us  [the longest x4 4.05 us: project(): pl.pallas_call(functools.partial(project_kernel, layer, far, groups), out...]
  transfers between devices with their start and end apart: 0 -> 6, of which waited for: 0 -> 4; matrix products, arithmetic and copies ran while one was open for 0% -> 0% of each run, Pallas kernels for 0% -> 0%
where the time goes in v2:
time: 215 us
  blocking collectives  107 us (50%)
  starting transfers between devices  61.5 us (29%)
  waiting for transfers between devices  30.7 us (14%)
  Pallas kernels  11.1 us (5%)
  local copies, waits for them, and re-layouts  3.11 us (1%)
    all_to_all x6, blocking collectives, exchange(): return lax.all_to_all(x, axis, 0, 0, tiled=True, axis_index_groups=groups)  107 us
    all_to_all x2, starting transfers between devices, exchange(): return lax.all_to_all(x, axis, 0, 0, tiled=True, axis_index_groups=groups)  51.6 us
    all_to_all x2, waiting for transfers between devices, exchange(): return lax.all_to_all(x, axis, 0, 0, tiled=True, axis_index_groups=groups)  17.2 us
    ppermute x4, waiting for transfers between devices, from_partner(): lax.ppermute(x, axis, [(i, i ^ 1) for i in range(lax.axis_size(axis))])  13.5 us
    ppermute x4, starting transfers between devices, from_partner(): lax.ppermute(x, axis, [(i, i ^ 1) for i in range(lax.axis_size(axis))])  9.94 us
    pallas_call x2, Pallas kernels, advance(): pl.pallas_call(functools.partial(advance_kernel, layer, rows, width), gri...  5.54 us
  transfers between devices with their start and end apart: 6, of which 4 were waited for; matrix products, arithmetic and copies ran while one was open for 0% of the time, Pallas kernels for 0%

profile of v2, /device:TPU:80, one launch (start us, length us, event | category | flops | bytes accessed | tf_op | source)
XLA Modules:
  0.0 214.6 jit_solution(10896418946798948491)
XLA Ops:
  0.6 1.4 broadcast_in_dim.20
  2.1 0.0 copy-start
  2.1 43.8 %all-to-all-start = ((bf16[16,32,256]{2,1,0:T(8,128)(2,1)}), bf16[16,32,256]{2,1,0:T(8,128)(2,1)S(1)}, u32[]{:S(2)}, u32[]{:S(2)}) async-start(bf16[16,32,256]{2,1,0:T(8,128)(2,1)} %broadcast_in_dim.20), calls=%async_computation | async-start | bytes 524288 | tf_op jit(solution)/shard_map/all_to_all | solution.py:252
  45.9 0.0 copy-start.1
  46.0 0.1 pad_add_fusion.place_ref
  46.0 0.0 copy-done
  46.0 0.8 copy-done.1
  46.8 17.2 %all-to-all-done.x_ref = bf16[16,32,256]{2,1,0:T(8,128)(2,1)S(1)} async-done(((bf16[16,32,256]{2,1,0:T(8,128)(2,1)}), bf16[16,32,256]{2,1,0:T(8,128)(2,1)S(1)}, u32[]{:S(2)}, u32[]{:S(2)}) %all-to-all-start) | async-done | bytes 262176 | tf_op jit(solution)/shard_map/all_to_all | solution.py:252
  64.0 0.0 copy-done.3
  64.0 0.0 copy-done.4
  64.1 0.0 copy-done.5
  64.1 0.0 copy-done.2
  64.1 0.0 copy-done.8
  64.1 0.8 shard_map.140
  64.9 2.0 collective-permute-start
  66.9 1.7 collective-permute-done.refs_6_
  68.6 1.6 shard_map.141
  70.2 7.8 %all-to-all-start.1 = ((bf16[16,104,128]{2,1,0:T(8,128)(2,1)}), bf16[16,104,128]{2,1,0:T(8,128)(2,1)S(1)}, u32[]{:S(2)}, u32[]{:S(2)}) async-start(bf16[16,104,128]{2,1,0:T(8,128)(2,1)} %bitcast.2), calls=%async_computation.1 | async-start | bytes 851968 | tf_op jit(solution)/shard_map/all_to_all | solution.py:252
  77.9 0.0 copy-start.7
  78.0 0.0 copy-start.10
  78.0 0.0 copy-start.9
  78.0 0.0 copy-start.11
  78.0 3.7 %collective-permute-start.2 = (bf16[6,256,128]{2,1,0:T(8,128)(2,1)S(1)}, bf16[6,256,128]{2,1,0:T(8,128)(2,1)S(1)}, u32[]{:S(2)}, u32[]{:S(2)}) collective-permute-start(bf16[6,256,128]{2,1,0:T(8,128)(2,1)S(1)} %slice_dynamic-update-slice_fusion), channel_id=1, source_target_pairs={{0,16},{16,0},{32,48},{48,32},{64,80},{80,64},{96,112},{112,96},{1... | collective-permute-start | bytes 1179656 | tf_op jit(solution)/shard_map/ppermute | solution.py:256
  81.7 0.0 copy-done.7
  81.8 2.3 %collective-permute-start.1 = (bf16[2,128,256]{2,1,0:T(8,128)(2,1)S(1)}, bf16[2,128,256]{2,1,0:T(8,128)(2,1)S(1)}, u32[]{:S(2)}, u32[]{:S(2)}) collective-permute-start(bf16[2,128,256]{2,1,0:T(8,128)(2,1)S(1)} %copy-done.7), channel_id=1, source_target_pairs={{0,16},{16,0},{32,48},{48,32},{64,80},{80,64},{96,112},{112,96},{1... | collective-permute-start | bytes 393224 | tf_op jit(solution)/shard_map/ppermute | solution.py:256
  84.1 10.0 %collective-permute-done.1.refs_0_.other_ref = bf16[2,128,256]{2,1,0:T(8,128)(2,1)S(1)} collective-permute-done((bf16[2,128,256]{2,1,0:T(8,128)(2,1)S(1)}, bf16[2,128,256]{2,1,0:T(8,128)(2,1)S(1)}, u32[]{:S(2)}, u32[]{:S(2)}) %collective-permute-start.1) | collective-permute-done | bytes 131104 | tf_op jit(solution)/shard_map/ppermute | solution.py:256
  94.1 0.0 collective-permute-done.2.refs_1_.refs_6_
  94.1 0.0 all-to-all-done.1.arrived_ref
  94.1 0.0 copy-done.6
  94.1 0.0 copy-done.10
  94.1 0.0 copy-done.9
  94.1 0.0 copy-done.11
  94.1 2.8 %shard_map.142 = (bf16[32,128]{1,0:T(8,128)(2,1)S(1)}, f32[2,512,128]{2,1,0:T(8,128)}) custom-call(bf16[16,104,128]{2,1,0:T(8,128)(2,1)S(1)} %all-to-all-done.1.arrived_ref, s32[8]{0:T(128)S(1)} %copy-done.11, f32[2,128]{1,0:T(2,128)S(1)} %copy-done.9, f32[2,128]{1,0:T(2,128)S(1)} %copy-done.10, f32[2,512,128]{2,1,0:T(8,128)S(1)} %bitcast.34, ...), custom_call_target="tpu_custom_call" | custom-call | flops 100000000 | bytes 2000000 | tf_op jit(solution)/shard_map/pallas_call | solution.py:233
  96.9 17.3 %all_to_all.40 = bf16[32,16,128]{2,1,0:T(8,128)(2,1)S(1)} all-to-all(bf16[32,16,128]{2,1,0:T(8,128)(2,1)S(1)} %bitcast.43), channel_id=1, replica_groups={{0,1,2,3,4,5,6,7,8,9,10,11,12,13,14,15,16,17,18,19,20,21,22,23,24,25,26..., dimensions={0} | all-to-all | bytes 262144 | tf_op jit(solution)/shard_map/all_to_all | solution.py:252
  114.2 0.7 shard_map.143
  115.0 20.2 %all_to_all.41 = bf16[16,16,256]{2,1,0:T(8,128)(2,1)S(1)} all-to-all(bf16[16,16,256]{2,1,0:T(8,128)(2,1)S(1)} %shard_map.143), channel_id=1, replica_groups=mesh['grp'=2,'tp'=16,'dp'=16] {'tp'}, dimensions={0} | all-to-all | bytes 262144 | tf_op jit(solution)/shard_map/all_to_all | solution.py:252
  135.2 0.7 copy-done.12
  135.9 17.9 %all_to_all.42.x_ref = bf16[16,16,256]{2,1,0:T(8,128)(2,1)S(1)} all-to-all(bf16[16,16,256]{2,1,0:T(8,128)(2,1)S(1)} %bitcast.45), channel_id=1, replica_groups=mesh['grp'=2,'tp'=16,'dp'=16] {'tp'}, dimensions={0} | all-to-all | bytes 262144 | tf_op jit(solution)/shard_map/all_to_all | solution.py:252
  153.8 0.8 shard_map.144
  154.6 2.0 collective-permute-start.3
  156.6 1.8 collective-permute-done.3.refs_7_
  158.4 0.8 shard_map.145
  159.2 18.9 %all_to_all.43.arrived_ref = bf16[32,56,128]{2,1,0:T(8,128)(2,1)S(1)} all-to-all(bf16[32,56,128]{2,1,0:T(8,128)(2,1)S(1)} %bitcast.36), channel_id=1, replica_groups={{0,1,2,3,4,5,6,7,8,9,10,11,12,13,14,15,16,17,18,19,20,21,22,23,24,25,26..., dimensions={0} | all-to-all | bytes 917504 | tf_op jit(solution)/shard_map/all_to_all | solution.py:252
  178.1 2.8 %shard_map.146 = (bf16[32,128]{1,0:T(8,128)(2,1)S(1)}, f32[2,512,128]{2,1,0:T(8,128)}) custom-call(bf16[32,56,128]{2,1,0:T(8,128)(2,1)S(1)} %all_to_all.43.arrived_ref, s32[8]{0:T(128)S(1)} %copy-done.11, f32[2,128]{1,0:T(2,128)S(1)} %copy-done.9, f32[2,128]{1,0:T(2,128)S(1)} %copy-done.10, ...), custom_call_target="tpu_custom_call", output_to_operand_aliasing={{1}: (5, {})} | custom-call | flops 100000000 | bytes 2000000 | tf_op jit(solution)/shard_map/pallas_call | solution.py:233
  180.9 14.1 %all_to_all.44 = bf16[32,16,128]{2,1,0:T(8,128)(2,1)S(1)} all-to-all(bf16[32,16,128]{2,1,0:T(8,128)(2,1)S(1)} %bitcast.44), channel_id=1, replica_groups={{0,1,2,3,4,5,6,7,8,9,10,11,12,13,14,15,16,17,18,19,20,21,22,23,24,25,26..., dimensions={0} | all-to-all | bytes 262144 | tf_op jit(solution)/shard_map/all_to_all | solution.py:252
  195.0 0.8 shard_map.147
  195.8 18.2 %all_to_all.45 = bf16[16,16,256]{2,1,0:T(8,128)(2,1)S(1)} all-to-all(bf16[16,16,256]{2,1,0:T(8,128)(2,1)S(1)} %shard_map.147), channel_id=1, replica_groups=mesh['grp'=2,'tp'=16,'dp'=16] {'tp'}, dimensions={0} | all-to-all | bytes 262144 | tf_op jit(solution)/shard_map/all_to_all | solution.py:252
  214.0 0.6 fusion
  (19 shorter events, 0.2 us)
Async XLA Ops:
  2.1 44.0 %copy-start = (bf16[2,256,128]{2,1,0:T(8,128)(2,1)S(1)}, bf16[2,256,128]{2,1,0:T(8,128)(2,1)}, u32[]{:S(2)}) copy-start(bf16[2,256,128]{2,1,0:T(8,128)(2,1)} %refs_0_.7) | copy-start | bytes 393220
  2.1 62.0 %copy-start.3 = (bf16[2,256,128]{2,1,0:T(8,128)(2,1)S(1)}, bf16[2,256,128]{2,1,0:T(8,128)(2,1)}, u32[]{:S(2)}) copy-start(bf16[2,256,128]{2,1,0:T(8,128)(2,1)} %refs_3_.7) | copy-start | bytes 393220
  2.1 62.0 %copy-start.4 = (bf16[2,256,128]{2,1,0:T(8,128)(2,1)S(1)}, bf16[2,256,128]{2,1,0:T(8,128)(2,1)}, u32[]{:S(2)}) copy-start(bf16[2,256,128]{2,1,0:T(8,128)(2,1)} %refs_4_.7) | copy-start | bytes 393220
  2.1 62.0 %copy-start.5 = (bf16[2,256,128]{2,1,0:T(8,128)(2,1)S(1)}, bf16[2,256,128]{2,1,0:T(8,128)(2,1)}, u32[]{:S(2)}) copy-start(bf16[2,256,128]{2,1,0:T(8,128)(2,1)} %refs_5_.7) | copy-start | bytes 393220
  2.1 62.0 %all-to-all-start = ((bf16[16,32,256]{2,1,0:T(8,128)(2,1)}), bf16[16,32,256]{2,1,0:T(8,128)(2,1)S(1)}, u32[]{:S(2)}, u32[]{:S(2)}) async-start(bf16[16,32,256]{2,1,0:T(8,128)(2,1)} %broadcast_in_dim.20), calls=%async_computation | async-start | bytes 524288 | tf_op jit(solution)/shard_map/all_to_all | solution.py:252
  45.9 0.9 copy-start.1
  46.0 18.0 %copy-start.2 = (bf16[2,256,128]{2,1,0:T(8,128)(2,1)S(1)}, bf16[2,256,128]{2,1,0:T(8,128)(2,1)}, u32[]{:S(2)}) copy-start(bf16[2,256,128]{2,1,0:T(8,128)(2,1)} %refs_2_.7) | copy-start | bytes 393220
  46.8 17.2 %copy-start.8 = (f32[2,256]{1,0:T(2,128)S(1)}, f32[2,256]{1,0:T(2,128)}, u32[]{:S(2)}) copy-start(f32[2,256]{1,0:T(2,128)} %gain_ref.10) | copy-start | bytes 6148
  64.9 3.7 %collective-permute-start = (bf16[1,16,104,128]{3,2,1,0:T(8,128)(2,1)S(1)}, bf16[1,16,104,128]{3,2,1,0:T(8,128)(2,1)S(1)}, u32[]{:S(2)}, u32[]{:S(2)}) collective-permute-start(bf16[1,16,104,128]{3,2,1,0:T(8,128)(2,1)S(1)} %shard_map.140), channel_id=1, source_target_pairs={{0,1},{1,0},{2,3},{3,2},{4,5},{5,4},{6,7},{7,6},{8,9},{9,8},{10,11... | collective-permute-start | bytes 1277960 | tf_op jit(solution)/shard_map/ppermute | solution.py:256
  70.2 23.9 %copy-start.6 = (f32[2,8,2,4096]{3,2,1,0:T(2,128)S(1)}, f32[2,8,2,4096]{3,2,1,0:T(2,128)}, u32[]{:S(2)}) copy-start(f32[2,8,2,4096]{3,2,1,0:T(2,128)} %param.25) | copy-start | bytes 1572868
  70.2 23.9 %all-to-all-start.1 = ((bf16[16,104,128]{2,1,0:T(8,128)(2,1)}), bf16[16,104,128]{2,1,0:T(8,128)(2,1)S(1)}, u32[]{:S(2)}, u32[]{:S(2)}) async-start(bf16[16,104,128]{2,1,0:T(8,128)(2,1)} %bitcast.2), calls=%async_computation.1 | async-start | bytes 851968 | tf_op jit(solution)/shard_map/all_to_all | solution.py:252
  77.9 3.8 %copy-start.7 = (bf16[2,128,256]{2,1,0:T(8,128)(2,1)S(1)}, bf16[2,128,256]{2,1,0:T(8,128)(2,1)}, u32[]{:S(2)}) copy-start(bf16[2,128,256]{2,1,0:T(8,128)(2,1)} %own_ref.3) | copy-start | bytes 393220
  78.0 16.2 %copy-start.10 = (f32[2,128]{1,0:T(2,128)S(1)}, f32[2,128]{1,0:T(2,128)}, u32[]{:S(2)}) copy-start(f32[2,128]{1,0:T(2,128)} %gain_ref.11) | copy-start | bytes 3076
  78.0 16.1 %copy-start.9 = (f32[2,128]{1,0:T(2,128)S(1)}, f32[2,128]{1,0:T(2,128)}, u32[]{:S(2)}) copy-start(f32[2,128]{1,0:T(2,128)} %base_ref.3) | copy-start | bytes 3076
  78.0 16.1 %copy-start.11 = (s32[8]{0:T(128)S(1)}, s32[8]{0:T(128)}, u32[]{:S(2)}) copy-start(s32[8]{0:T(128)} %lengths_ref.3) | copy-start | bytes 100
  78.0 16.1 %collective-permute-start.2 = (bf16[6,256,128]{2,1,0:T(8,128)(2,1)S(1)}, bf16[6,256,128]{2,1,0:T(8,128)(2,1)S(1)}, u32[]{:S(2)}, u32[]{:S(2)}) collective-permute-start(bf16[6,256,128]{2,1,0:T(8,128)(2,1)S(1)} %slice_dynamic-update-slice_fusion), channel_id=1, source_target_pairs={{0,16},{16,0},{32,48},{48,32},{64,80},{80,64},{96,112},{112,96},{1... | collective-permute-start | bytes 1179656 | tf_op jit(solution)/shard_map/ppermute | solution.py:256
  81.8 12.4 %collective-permute-start.1 = (bf16[2,128,256]{2,1,0:T(8,128)(2,1)S(1)}, bf16[2,128,256]{2,1,0:T(8,128)(2,1)S(1)}, u32[]{:S(2)}, u32[]{:S(2)}) collective-permute-start(bf16[2,128,256]{2,1,0:T(8,128)(2,1)S(1)} %copy-done.7), channel_id=1, source_target_pairs={{0,16},{16,0},{32,48},{48,32},{64,80},{80,64},{96,112},{112,96},{1... | collective-permute-start | bytes 393224 | tf_op jit(solution)/shard_map/ppermute | solution.py:256
  135.2 0.7 copy-start.12
  154.6 3.7 %collective-permute-start.3 = (bf16[2,16,56,128]{3,2,1,0:T(8,128)(2,1)S(1)}, bf16[2,16,56,128]{3,2,1,0:T(8,128)(2,1)S(1)}, u32[]{:S(2)}, u32[]{:S(2)}) collective-permute-start(bf16[2,16,56,128]{3,2,1,0:T(8,128)(2,1)S(1)} %shard_map.144), channel_id=1, source_target_pairs={{0,1},{1,0},{2,3},{3,2},{4,5},{5,4},{6,7},{7,6},{8,9},{9,8},{10,11... | collective-permute-start | bytes 1376264 | tf_op jit(solution)/shard_map/ppermute | solution.py:256

commit v3 on v2

--- a/solution.py
+++ b/solution.py
@@ -6,6 +6,7 @@
 from jax.experimental import pallas as pl
 from jax.experimental.pallas import tpu as pltpu
 from jax.sharding import PartitionSpec as P
+
 
 HEAD = 64
 NEW = 4
@@ -167,8 +168,9 @@
     mixed_ref[...] = jnp.where(live, normed * jax.nn.sigmoid(gate_pre), 0.0).astype(jnp.bfloat16)
 
 
-def out_kernel(layer, place_ref, mixed_ref, own_ref, other_ref, out_ref):
-    pair, blocks, rows, _ = mixed_ref.shape
+def out_kernel(layer, place_ref, mixed_ref, own_ref, other_ref, *refs):
+    out_ref = refs[-1]
+    _, blocks, rows, _ = mixed_ref.shape
     first = place_ref[1] == 0
     own, other = own_ref[layer], other_ref[layer]
     total = 0.0
@@ -205,15 +207,15 @@
     )(place, x, gain, *weights, *extra)
 
 
-def project_out(layer, place, mixed, own, other):
+def project_out(layer, place, mixed, own, other, awaited):
     _, blocks, rows, _ = mixed.shape
     return pl.pallas_call(
         functools.partial(out_kernel, layer),
         out_shape=jax.ShapeDtypeStruct((blocks, rows, own.shape[2]), jnp.bfloat16),
-        in_specs=[SMEM] + [VMEM] * 3,
+        in_specs=[SMEM] + [VMEM] * 3 + [pl.BlockSpec(memory_space=pl.ANY)] * len(awaited),
         out_specs=VMEM,
         **params(),
-    )(place, mixed, own, other)
+    )(place, mixed, own, other, *awaited)
 
 
 def advance(layer, width, arrived, lengths, base, gain, states, held, awaited):
@@ -306,12 +308,13 @@
         arrived = exchange(near, "dp") if layer == 0 else exchange(near, both, pairs)
         mixed, held = advance(
             layer, width, arrived, lengths, decay_base, group_gain, folded, held,
-            [] if layer else [other_out, other_weights],
+            [] if layer else [other_out],
         )
         shared = jnp.broadcast_to(mixed.reshape(2, 1, half, LANES), (2, owners, half, LANES))
         shared = exchange(shared.reshape(2 * owners, half, LANES), both, pairs)
         product = project_out(
-            layer, place, shared.reshape(2, owners, half, LANES), w_out, other_out
+            layer, place, shared.reshape(2, owners, half, LANES), w_out, other_out,
+            [] if layer else [other_weights],
         )
         summed = exchange(product, "tp").astype(jnp.float32)
         summed = jnp.sum(summed.reshape(columns // 2, 2, half, depth), 0)

time: 215 us -> 220 us (1.023)
  blocking collectives: 107 us -> 92 us
  waiting for transfers between devices: 30.7 us -> 44 us
  starting transfers between devices: 61.5 us -> 67.2 us
    all_to_all x2 -> x3, waiting for transfers between devices: 17.2 us -> 31.9 us  [exchange(): return lax.all_to_all(x, axis, 0, 0, tiled=True, axis_index_groups=groups)]
    all_to_all x6 -> x5, blocking collectives: 107 us -> 92 us  [exchange(): return lax.all_to_all(x, axis, 0, 0, tiled=True, axis_index_groups=groups)]
    all_to_all x2 -> x3, starting transfers between devices: 51.6 us -> 56.4 us  [exchange(): return lax.all_to_all(x, axis, 0, 0, tiled=True, axis_index_groups=groups)]
  transfers between devices with their start and end apart: 6 -> 7, of which waited for: 4 -> 4; matrix products, arithmetic and copies ran while one was open for 0% -> 0% of each run, Pallas kernels for 0% -> 1%
where the time goes in v3:
time: 220 us; the launch traced here: 219 us
  blocking collectives  92 us (42%)
  starting transfers between devices  67.2 us (31%)
  waiting for transfers between devices  44 us (20%)
  Pallas kernels  11.1 us (5%)
  local copies, waits for them, and re-layouts  3.02 us (1%)
    all_to_all x5, blocking collectives, exchange(): return lax.all_to_all(x, axis, 0, 0, tiled=True, axis_index_groups=groups)  92 us
    all_to_all x3, starting transfers between devices, exchange(): return lax.all_to_all(x, axis, 0, 0, tiled=True, axis_index_groups=groups)  56.4 us
    all_to_all x3, waiting for transfers between devices, exchange(): return lax.all_to_all(x, axis, 0, 0, tiled=True, axis_index_groups=groups)  31.9 us
    ppermute x4, waiting for transfers between devices, from_partner(): lax.ppermute(x, axis, [(i, i ^ 1) for i in range(lax.axis_size(axis))])  12.1 us
    ppermute x4, starting transfers between devices, from_partner(): lax.ppermute(x, axis, [(i, i ^ 1) for i in range(lax.axis_size(axis))])  10.8 us
    pallas_call x2, Pallas kernels, advance(): pl.pallas_call(functools.partial(advance_kernel, layer, rows, width), gri...  5.54 us
  transfers between devices with their start and end apart: 7, of which 4 were waited for; matrix products, arithmetic and copies ran while one was open for 0% of the time, Pallas kernels for 1%

profile of v3, /device:TPU:80, one launch (start us, length us, event | category | flops | bytes accessed | tf_op | source)
XLA Modules:
  0.0 219.0 jit_solution(12823011457890101906)
XLA Ops:
  0.6 0.0 copy-start.4
  0.6 0.0 copy-start.5
  0.6 1.5 broadcast_in_dim.20
  2.1 43.8 %all-to-all-start = ((bf16[16,32,256]{2,1,0:T(8,128)(2,1)}), bf16[16,32,256]{2,1,0:T(8,128)(2,1)S(1)}, u32[]{:S(2)}, u32[]{:S(2)}) async-start(bf16[16,32,256]{2,1,0:T(8,128)(2,1)} %broadcast_in_dim.20), calls=%async_computation | async-start | bytes 524288 | tf_op jit(solution)/shard_map/all_to_all | solution.py:254
  46.0 0.0 copy-start.8
  46.0 0.1 pad_add_fusion.place_ref
  46.1 18.0 %all-to-all-done.x_ref = bf16[16,32,256]{2,1,0:T(8,128)(2,1)S(1)} async-done(((bf16[16,32,256]{2,1,0:T(8,128)(2,1)}), bf16[16,32,256]{2,1,0:T(8,128)(2,1)S(1)}, u32[]{:S(2)}, u32[]{:S(2)}) %all-to-all-start) | async-done | bytes 262176 | tf_op jit(solution)/shard_map/all_to_all | solution.py:254
  64.1 0.0 copy-done.4
  64.1 0.0 copy-done.5
  64.1 0.0 copy-done
  64.1 0.0 copy-done.1
  64.1 0.0 copy-done.2
  64.1 0.0 copy-done.3
  64.1 0.0 copy-done.8
  64.2 0.8 shard_map.140
  65.0 2.0 collective-permute-start
  66.9 0.0 copy-done.7
  66.9 3.6 %collective-permute-start.1 = (bf16[2,128,256]{2,1,0:T(8,128)(2,1)S(1)}, bf16[2,128,256]{2,1,0:T(8,128)(2,1)S(1)}, u32[]{:S(2)}, u32[]{:S(2)}) collective-permute-start(bf16[2,128,256]{2,1,0:T(8,128)(2,1)S(1)} %copy-done.7), channel_id=1, source_target_pairs={{0,16},{16,0},{32,48},{48,32},{64,80},{80,64},{96,112},{112,96},{1... | collective-permute-start | bytes 393224 | tf_op jit(solution)/shard_map/ppermute | solution.py:258
  70.6 0.0 collective-permute-done.refs_6_
  70.6 1.6 shard_map.141
  72.1 7.8 %all-to-all-start.1 = ((bf16[16,104,128]{2,1,0:T(8,128)(2,1)}), bf16[16,104,128]{2,1,0:T(8,128)(2,1)S(1)}, u32[]{:S(2)}, u32[]{:S(2)}) async-start(bf16[16,104,128]{2,1,0:T(8,128)(2,1)} %bitcast.2), calls=%async_computation.1 | async-start | bytes 851968 | tf_op jit(solution)/shard_map/all_to_all | solution.py:254
  80.0 0.0 copy-start.10
  80.0 0.0 copy-start.9
  80.0 0.0 copy-start.11
  80.0 0.0 collective-permute-done.1.refs_0_.other_ref
  80.0 13.9 %all-to-all-done.1.arrived_ref = bf16[16,104,128]{2,1,0:T(8,128)(2,1)S(1)} async-done(((bf16[16,104,128]{2,1,0:T(8,128)(2,1)}), bf16[16,104,128]{2,1,0:T(8,128)(2,1)S(1)}, u32[]{:S(2)}, u32[]{:S(2)}) %all-to-all-start.1) | async-done | bytes 426016 | tf_op jit(solution)/shard_map/all_to_all | solution.py:254
  93.9 0.0 copy-done.6
  93.9 0.0 copy-done.9
  93.9 2.8 %shard_map.142 = (bf16[32,128]{1,0:T(8,128)(2,1)S(1)}, f32[2,512,128]{2,1,0:T(8,128)}) custom-call(bf16[16,104,128]{2,1,0:T(8,128)(2,1)S(1)} %all-to-all-done.1.arrived_ref, s32[8]{0:T(128)S(1)} %copy-done.11, f32[2,128]{1,0:T(2,128)S(1)} %copy-done.9, f32[2,128]{1,0:T(2,128)S(1)} %copy-done.10, f32[2,512,128]{2,1,0:T(8,128)S(1)} %bitcast.34, ...), custom_call_target="tpu_custom_call" | custom-call | flops 100000000 | bytes 2000000 | tf_op jit(solution)/shard_map/pallas_call | solution.py:235
  96.7 0.7 broadcast_in_dim.22
  97.4 4.8 %all-to-all-start.2 = ((bf16[32,16,128]{2,1,0:T(8,128)(2,1)}), bf16[32,16,128]{2,1,0:T(8,128)(2,1)S(1)}, u32[]{:S(2)}, u32[]{:S(2)}) async-start(bf16[32,16,128]{2,1,0:T(8,128)(2,1)} %bitcast.7), calls=%async_computation.2 | async-start | bytes 262144 | tf_op jit(solution)/shard_map/all_to_all | solution.py:254
  102.3 3.3 %collective-permute-start.2 = (bf16[6,256,128]{2,1,0:T(8,128)(2,1)S(1)}, bf16[6,256,128]{2,1,0:T(8,128)(2,1)S(1)}, u32[]{:S(2)}, u32[]{:S(2)}) collective-permute-start(bf16[6,256,128]{2,1,0:T(8,128)(2,1)S(1)} %slice_dynamic-update-slice_fusion), channel_id=1, source_target_pairs={{0,16},{16,0},{32,48},{48,32},{64,80},{80,64},{96,112},{112,96},{1... | collective-permute-start | bytes 1179656 | tf_op jit(solution)/shard_map/ppermute | solution.py:258
  105.5 10.4 %collective-permute-done.2.refs_0_.refs_6_ = bf16[6,256,128]{2,1,0:T(8,128)(2,1)S(1)} collective-permute-done((bf16[6,256,128]{2,1,0:T(8,128)(2,1)S(1)}, bf16[6,256,128]{2,1,0:T(8,128)(2,1)S(1)}, u32[]{:S(2)}, u32[]{:S(2)}) %collective-permute-start.2) | collective-permute-done | bytes 393248 | tf_op jit(solution)/shard_map/ppermute | solution.py:258
  115.9 0.0 all-to-all-done.2
  115.9 0.8 shard_map.143
  116.7 20.0 %all_to_all.40 = bf16[16,16,256]{2,1,0:T(8,128)(2,1)S(1)} all-to-all(bf16[16,16,256]{2,1,0:T(8,128)(2,1)S(1)} %shard_map.143), channel_id=1, replica_groups=mesh['grp'=2,'tp'=16,'dp'=16] {'tp'}, dimensions={0} | all-to-all | bytes 262144 | tf_op jit(solution)/shard_map/all_to_all | solution.py:254
  136.7 0.7 copy-done.12
  137.4 17.7 %all_to_all.41.x_ref = bf16[16,16,256]{2,1,0:T(8,128)(2,1)S(1)} all-to-all(bf16[16,16,256]{2,1,0:T(8,128)(2,1)S(1)} %bitcast.44), channel_id=1, replica_groups=mesh['grp'=2,'tp'=16,'dp'=16] {'tp'}, dimensions={0} | all-to-all | bytes 262144 | tf_op jit(solution)/shard_map/all_to_all | solution.py:254
  155.1 0.8 shard_map.144
  155.9 2.0 collective-permute-start.3
  157.9 1.8 collective-permute-done.3.refs_7_
  159.7 0.8 shard_map.145
  160.5 21.3 %all_to_all.42.arrived_ref = bf16[32,56,128]{2,1,0:T(8,128)(2,1)S(1)} all-to-all(bf16[32,56,128]{2,1,0:T(8,128)(2,1)S(1)} %bitcast.36), channel_id=1, replica_groups={{0,1,2,3,4,5,6,7,8,9,10,11,12,13,14,15,16,17,18,19,20,21,22,23,24,25,26..., dimensions={0} | all-to-all | bytes 917504 | tf_op jit(solution)/shard_map/all_to_all | solution.py:254
  181.9 2.8 %shard_map.146 = (bf16[32,128]{1,0:T(8,128)(2,1)S(1)}, f32[2,512,128]{2,1,0:T(8,128)}) custom-call(bf16[32,56,128]{2,1,0:T(8,128)(2,1)S(1)} %all_to_all.42.arrived_ref, s32[8]{0:T(128)S(1)} %copy-done.11, f32[2,128]{1,0:T(2,128)S(1)} %copy-done.9, f32[2,128]{1,0:T(2,128)S(1)} %copy-done.10, ...), custom_call_target="tpu_custom_call", output_to_operand_aliasing={{1}: (5, {})} | custom-call | flops 100000000 | bytes 2000000 | tf_op jit(solution)/shard_map/pallas_call | solution.py:235
  184.7 14.1 %all_to_all.43 = bf16[32,16,128]{2,1,0:T(8,128)(2,1)S(1)} all-to-all(bf16[32,16,128]{2,1,0:T(8,128)(2,1)S(1)} %bitcast.43), channel_id=1, replica_groups={{0,1,2,3,4,5,6,7,8,9,10,11,12,13,14,15,16,17,18,19,20,21,22,23,24,25,26..., dimensions={0} | all-to-all | bytes 262144 | tf_op jit(solution)/shard_map/all_to_all | solution.py:254
  198.8 0.7 shard_map.147
  199.5 18.8 %all_to_all.44 = bf16[16,16,256]{2,1,0:T(8,128)(2,1)S(1)} all-to-all(bf16[16,16,256]{2,1,0:T(8,128)(2,1)S(1)} %shard_map.147), channel_id=1, replica_groups=mesh['grp'=2,'tp'=16,'dp'=16] {'tp'}, dimensions={0} | all-to-all | bytes 262144 | tf_op jit(solution)/shard_map/all_to_all | solution.py:254
  218.3 0.6 fusion
  (20 shorter events, 0.2 us)
Async XLA Ops:
  0.6 63.5 %copy-start.4 = (bf16[2,256,128]{2,1,0:T(8,128)(2,1)S(1)}, bf16[2,256,128]{2,1,0:T(8,128)(2,1)}, u32[]{:S(2)}) copy-start(bf16[2,256,128]{2,1,0:T(8,128)(2,1)} %refs_4_.7) | copy-start | bytes 393220
  0.6 63.5 %copy-start.5 = (bf16[2,256,128]{2,1,0:T(8,128)(2,1)S(1)}, bf16[2,256,128]{2,1,0:T(8,128)(2,1)}, u32[]{:S(2)}) copy-start(bf16[2,256,128]{2,1,0:T(8,128)(2,1)} %refs_5_.7) | copy-start | bytes 393220
  2.1 62.0 %copy-start = (bf16[2,256,128]{2,1,0:T(8,128)(2,1)S(1)}, bf16[2,256,128]{2,1,0:T(8,128)(2,1)}, u32[]{:S(2)}) copy-start(bf16[2,256,128]{2,1,0:T(8,128)(2,1)} %refs_0_.7) | copy-start | bytes 393220
  2.1 62.0 %copy-start.1 = (bf16[2,256,128]{2,1,0:T(8,128)(2,1)S(1)}, bf16[2,256,128]{2,1,0:T(8,128)(2,1)}, u32[]{:S(2)}) copy-start(bf16[2,256,128]{2,1,0:T(8,128)(2,1)} %refs_1_.7) | copy-start | bytes 393220
  2.1 62.0 %copy-start.2 = (bf16[2,256,128]{2,1,0:T(8,128)(2,1)S(1)}, bf16[2,256,128]{2,1,0:T(8,128)(2,1)}, u32[]{:S(2)}) copy-start(bf16[2,256,128]{2,1,0:T(8,128)(2,1)} %refs_2_.7) | copy-start | bytes 393220
  2.1 62.0 %copy-start.3 = (bf16[2,256,128]{2,1,0:T(8,128)(2,1)S(1)}, bf16[2,256,128]{2,1,0:T(8,128)(2,1)}, u32[]{:S(2)}) copy-start(bf16[2,256,128]{2,1,0:T(8,128)(2,1)} %refs_3_.7) | copy-start | bytes 393220
  2.1 62.0 %all-to-all-start = ((bf16[16,32,256]{2,1,0:T(8,128)(2,1)}), bf16[16,32,256]{2,1,0:T(8,128)(2,1)S(1)}, u32[]{:S(2)}, u32[]{:S(2)}) async-start(bf16[16,32,256]{2,1,0:T(8,128)(2,1)} %broadcast_in_dim.20), calls=%async_computation | async-start | bytes 524288 | tf_op jit(solution)/shard_map/all_to_all | solution.py:254
  46.0 18.1 %copy-start.8 = (f32[2,256]{1,0:T(2,128)S(1)}, f32[2,256]{1,0:T(2,128)}, u32[]{:S(2)}) copy-start(f32[2,256]{1,0:T(2,128)} %gain_ref.10) | copy-start | bytes 6148
  46.1 20.9 %copy-start.7 = (bf16[2,128,256]{2,1,0:T(8,128)(2,1)S(1)}, bf16[2,128,256]{2,1,0:T(8,128)(2,1)}, u32[]{:S(2)}) copy-start(bf16[2,128,256]{2,1,0:T(8,128)(2,1)} %own_ref.3) | copy-start | bytes 393220
  65.0 5.6 %collective-permute-start = (bf16[1,16,104,128]{3,2,1,0:T(8,128)(2,1)S(1)}, bf16[1,16,104,128]{3,2,1,0:T(8,128)(2,1)S(1)}, u32[]{:S(2)}, u32[]{:S(2)}) collective-permute-start(bf16[1,16,104,128]{3,2,1,0:T(8,128)(2,1)S(1)} %shard_map.140), channel_id=1, source_target_pairs={{0,1},{1,0},{2,3},{3,2},{4,5},{5,4},{6,7},{7,6},{8,9},{9,8},{10,11... | collective-permute-start | bytes 1277960 | tf_op jit(solution)/shard_map/ppermute | solution.py:258
  66.9 13.1 %collective-permute-start.1 = (bf16[2,128,256]{2,1,0:T(8,128)(2,1)S(1)}, bf16[2,128,256]{2,1,0:T(8,128)(2,1)S(1)}, u32[]{:S(2)}, u32[]{:S(2)}) collective-permute-start(bf16[2,128,256]{2,1,0:T(8,128)(2,1)S(1)} %copy-done.7), channel_id=1, source_target_pairs={{0,16},{16,0},{32,48},{48,32},{64,80},{80,64},{96,112},{112,96},{1... | collective-permute-start | bytes 393224 | tf_op jit(solution)/shard_map/ppermute | solution.py:258
  72.1 21.8 %copy-start.6 = (f32[2,8,2,4096]{3,2,1,0:T(2,128)S(1)}, f32[2,8,2,4096]{3,2,1,0:T(2,128)}, u32[]{:S(2)}) copy-start(f32[2,8,2,4096]{3,2,1,0:T(2,128)} %param.25) | copy-start | bytes 1572868
  72.1 21.8 %all-to-all-start.1 = ((bf16[16,104,128]{2,1,0:T(8,128)(2,1)}), bf16[16,104,128]{2,1,0:T(8,128)(2,1)S(1)}, u32[]{:S(2)}, u32[]{:S(2)}) async-start(bf16[16,104,128]{2,1,0:T(8,128)(2,1)} %bitcast.2), calls=%async_computation.1 | async-start | bytes 851968 | tf_op jit(solution)/shard_map/all_to_all | solution.py:254
  80.0 14.0 %copy-start.10 = (f32[2,128]{1,0:T(2,128)S(1)}, f32[2,128]{1,0:T(2,128)}, u32[]{:S(2)}) copy-start(f32[2,128]{1,0:T(2,128)} %gain_ref.11) | copy-start | bytes 3076
  80.0 13.9 %copy-start.9 = (f32[2,128]{1,0:T(2,128)S(1)}, f32[2,128]{1,0:T(2,128)}, u32[]{:S(2)}) copy-start(f32[2,128]{1,0:T(2,128)} %base_ref.3) | copy-start | bytes 3076
  80.0 13.9 %copy-start.11 = (s32[8]{0:T(128)S(1)}, s32[8]{0:T(128)}, u32[]{:S(2)}) copy-start(s32[8]{0:T(128)} %lengths_ref.3) | copy-start | bytes 100
  97.4 18.5 %all-to-all-start.2 = ((bf16[32,16,128]{2,1,0:T(8,128)(2,1)}), bf16[32,16,128]{2,1,0:T(8,128)(2,1)S(1)}, u32[]{:S(2)}, u32[]{:S(2)}) async-start(bf16[32,16,128]{2,1,0:T(8,128)(2,1)} %bitcast.7), calls=%async_computation.2 | async-start | bytes 262144 | tf_op jit(solution)/shard_map/all_to_all | solution.py:254
  102.3 13.6 %collective-permute-start.2 = (bf16[6,256,128]{2,1,0:T(8,128)(2,1)S(1)}, bf16[6,256,128]{2,1,0:T(8,128)(2,1)S(1)}, u32[]{:S(2)}, u32[]{:S(2)}) collective-permute-start(bf16[6,256,128]{2,1,0:T(8,128)(2,1)S(1)} %slice_dynamic-update-slice_fusion), channel_id=1, source_target_pairs={{0,16},{16,0},{32,48},{48,32},{64,80},{80,64},{96,112},{112,96},{1... | collective-permute-start | bytes 1179656 | tf_op jit(solution)/shard_map/ppermute | solution.py:258
  136.7 0.7 copy-start.12
  155.9 3.7 %collective-permute-start.3 = (bf16[2,16,56,128]{3,2,1,0:T(8,128)(2,1)S(1)}, bf16[2,16,56,128]{3,2,1,0:T(8,128)(2,1)S(1)}, u32[]{:S(2)}, u32[]{:S(2)}) collective-permute-start(bf16[2,16,56,128]{3,2,1,0:T(8,128)(2,1)S(1)} %shard_map.144), channel_id=1, source_target_pairs={{0,1},{1,0},{2,3},{3,2},{4,5},{5,4},{6,7},{7,6},{8,9},{9,8},{10,11... | collective-permute-start | bytes 1376264 | tf_op jit(solution)/shard_map/ppermute | solution.py:258

commit v4 on v3

--- a/solution.py
+++ b/solution.py
@@ -32,44 +32,75 @@
     )
 
 
-def project_kernel(layer, far, groups, place_ref, x_ref, gain_ref, *refs):
+def squares_tail(row):
+    pick = iota((8, LANES), 0)
+    high = row.astype(jnp.bfloat16).astype(jnp.float32)
+    return jnp.where(pick == 0, high, jnp.where(pick == 1, row - high, 0.0)).astype(jnp.bfloat16)
+
+
+def project_kernel(far, place_ref, x_ref, gain_ref, *refs):
     out_ref = refs[-1]
-    core, column = place_ref[0], place_ref[1]
     blocks, rows, depth = x_ref.shape
     half = rows // 2
-    first_half = core == (1 if far else 0)
+    first_half = place_ref[0] == (1 if far else 0)
     x = x_ref[...].astype(jnp.float32)
     x = jnp.where(first_half, x[:, :half], x[:, half:]).reshape(blocks * half, depth)
-    scaled = (x * gain_ref[layer : layer + 1, :]).astype(jnp.bfloat16)
+    scaled = (x * gain_ref[0:1, :]).astype(jnp.bfloat16)
     squares = jnp.sum(x * x, -1, keepdims=True)
     eye = iota((half, LANES), 0) == iota((half, LANES), 1)
-    pick = iota((8, LANES), 0)
-    for group in range(groups):
-        owner = jnp.bitwise_xor(column, group) if groups > 1 else 0
+    for first in range(0, 6, 2):
+        pair = jnp.concatenate([refs[first][0], refs[first + 1][0]], 1)
+        product = jnp.dot(scaled, pair, preferred_element_type=jnp.float32)
+        for side in range(2):
+            part = product[:, side * LANES : (side + 1) * LANES].reshape(blocks, half, LANES)
+            where = pl.ds((first + side) * half, half)
+            if not far:
+                part = part + refs[-2][:, where, :].astype(jnp.float32)
+            out_ref[:, where, :] = part.astype(jnp.bfloat16)
+    for block in range(blocks):
+        row = jnp.sum(
+            jnp.where(eye, squares[block * half : (block + 1) * half], 0.0), 0, keepdims=True
+        )
+        if not far:
+            came = refs[-2][block, pl.ds(6 * half, 8), :].astype(jnp.float32)
+            row = row + came[0:1] + came[1:2]
+        out_ref[block, pl.ds(6 * half, 8), :] = squares_tail(row)
+
+
+def project_pair_kernel(place_ref, x_ref, gain_ref, packed_ref, *refs):
+    *weight_refs, other_ref, core_own_ref, core_other_ref, out_ref = refs
+    column = place_ref[1]
+    blocks, rows, both = x_ref.shape
+    depth = both // 2
+    x = x_ref[...].astype(jnp.float32).reshape(blocks * rows, both)
+    core_gain = packed_ref[pl.ds(packed_ref.shape[0] - 16, 16), :].astype(jnp.float32)
+    core_gain = core_gain[0:1] + core_gain[1:2] + core_gain[2:3]
+    own_scaled = (x[:, :depth] * gain_ref[1:2, :]).astype(jnp.bfloat16)
+    core_scaled = (x[:, depth:] * core_gain).astype(jnp.bfloat16)
+    squares = jnp.sum(x * x, -1, keepdims=True)
+    eye = iota((rows, LANES), 0) == iota((rows, LANES), 1)
+    for group in range(2):
+        member = jnp.bitwise_xor(column, group)
         for first in range(0, 6, 2):
             if group:
-                pair = [refs[6][first], refs[6][first + 1]]
+                near = [other_ref[first], other_ref[first + 1]]
+                core = [core_other_ref[first], core_other_ref[first + 1]]
             else:
-                pair = [refs[first][layer], refs[first + 1][layer]]
+                near = [weight_refs[first][1], weight_refs[first + 1][1]]
+                core = [core_own_ref[first], core_own_ref[first + 1]]
             product = jnp.dot(
-                scaled, jnp.concatenate(pair, 1), preferred_element_type=jnp.float32
-            )
+                own_scaled, jnp.concatenate(near, 1), preferred_element_type=jnp.float32
+            ) + jnp.dot(core_scaled, jnp.concatenate(core, 1), preferred_element_type=jnp.float32)
             for side in range(2):
-                part = product[:, side * LANES : (side + 1) * LANES].reshape(blocks, half, LANES)
-                where = pl.ds((first + side) * half, half)
-                if not far:
-                    part = part + refs[-2][owner, :, where, :].astype(jnp.float32)
-                out_ref[owner, :, where, :] = part.astype(jnp.bfloat16)
+                part = product[:, side * LANES : (side + 1) * LANES]
+                out_ref[member, :, pl.ds((first + side) * rows, rows), :] = part.reshape(
+                    blocks, rows, LANES
+                ).astype(jnp.bfloat16)
         for block in range(blocks):
             row = jnp.sum(
-                jnp.where(eye, squares[block * half : (block + 1) * half], 0.0), 0, keepdims=True
+                jnp.where(eye, squares[block * rows : (block + 1) * rows], 0.0), 0, keepdims=True
             )
-            if not far:
-                came = refs[-2][owner, block, pl.ds(6 * half, 8), :].astype(jnp.float32)
-                row = row + came[0:1] + came[1:2]
-            high = row.astype(jnp.bfloat16).astype(jnp.float32)
-            tail = jnp.where(pick == 0, high, jnp.where(pick == 1, row - high, 0.0))
-            out_ref[owner, block, pl.ds(6 * half, 8), :] = tail.astype(jnp.bfloat16)
+            out_ref[member, block, pl.ds(6 * rows, 8), :] = squares_tail(row)
 
 
 def advance_kernel(layer, rows, width, arrived_ref, lengths_ref, base_ref, gain_ref, state_ref, *refs):
@@ -138,7 +169,9 @@
         against = jnp.concatenate(
             [(s * spread(1, t)).reshape(HEAD, LANES) for s, t in zip(state, tokens)], 0
         )
-        removed = split_dot(against, same_head)
+        removed = jnp.dot(
+            against.astype(jnp.bfloat16), same_head, preferred_element_type=jnp.float32
+        )
         written = jnp.concatenate(
             [jnp.where(place_mask, line_ref[10, pl.ds(t, 1), :], 0.0) for t in tokens], 0
         ).astype(jnp.bfloat16)
@@ -153,7 +186,9 @@
         read = jnp.concatenate(
             [(s * spread(4, t)).reshape(HEAD, LANES) for s, t in zip(state, tokens)], 0
         )
-        read = split_dot(read, parity_back)
+        read = jnp.dot(
+            read.astype(jnp.bfloat16), parity_back, preferred_element_type=jnp.float32
+        )
         for seq, t in enumerate(tokens):
             part = slice(seq * HEAD, (seq + 1) * HEAD)
             read_ref[pl.ds(t, 1), :] = jnp.sum(
@@ -165,24 +200,65 @@
     centred = read - split_dot(read, same_head) / HEAD
     variance = split_dot(centred * centred, same_head) / HEAD
     normed = centred * lax.rsqrt(variance + group_epsilon) * gain_ref[layer : layer + 1, :]
-    mixed_ref[...] = jnp.where(live, normed * jax.nn.sigmoid(gate_pre), 0.0).astype(jnp.bfloat16)
+    mixed = jnp.where(live, normed * jax.nn.sigmoid(gate_pre), 0.0)
+    members, owners, share, _ = mixed_ref.shape
+    for member in range(members):
+        for owner in range(owners):
+            start = member * (rows // members) + (owner % 2) * share * (share * members < rows)
+            mixed_ref[member, owner] = mixed[start : start + share].astype(jnp.bfloat16)
 
 
 def out_kernel(layer, place_ref, mixed_ref, own_ref, other_ref, *refs):
     out_ref = refs[-1]
     _, blocks, rows, _ = mixed_ref.shape
+    depth = own_ref.shape[2]
     first = place_ref[1] == 0
-    own, other = own_ref[layer], other_ref[layer]
-    total = 0.0
-    for member, matrix in enumerate(
-        (jnp.where(first, own, other), jnp.where(first, other, own))
-    ):
-        total += jnp.dot(
-            mixed_ref[member].reshape(blocks * rows, LANES),
-            matrix,
-            preferred_element_type=jnp.float32,
-        )
-    out_ref[...] = total.astype(jnp.bfloat16).reshape(out_ref.shape)
+    sides = [(own_ref[layer], other_ref[layer])]
+    if layer == 0:
+        sides.append((refs[0][pl.ds(0, LANES), :], refs[0][pl.ds(LANES, LANES), :]))
+    for side, (own, other) in enumerate(sides):
+        total = 0.0
+        for member, matrix in enumerate(
+            (jnp.where(first, own, other), jnp.where(first, other, own))
+        ):
+            lines = mixed_ref[member].astype(jnp.float32).reshape(blocks * rows, LANES)
+            total += jnp.dot(
+                lines.astype(jnp.bfloat16), matrix, preferred_element_type=jnp.float32
+            )
+        out_ref[:, :, pl.ds(side * depth, depth)] = total.reshape(blocks, rows, depth).astype(
+            jnp.bfloat16
+        )
+
+
+def settle_kernel(place_ref, summed_ref, tokens_ref, packed_ref, *refs):
+    rows_ref, spread_ref = refs[-2:]
+    columns, rows, _ = summed_ref.shape
+    first = place_ref[0] == 0
+    for member in range(2):
+        total = summed_ref[member].astype(jnp.float32)
+        for column in range(member + 2, columns, 2):
+            total += summed_ref[column].astype(jnp.float32)
+        near = tokens_ref[pl.ds(member * 2 * rows, 2 * rows), :].astype(jnp.float32)
+        near = jnp.where(first, near[:rows], near[rows:])
+        core = packed_ref[pl.ds(2 * LANES, 2 * rows), :].astype(jnp.float32)
+        core = core[member * rows : (member + 1) * rows]
+        total = (total + jnp.concatenate([near, core], 1)).astype(jnp.bfloat16)
+        rows_ref[member] = total
+        for column in range(member, columns, 2):
+            spread_ref[column] = total
+
+
+def finish_kernel(place_ref, summed_ref, rows_ref, back_ref, out_ref):
+    columns, half, depth = summed_ref.shape
+    first = place_ref[0] == 0
+    for member in range(2):
+        total = summed_ref[member].astype(jnp.float32)
+        for column in range(member + 2, columns, 2):
+            total += summed_ref[column].astype(jnp.float32)
+        near = rows_ref[member].astype(jnp.float32)[:, :depth]
+        core = back_ref[member].astype(jnp.float32)
+        held = jnp.concatenate([jnp.where(first, near, core), jnp.where(first, core, near)], 0)
+        out_ref[pl.ds(member * half, half), :] = (total + held).astype(jnp.bfloat16)
 
 
 def params():
@@ -194,31 +270,23 @@
     }
 
 
-def project(layer, far, place, x, gain, weights, others, came):
-    blocks, rows, _ = x.shape
-    groups = 1 if others is None else 2
-    extra = ([] if others is None else [others]) + ([] if came is None else [came])
+def call(kernel, outs, *operands, awaited=()):
     return pl.pallas_call(
-        functools.partial(project_kernel, layer, far, groups),
-        out_shape=jax.ShapeDtypeStruct((groups, blocks, 3 * rows + 8, LANES), jnp.bfloat16),
-        in_specs=[SMEM] + [VMEM] * (8 + len(extra)),
-        out_specs=VMEM,
+        kernel,
+        out_shape=outs,
+        in_specs=[SMEM]
+        + [VMEM] * (len(operands) - 1)
+        + [pl.BlockSpec(memory_space=pl.ANY)] * len(awaited),
+        out_specs=jax.tree.map(lambda _: VMEM, outs),
         **params(),
-    )(place, x, gain, *weights, *extra)
-
-
-def project_out(layer, place, mixed, own, other, awaited):
-    _, blocks, rows, _ = mixed.shape
-    return pl.pallas_call(
-        functools.partial(out_kernel, layer),
-        out_shape=jax.ShapeDtypeStruct((blocks, rows, own.shape[2]), jnp.bfloat16),
-        in_specs=[SMEM] + [VMEM] * 3 + [pl.BlockSpec(memory_space=pl.ANY)] * len(awaited),
-        out_specs=VMEM,
-        **params(),
-    )(place, mixed, own, other, *awaited)
-
-
-def advance(layer, width, arrived, lengths, base, gain, states, held, awaited):
+    )(*operands, *awaited)
+
+
+def bf16(*shape):
+    return jax.ShapeDtypeStruct(shape, jnp.bfloat16)
+
+
+def advance(layer, width, shared, arrived, lengths, base, gain, states, held, awaited):
     rows = lengths.shape[0] * NEW
     state_rows = states.shape[1]
     block = pl.BlockSpec((1, state_rows, LANES), lambda i: (layer, 0, 0))
@@ -236,11 +304,11 @@
         functools.partial(advance_kernel, layer, rows, width),
         grid=(1,),
         out_shape=(
-            jax.ShapeDtypeStruct((rows, LANES), jnp.bfloat16),
+            jax.ShapeDtypeStruct(shared, jnp.bfloat16),
             jax.ShapeDtypeStruct(states.shape, jnp.float32),
         ),
         in_specs=in_specs,
-        out_specs=(pl.BlockSpec((rows, LANES), lambda i: (0, 0)), block),
+        out_specs=(pl.BlockSpec(shared, lambda i: (0, 0, 0, 0)), block),
         scratch_shapes=[
             pltpu.VMEM((11, rows, LANES), jnp.float32),
             pltpu.VMEM((rows, LANES), jnp.float32),
@@ -286,41 +354,83 @@
         [column * owners + owner for column in (first, first + 1) for owner in range(owners)]
         for first in range(0, columns, 2)
     ]
-    half = own_count // 2
+    half, quarter = own_count // 2, own_count // 4
+    core = place[0]
+    gathered = exchange(jnp.broadcast_to(tokens, (columns, own_count, depth)), "tp")
     other_out = from_partner(w_out, "tp")
-    other_weights = from_partner(jnp.stack([weight[1] for weight in weights]), "tp")
-    own_rows = tokens
-    held = None
-    for layer in range(2):
-        if layer == 0:
-            spread = jnp.broadcast_to(own_rows, (columns, own_count, depth))
-            others = None
-        else:
-            spread = jnp.broadcast_to(
-                own_rows.reshape(2, half, depth), (columns // 2, 2, half, depth)
-            ).reshape(columns, half, depth)
-            others = other_weights
-        gathered = exchange(spread, "tp")
-        far = project(layer, True, place, gathered, norm_gain, weights, others, None)
-        came = from_partner(far, "dp")
-        near = project(layer, False, place, gathered, norm_gain, weights, others, came)
-        near = near.reshape(-1, *near.shape[2:])
-        arrived = exchange(near, "dp") if layer == 0 else exchange(near, both, pairs)
-        mixed, held = advance(
-            layer, width, arrived, lengths, decay_base, group_gain, folded, held,
-            [] if layer else [other_out],
-        )
-        shared = jnp.broadcast_to(mixed.reshape(2, 1, half, LANES), (2, owners, half, LANES))
-        shared = exchange(shared.reshape(2 * owners, half, LANES), both, pairs)
-        product = project_out(
-            layer, place, shared.reshape(2, owners, half, LANES), w_out, other_out,
-            [] if layer else [other_weights],
-        )
-        summed = exchange(product, "tp").astype(jnp.float32)
-        summed = jnp.sum(summed.reshape(columns // 2, 2, half, depth), 0)
-        own_rows = (
-            own_rows.astype(jnp.float32) + summed.reshape(own_count, depth)
-        ).astype(jnp.bfloat16)
+    own_weights = jnp.stack([weight[1] for weight in weights])
+    other_weights = from_partner(own_weights, "tp")
+    quarters = tokens.reshape(2, 2, quarter, depth)
+    quarters = jnp.where(core == 0, quarters[:, 1], quarters[:, 0])
+    gain_line = norm_gain[1:2]
+    gain_lines = []
+    for _ in range(3):
+        term = lax.reduce_precision(gain_line, 8, 7)
+        gain_lines.append(term.astype(jnp.bfloat16))
+        gain_line = gain_line - term
+    packed = jnp.concatenate(
+        [
+            w_out[0],
+            other_out[0],
+            quarters.reshape(half, depth),
+            *gain_lines,
+            jnp.zeros((13, depth), jnp.bfloat16),
+        ],
+        0,
+    )
+    packed = from_partner(packed, "dp")
+    core_own = from_partner(own_weights, "dp")
+    core_other = from_partner(other_weights, "dp")
+    far = call(
+        functools.partial(project_kernel, True),
+        bf16(columns, 3 * own_count + 8, LANES),
+        place, gathered, norm_gain, *weights,
+    )
+    came = from_partner(far, "dp")
+    near = call(
+        functools.partial(project_kernel, False),
+        bf16(columns, 3 * own_count + 8, LANES),
+        place, gathered, norm_gain, *weights, came,
+    )
+    arrived = exchange(near, "dp")
+    shared, held = advance(
+        0, width, (2, owners, quarter, LANES), arrived, lengths, decay_base, group_gain,
+        folded, None, [other_out],
+    )
+    shared = exchange(shared.reshape(2 * owners, quarter, LANES), both, pairs)
+    product = call(
+        functools.partial(out_kernel, 0),
+        bf16(columns, quarter, 2 * depth),
+        place, shared.reshape(2, owners, quarter, LANES), w_out, other_out, packed,
+        awaited=[other_weights],
+    )
+    summed = exchange(product, "tp")
+    rows, spread = call(
+        settle_kernel,
+        (bf16(2, quarter, 2 * depth), bf16(columns, quarter, 2 * depth)),
+        place, summed, tokens, packed,
+        awaited=[core_own, core_other],
+    )
+    gathered = exchange(spread, "tp")
+    near = call(
+        project_pair_kernel,
+        bf16(2, columns, 6 * quarter + 8, LANES),
+        place, gathered, norm_gain, packed, *weights, other_weights, core_own, core_other,
+    )
+    arrived = exchange(near.reshape(-1, *near.shape[2:]), both, pairs)
+    back = from_partner(rows[:, :, depth:], "dp")
+    shared, held = advance(
+        1, width, (2, owners, half, LANES), arrived, lengths, decay_base, group_gain,
+        folded, held, [],
+    )
+    shared = exchange(shared.reshape(2 * owners, half, LANES), both, pairs)
+    product = call(
+        functools.partial(out_kernel, 1),
+        bf16(columns, half, depth),
+        place, shared.reshape(2, owners, half, LANES), w_out, other_out,
+    )
+    summed = exchange(product, "tp")
+    own_rows = call(finish_kernel, bf16(own_count, depth), place, summed, rows, back)
     new_states = jnp.swapaxes(held.reshape(blocks, seqs, HEAD // 2, heads, LANES), 2, 3)
     return (own_rows, new_states.reshape(states.shape))
 

time: 220 us -> 207 us (0.941)
  blocking collectives: 92 us -> 51.1 us
  starting transfers between devices: 67.2 us -> 86.3 us
  waiting for transfers between devices: 44 us -> 52 us
    all_to_all x5 -> x3, blocking collectives: 92 us -> 51.1 us  [exchange(): return lax.all_to_all(x, axis, 0, 0, tiled=True, axis_index_groups=groups)]
    all_to_all x3 -> x5, waiting for transfers between devices: 31.9 us -> 46.5 us  [exchange(): return lax.all_to_all(x, axis, 0, 0, tiled=True, axis_index_groups=groups)]
    all_to_all x3 -> x5, starting transfers between devices: 56.4 us -> 67.4 us  [exchange(): return lax.all_to_all(x, axis, 0, 0, tiled=True, axis_index_groups=groups)]
    ppermute x4 -> x7, starting transfers between devices: 10.8 us -> 18.9 us  [from_partner(): lax.ppermute(x, axis, [(i, i ^ 1) for i in range(lax.axis_size(axis))])]
    ppermute x4 -> x7, waiting for transfers between devices: 12.1 us -> 5.5 us  [from_partner(): lax.ppermute(x, axis, [(i, i ^ 1) for i in range(lax.axis_size(axis))])]
    pallas_call x6 -> x7, Pallas kernels: 5.54 us -> 7.86 us  [call(): pl.pallas_call(kernel, out_shape=outs, in_specs=[SMEM] + [VMEM] * (len(op...]
  transfers between devices with their start and end apart: 7 -> 12, of which waited for: 4 -> 9; matrix products, arithmetic and copies ran while one was open for 0% -> 0% of each run, Pallas kernels for 1% -> 2%
where the time goes in v4:
time: 207 us; the launch traced here: 206 us
  starting transfers between devices  86.3 us (42%)
  waiting for transfers between devices  52 us (25%)
  blocking collectives  51.1 us (25%)
  Pallas kernels  13 us (6%)
  local copies, waits for them, and re-layouts  2.61 us (1%)
    all_to_all x5, starting transfers between devices, exchange(): return lax.all_to_all(x, axis, 0, 0, tiled=True, axis_index_groups=groups)  67.4 us
    all_to_all x3, blocking collectives, exchange(): return lax.all_to_all(x, axis, 0, 0, tiled=True, axis_index_groups=groups)  51.1 us
    all_to_all x5, waiting for transfers between devices, exchange(): return lax.all_to_all(x, axis, 0, 0, tiled=True, axis_index_groups=groups)  46.5 us
    ppermute x7, starting transfers between devices, from_partner(): lax.ppermute(x, axis, [(i, i ^ 1) for i in range(lax.axis_size(axis))])  18.9 us
    pallas_call x7, Pallas kernels, call(): pl.pallas_call(kernel, out_shape=outs, in_specs=[SMEM] + [VMEM] * (len(op...  7.86 us
    ppermute x7, waiting for transfers between devices, from_partner(): lax.ppermute(x, axis, [(i, i ^ 1) for i in range(lax.axis_size(axis))])  5.5 us
    pallas_call x2, Pallas kernels, advance(): pl.pallas_call(functools.partial(advance_kernel, layer, rows, width), gri...  5.12 us
  transfers between devices with their start and end apart: 12, of which 9 were waited for; matrix products, arithmetic and copies ran while one was open for 0% of the time, Pallas kernels for 2%

profile of v4, /device:TPU:80, one launch (start us, length us, event | category | flops | bytes accessed | tf_op | source)
XLA Modules:
  0.0 206.1 jit_solution(17177036984042845116)
XLA Ops:
  0.6 1.4 broadcast_in_dim.6
  2.1 43.8 %all-to-all-start = ((bf16[16,32,256]{2,1,0:T(8,128)(2,1)}), bf16[16,32,256]{2,1,0:T(8,128)(2,1)S(1)}, u32[]{:S(2)}, u32[]{:S(2)}) async-start(bf16[16,32,256]{2,1,0:T(8,128)(2,1)} %broadcast_in_dim.6), calls=%async_computation | async-start | bytes 524288 | tf_op jit(solution)/shard_map/all_to_all | solution.py:322
  45.9 0.0 copy-start.2
  45.9 3.8 %collective-permute-start.1 = (bf16[2,128,256]{2,1,0:T(8,128)(2,1)S(1)}, bf16[2,128,256]{2,1,0:T(8,128)(2,1)S(1)}, u32[]{:S(2)}, u32[]{:S(2)}) collective-permute-start(bf16[2,128,256]{2,1,0:T(8,128)(2,1)S(1)} %copy-done.7), channel_id=1, source_target_pairs={{0,16},{16,0},{32,48},{48,32},{64,80},{80,64},{96,112},{112,96},{1... | collective-permute-start | bytes 393224 | tf_op jit(solution)/shard_map/ppermute | solution.py:326
  49.8 0.1 pad_add_fusion.place_ref
  49.9 0.0 copy-start.4
  49.9 0.9 copy-done.3
  50.8 13.3 %all-to-all-done.x_ref = bf16[16,32,256]{2,1,0:T(8,128)(2,1)S(1)} async-done(((bf16[16,32,256]{2,1,0:T(8,128)(2,1)}), bf16[16,32,256]{2,1,0:T(8,128)(2,1)S(1)}, u32[]{:S(2)}, u32[]{:S(2)}) %all-to-all-start) | async-done | bytes 262176 | tf_op jit(solution)/shard_map/all_to_all | solution.py:322
  64.1 0.0 copy-done.9
  64.1 0.8 shard_map.140
  64.9 2.0 collective-permute-start
  66.9 1.7 collective-permute-done.refs_6_
  68.6 1.6 shard_map.141
  70.2 7.8 %all-to-all-start.1 = ((bf16[16,104,128]{2,1,0:T(8,128)(2,1)}), bf16[16,104,128]{2,1,0:T(8,128)(2,1)S(1)}, u32[]{:S(2)}, u32[]{:S(2)}) async-start(bf16[16,104,128]{2,1,0:T(8,128)(2,1)} %shard_map.141), calls=%async_computation.1 | async-start | bytes 851968 | tf_op jit(solution)/shard_map/all_to_all | solution.py:322
  77.9 0.0 copy-start.8
  78.0 4.9 %collective-permute-start.3 = (bf16[6,256,128]{2,1,0:T(8,128)(2,1)S(1)}, bf16[6,256,128]{2,1,0:T(8,128)(2,1)S(1)}, u32[]{:S(2)}, u32[]{:S(2)}) collective-permute-start(bf16[6,256,128]{2,1,0:T(8,128)(2,1)S(1)} %slice_dynamic-update-slice_fusion), channel_id=1, source_target_pairs={{0,16},{16,0},{32,48},{48,32},{64,80},{80,64},{96,112},{112,96},{1... | collective-permute-start | bytes 1179656 | tf_op jit(solution)/shard_map/ppermute | solution.py:326
  82.9 0.0 copy-start.11
  82.9 0.0 copy-start.10
  82.9 0.0 copy-start.12
  83.0 0.0 collective-permute-done.1.refs_0_.other_ref
  83.0 9.0 %all-to-all-done.1.arrived_ref = bf16[16,104,128]{2,1,0:T(8,128)(2,1)S(1)} async-done(((bf16[16,104,128]{2,1,0:T(8,128)(2,1)}), bf16[16,104,128]{2,1,0:T(8,128)(2,1)S(1)}, u32[]{:S(2)}, u32[]{:S(2)}) %all-to-all-start.1) | async-done | bytes 426016 | tf_op jit(solution)/shard_map/all_to_all | solution.py:322
  91.9 0.0 copy-done
  92.0 2.7 %shard_map.142 = (bf16[2,16,8,128]{3,2,1,0:T(8,128)(2,1)}, f32[2,512,128]{2,1,0:T(8,128)}) custom-call(bf16[16,104,128]{2,1,0:T(8,128)(2,1)S(1)} %all-to-all-done.1.arrived_ref, s32[8]{0:T(128)S(1)} %copy-done.12, f32[2,128]{1,0:T(2,128)S(1)} %copy-done.10, f32[2,128]{1,0:T(2,128)S(1)} %copy-done.11, f32[2,512,128]{2,1,0:T(8,128)S(1)} %bitcast.34, ...), custom_call_target="tpu_custom_call" | custom-call | flops 100000000 | bytes 2000000 | tf_op jit(solution)/shard_map/pallas_call | solution.py:303
  94.7 7.2 %all-to-all-start.2 = ((bf16[32,8,128]{2,1,0:T(8,128)(2,1)}), bf16[32,8,128]{2,1,0:T(8,128)(2,1)S(1)}, u32[]{:S(2)}, u32[]{:S(2)}) async-start(bf16[32,8,128]{2,1,0:T(8,128)(2,1)} %bitcast.5), calls=%async_computation.2 | async-start | bytes 131072 | tf_op jit(solution)/shard_map/all_to_all | solution.py:322
  102.0 0.2 concatenate.3
  102.1 2.0 collective-permute-start.2
  104.1 1.3 collective-permute-done.2.refs_0_.packed_ref
  105.4 0.0 collective-permute-done.3.refs_1_.refs_6_
  105.4 4.5 %all-to-all-done.2 = bf16[32,8,128]{2,1,0:T(8,128)(2,1)S(1)} async-done(((bf16[32,8,128]{2,1,0:T(8,128)(2,1)}), bf16[32,8,128]{2,1,0:T(8,128)(2,1)S(1)}, u32[]{:S(2)}, u32[]{:S(2)}) %all-to-all-start.2) | async-done | bytes 65568 | tf_op jit(solution)/shard_map/all_to_all | solution.py:322
  109.9 1.4 shard_map.143
  111.3 4.6 %all-to-all-start.3 = ((bf16[16,8,512]{2,1,0:T(8,128)(2,1)}), bf16[16,8,512]{2,1,0:T(8,128)(2,1)S(1)}, u32[]{:S(2)}, u32[]{:S(2)}) async-start(bf16[16,8,512]{2,1,0:T(8,128)(2,1)} %shard_map.143), calls=%async_computation.3 | async-start | bytes 262144 | tf_op jit(solution)/shard_map/all_to_all | solution.py:322
  116.0 2.0 collective-permute-start.4
  117.9 2.4 %collective-permute-start.5 = (bf16[6,256,128]{2,1,0:T(8,128)(2,1)S(1)}, bf16[6,256,128]{2,1,0:T(8,128)(2,1)S(1)}, u32[]{:S(2)}, u32[]{:S(2)}) collective-permute-start(bf16[6,256,128]{2,1,0:T(8,128)(2,1)S(1)} %collective-permute-done.3.refs_1_.refs_6_), channel_id=1, source_target_pairs={{0,1},{1,0},{2,3},{3,2},{4,5},{5,4},{6,7},{7,6},{8,9},{9,8},{10,11... | collective-permute-start | bytes 1179656 | tf_op jit(solution)/shard_map/ppermute | solution.py:326
  120.4 0.0 collective-permute-done.4.refs_0_.refs_7_
  120.4 1.3 collective-permute-done.5.refs_1_.refs_8_
  121.7 8.5 %all-to-all-done.3.summed_ref = bf16[16,8,512]{2,1,0:T(8,128)(2,1)S(1)} async-done(((bf16[16,8,512]{2,1,0:T(8,128)(2,1)}), bf16[16,8,512]{2,1,0:T(8,128)(2,1)S(1)}, u32[]{:S(2)}, u32[]{:S(2)}) %all-to-all-start.3) | async-done | bytes 131104 | tf_op jit(solution)/shard_map/all_to_all | solution.py:322
  130.2 0.6 shard_map.144
  130.8 18.5 %all_to_all.40.x_ref = bf16[16,8,512]{2,1,0:T(8,128)(2,1)S(1)} all-to-all(bf16[16,8,512]{2,1,0:T(8,128)(2,1)S(1)} %get-tuple-element.9), channel_id=1, replica_groups=mesh['grp'=2,'tp'=16,'dp'=16] {'tp'}, dimensions={0} | all-to-all | bytes 262144 | tf_op jit(solution)/shard_map/all_to_all | solution.py:322
  149.2 0.9 shard_map.145
  150.1 18.5 %all_to_all.41.arrived_ref = bf16[32,56,128]{2,1,0:T(8,128)(2,1)S(1)} all-to-all(bf16[32,56,128]{2,1,0:T(8,128)(2,1)S(1)} %bitcast.36), channel_id=1, replica_groups={{0,1,2,3,4,5,6,7,8,9,10,11,12,13,14,15,16,17,18,19,20,21,22,23,24,25,26..., dimensions={0} | all-to-all | bytes 917504 | tf_op jit(solution)/shard_map/all_to_all | solution.py:322
  168.7 2.4 %shard_map.146 = (bf16[2,16,16,128]{3,2,1,0:T(8,128)(2,1)S(1)}, f32[2,512,128]{2,1,0:T(8,128)}) custom-call(bf16[32,56,128]{2,1,0:T(8,128)(2,1)S(1)} %all_to_all.41.arrived_ref, s32[8]{0:T(128)S(1)} %copy-done.12, f32[2,128]{1,0:T(2,128)S(1)} %copy-done.10, f32[2,128]{1,0:T(2,128)S(1)} %copy-done.11, ...), custom_call_target="tpu_custom_call", output_to_operand_aliasing={{1}: (5, {})} | custom-call | flops 100000000 | bytes 2000000 | tf_op jit(solution)/shard_map/pallas_call | solution.py:303
  171.1 14.1 %all_to_all.42 = bf16[32,16,128]{2,1,0:T(8,128)(2,1)S(1)} all-to-all(bf16[32,16,128]{2,1,0:T(8,128)(2,1)S(1)} %bitcast.40), channel_id=1, replica_groups={{0,1,2,3,4,5,6,7,8,9,10,11,12,13,14,15,16,17,18,19,20,21,22,23,24,25,26..., dimensions={0} | all-to-all | bytes 262144 | tf_op jit(solution)/shard_map/all_to_all | solution.py:322
  185.2 1.4 shard_map.147
  186.6 4.0 %all-to-all-start.7 = ((bf16[16,16,256]{2,1,0:T(8,128)(2,1)}), bf16[16,16,256]{2,1,0:T(8,128)(2,1)S(1)}, u32[]{:S(2)}, u32[]{:S(2)}) async-start(bf16[16,16,256]{2,1,0:T(8,128)(2,1)} %shard_map.147), calls=%async_computation.7 | async-start | bytes 262144 | tf_op jit(solution)/shard_map/all_to_all | solution.py:322
  190.6 2.0 collective-permute-start.6
  192.5 1.1 collective-permute-done.6.back_ref
  193.7 11.2 %all-to-all-done.7.summed_ref = bf16[16,16,256]{2,1,0:T(8,128)(2,1)S(1)} async-done(((bf16[16,16,256]{2,1,0:T(8,128)(2,1)}), bf16[16,16,256]{2,1,0:T(8,128)(2,1)S(1)}, u32[]{:S(2)}, u32[]{:S(2)}) %all-to-all-start.7) | async-done | bytes 131104 | tf_op jit(solution)/shard_map/all_to_all | solution.py:322
  204.9 1.2 shard_map.148
  (29 shorter events, 0.1 us)
Async XLA Ops:
  2.1 43.8 %copy-start.7 = (bf16[2,128,256]{2,1,0:T(8,128)(2,1)S(1)}, bf16[2,128,256]{2,1,0:T(8,128)(2,1)}, u32[]{:S(2)}) copy-start(bf16[2,128,256]{2,1,0:T(8,128)(2,1)} %own_ref.3) | copy-start | bytes 393220
  2.1 47.8 %copy-start.1 = (bf16[2,256,128]{2,1,0:T(8,128)(2,1)S(1)}, bf16[2,256,128]{2,1,0:T(8,128)(2,1)}, u32[]{:S(2)}) copy-start(bf16[2,256,128]{2,1,0:T(8,128)(2,1)} %refs_0_.5) | copy-start | bytes 393220
  2.1 62.0 %copy-start.5 = (bf16[2,256,128]{2,1,0:T(8,128)(2,1)S(1)}, bf16[2,256,128]{2,1,0:T(8,128)(2,1)}, u32[]{:S(2)}) copy-start(bf16[2,256,128]{2,1,0:T(8,128)(2,1)} %refs_4_.5) | copy-start | bytes 393220
  2.1 62.0 %copy-start.6 = (bf16[2,256,128]{2,1,0:T(8,128)(2,1)S(1)}, bf16[2,256,128]{2,1,0:T(8,128)(2,1)}, u32[]{:S(2)}) copy-start(bf16[2,256,128]{2,1,0:T(8,128)(2,1)} %refs_5_.5) | copy-start | bytes 393220
  2.1 62.0 %all-to-all-start = ((bf16[16,32,256]{2,1,0:T(8,128)(2,1)}), bf16[16,32,256]{2,1,0:T(8,128)(2,1)S(1)}, u32[]{:S(2)}, u32[]{:S(2)}) async-start(bf16[16,32,256]{2,1,0:T(8,128)(2,1)} %broadcast_in_dim.6), calls=%async_computation | async-start | bytes 524288 | tf_op jit(solution)/shard_map/all_to_all | solution.py:322
  45.9 3.9 %copy-start.2 = (bf16[2,256,128]{2,1,0:T(8,128)(2,1)S(1)}, bf16[2,256,128]{2,1,0:T(8,128)(2,1)}, u32[]{:S(2)}) copy-start(bf16[2,256,128]{2,1,0:T(8,128)(2,1)} %refs_1_.5) | copy-start | bytes 393220
  45.9 37.0 %collective-permute-start.1 = (bf16[2,128,256]{2,1,0:T(8,128)(2,1)S(1)}, bf16[2,128,256]{2,1,0:T(8,128)(2,1)S(1)}, u32[]{:S(2)}, u32[]{:S(2)}) collective-permute-start(bf16[2,128,256]{2,1,0:T(8,128)(2,1)S(1)} %copy-done.7), channel_id=1, source_target_pairs={{0,16},{16,0},{32,48},{48,32},{64,80},{80,64},{96,112},{112,96},{1... | collective-permute-start | bytes 393224 | tf_op jit(solution)/shard_map/ppermute | solution.py:326
  49.8 0.9 copy-start.3
  49.9 14.2 %copy-start.4 = (bf16[2,256,128]{2,1,0:T(8,128)(2,1)S(1)}, bf16[2,256,128]{2,1,0:T(8,128)(2,1)}, u32[]{:S(2)}) copy-start(bf16[2,256,128]{2,1,0:T(8,128)(2,1)} %refs_3_.5) | copy-start | bytes 393220
  50.7 13.3 %copy-start.9 = (f32[2,256]{1,0:T(2,128)S(1)}, f32[2,256]{1,0:T(2,128)}, u32[]{:S(2)}) copy-start(f32[2,256]{1,0:T(2,128)} %gain_ref.8) | copy-start | bytes 6148
  64.9 3.7 %collective-permute-start = (bf16[16,104,128]{2,1,0:T(8,128)(2,1)S(1)}, bf16[16,104,128]{2,1,0:T(8,128)(2,1)S(1)}, u32[]{:S(2)}, u32[]{:S(2)}) collective-permute-start(bf16[16,104,128]{2,1,0:T(8,128)(2,1)S(1)} %shard_map.140), channel_id=1, source_target_pairs={{0,1},{1,0},{2,3},{3,2},{4,5},{5,4},{6,7},{7,6},{8,9},{9,8},{10,11... | collective-permute-start | bytes 1277960 | tf_op jit(solution)/shard_map/ppermute | solution.py:326
  70.2 21.8 %copy-start = (f32[2,8,2,4096]{3,2,1,0:T(2,128)S(1)}, f32[2,8,2,4096]{3,2,1,0:T(2,128)}, u32[]{:S(2)}) copy-start(f32[2,8,2,4096]{3,2,1,0:T(2,128)} %param.25) | copy-start | bytes 1572868
  70.2 21.8 %all-to-all-start.1 = ((bf16[16,104,128]{2,1,0:T(8,128)(2,1)}), bf16[16,104,128]{2,1,0:T(8,128)(2,1)S(1)}, u32[]{:S(2)}, u32[]{:S(2)}) async-start(bf16[16,104,128]{2,1,0:T(8,128)(2,1)} %shard_map.141), calls=%async_computation.1 | async-start | bytes 851968 | tf_op jit(solution)/shard_map/all_to_all | solution.py:322
  77.9 4.9 %copy-start.8 = (bf16[32,256]{1,0:T(8,128)(2,1)S(1)}, bf16[32,256]{1,0:T(8,128)(2,1)}, u32[]{:S(2)}) copy-start(bf16[32,256]{1,0:T(8,128)(2,1)} %tokens_ref.1) | copy-start | bytes 49156
  78.0 27.5 %collective-permute-start.3 = (bf16[6,256,128]{2,1,0:T(8,128)(2,1)S(1)}, bf16[6,256,128]{2,1,0:T(8,128)(2,1)S(1)}, u32[]{:S(2)}, u32[]{:S(2)}) collective-permute-start(bf16[6,256,128]{2,1,0:T(8,128)(2,1)S(1)} %slice_dynamic-update-slice_fusion), channel_id=1, source_target_pairs={{0,16},{16,0},{32,48},{48,32},{64,80},{80,64},{96,112},{112,96},{1... | collective-permute-start | bytes 1179656 | tf_op jit(solution)/shard_map/ppermute | solution.py:326
  82.9 9.0 %copy-start.11 = (f32[2,128]{1,0:T(2,128)S(1)}, f32[2,128]{1,0:T(2,128)}, u32[]{:S(2)}) copy-start(f32[2,128]{1,0:T(2,128)} %gain_ref.9) | copy-start | bytes 3076
  82.9 9.0 %copy-start.10 = (f32[2,128]{1,0:T(2,128)S(1)}, f32[2,128]{1,0:T(2,128)}, u32[]{:S(2)}) copy-start(f32[2,128]{1,0:T(2,128)} %base_ref.3) | copy-start | bytes 3076
  82.9 9.0 %copy-start.12 = (s32[8]{0:T(128)S(1)}, s32[8]{0:T(128)}, u32[]{:S(2)}) copy-start(s32[8]{0:T(128)} %lengths_ref.3) | copy-start | bytes 100
  94.7 15.2 %all-to-all-start.2 = ((bf16[32,8,128]{2,1,0:T(8,128)(2,1)}), bf16[32,8,128]{2,1,0:T(8,128)(2,1)S(1)}, u32[]{:S(2)}, u32[]{:S(2)}) async-start(bf16[32,8,128]{2,1,0:T(8,128)(2,1)} %bitcast.5), calls=%async_computation.2 | async-start | bytes 131072 | tf_op jit(solution)/shard_map/all_to_all | solution.py:322
  102.1 3.3 %collective-permute-start.2 = (bf16[288,256]{1,0:T(8,128)(2,1)S(1)}, bf16[288,256]{1,0:T(8,128)(2,1)S(1)}, u32[]{:S(2)}, u32[]{:S(2)}) collective-permute-start(bf16[288,256]{1,0:T(8,128)(2,1)S(1)} %concatenate.3), channel_id=1, source_target_pairs={{0,1},{1,0},{2,3},{3,2},{4,5},{5,4},{6,7},{7,6},{8,9},{9,8},{10,11... | collective-permute-start | bytes 442376 | tf_op jit(solution)/shard_map/ppermute | solution.py:326
  111.3 18.9 %all-to-all-start.3 = ((bf16[16,8,512]{2,1,0:T(8,128)(2,1)}), bf16[16,8,512]{2,1,0:T(8,128)(2,1)S(1)}, u32[]{:S(2)}, u32[]{:S(2)}) async-start(bf16[16,8,512]{2,1,0:T(8,128)(2,1)} %shard_map.143), calls=%async_computation.3 | async-start | bytes 262144 | tf_op jit(solution)/shard_map/all_to_all | solution.py:322
  116.0 4.4 %collective-permute-start.4 = (bf16[6,256,128]{2,1,0:T(8,128)(2,1)S(1)}, bf16[6,256,128]{2,1,0:T(8,128)(2,1)S(1)}, u32[]{:S(2)}, u32[]{:S(2)}) collective-permute-start(bf16[6,256,128]{2,1,0:T(8,128)(2,1)S(1)} %slice_dynamic-update-slice_fusion), channel_id=1, source_target_pairs={{0,1},{1,0},{2,3},{3,2},{4,5},{5,4},{6,7},{7,6},{8,9},{9,8},{10,11... | collective-permute-start | bytes 1179656 | tf_op jit(solution)/shard_map/ppermute | solution.py:326
  117.9 3.8 %collective-permute-start.5 = (bf16[6,256,128]{2,1,0:T(8,128)(2,1)S(1)}, bf16[6,256,128]{2,1,0:T(8,128)(2,1)S(1)}, u32[]{:S(2)}, u32[]{:S(2)}) collective-permute-start(bf16[6,256,128]{2,1,0:T(8,128)(2,1)S(1)} %collective-permute-done.3.refs_1_.refs_6_), channel_id=1, source_target_pairs={{0,1},{1,0},{2,3},{3,2},{4,5},{5,4},{6,7},{7,6},{8,9},{9,8},{10,11... | collective-permute-start | bytes 1179656 | tf_op jit(solution)/shard_map/ppermute | solution.py:326
  186.6 18.3 %all-to-all-start.7 = ((bf16[16,16,256]{2,1,0:T(8,128)(2,1)}), bf16[16,16,256]{2,1,0:T(8,128)(2,1)S(1)}, u32[]{:S(2)}, u32[]{:S(2)}) async-start(bf16[16,16,256]{2,1,0:T(8,128)(2,1)} %shard_map.147), calls=%async_computation.7 | async-start | bytes 262144 | tf_op jit(solution)/shard_map/all_to_all | solution.py:322
  190.6 3.1 %collective-permute-start.6 = (bf16[2,8,256]{2,1,0:T(8,128)(2,1)S(1)}, bf16[2,8,256]{2,1,0:T(8,128)(2,1)S(1)}, u32[]{:S(2)}, u32[]{:S(2)}) collective-permute-start(bf16[2,8,256]{2,1,0:T(8,128)(2,1)S(1)} %slice.47), channel_id=1, source_target_pairs={{0,1},{1,0},{2,3},{3,2},{4,5},{5,4},{6,7},{7,6},{8,9},{9,8},{10,11... | collective-permute-start | bytes 24584 | tf_op jit(solution)/shard_map/ppermute | solution.py:326

commit v5 on v4

--- a/solution.py
+++ b/solution.py
@@ -17,7 +17,10 @@
 group_epsilon = 0.00064
 
 VMEM = pl.BlockSpec(memory_space=pltpu.VMEM)
-SMEM = pl.BlockSpec(memory_space=pltpu.SMEM)
+
+
+def place():
+    return lax.rem(lax.axis_index("dp"), 2), lax.rem(lax.axis_index("tp"), 2)
 
 
 def iota(shape, dim):
@@ -38,11 +41,11 @@
     return jnp.where(pick == 0, high, jnp.where(pick == 1, row - high, 0.0)).astype(jnp.bfloat16)
 
 
-def project_kernel(far, place_ref, x_ref, gain_ref, *refs):
+def project_kernel(far, x_ref, gain_ref, *refs):
     out_ref = refs[-1]
     blocks, rows, depth = x_ref.shape
     half = rows // 2
-    first_half = place_ref[0] == (1 if far else 0)
+    first_half = place()[0] == (1 if far else 0)
     x = x_ref[...].astype(jnp.float32)
     x = jnp.where(first_half, x[:, :half], x[:, half:]).reshape(blocks * half, depth)
     scaled = (x * gain_ref[0:1, :]).astype(jnp.bfloat16)
@@ -67,9 +70,9 @@
         out_ref[block, pl.ds(6 * half, 8), :] = squares_tail(row)
 
 
-def project_pair_kernel(place_ref, x_ref, gain_ref, packed_ref, *refs):
+def project_pair_kernel(x_ref, gain_ref, packed_ref, *refs):
     *weight_refs, other_ref, core_own_ref, core_other_ref, out_ref = refs
-    column = place_ref[1]
+    column = place()[1]
     blocks, rows, both = x_ref.shape
     depth = both // 2
     x = x_ref[...].astype(jnp.float32).reshape(blocks * rows, both)
@@ -103,7 +106,7 @@
             out_ref[member, block, pl.ds(6 * rows, 8), :] = squares_tail(row)
 
 
-def advance_kernel(layer, rows, width, arrived_ref, lengths_ref, base_ref, gain_ref, state_ref, *refs):
+def advance_kernel(layer, rows, width, arrived_ref, limits_ref, base_ref, gain_ref, state_ref, *refs):
     mixed_ref, new_ref, line_ref, read_ref = refs[-4:]
     seqs = rows // NEW
     parts, part_rows = arrived_ref.shape[0], (arrived_ref.shape[1] - 8) // 6
@@ -132,11 +135,7 @@
     decays = jnp.exp(jax.nn.sigmoid(log_rate) * (-0.6065306597126334))
     rates = jax.nn.sigmoid(rate_pre)
     unit = keys * lax.rsqrt(split_dot(keys * keys, same_head) + unit_epsilon)
-    slot = iota((rows, LANES), 0)
-    limit = jnp.zeros((rows, LANES), jnp.int32)
-    for seq in range(seqs):
-        limit = jnp.where(slot // NEW == seq, lengths_ref[seq], limit)
-    live = slot % NEW < limit
+    live = iota((rows, LANES), 0) % NEW < limits_ref[...]
     decays = jnp.where(live, decays, 1.0)
     unit = jnp.where(live, unit, 0.0)
     keys = jnp.where(live, keys, 0.0)
@@ -162,7 +161,7 @@
         )[None]
 
     state = [
-        state_ref[pl.ds(seq * HEAD, HEAD), :].reshape(8, 8, LANES) for seq in range(seqs)
+        state_ref[layer, pl.ds(seq * HEAD, HEAD), :].reshape(8, 8, LANES) for seq in range(seqs)
     ]
     for position in range(NEW):
         tokens = [seq * NEW + position for seq in range(seqs)]
@@ -195,7 +194,7 @@
                 jnp.where(place_mask, read[part], 0.0), 0, keepdims=True
             )
     for seq in range(seqs):
-        new_ref[0, pl.ds(seq * HEAD, HEAD), :] = state[seq].reshape(HEAD, LANES)
+        new_ref[pl.ds(seq * HEAD, HEAD), :] = state[seq].reshape(HEAD, LANES)
     read = read_ref[...]
     centred = read - split_dot(read, same_head) / HEAD
     variance = split_dot(centred * centred, same_head) / HEAD
@@ -208,11 +207,11 @@
             mixed_ref[member, owner] = mixed[start : start + share].astype(jnp.bfloat16)
 
 
-def out_kernel(layer, place_ref, mixed_ref, own_ref, other_ref, *refs):
+def out_kernel(layer, mixed_ref, own_ref, other_ref, *refs):
     out_ref = refs[-1]
     _, blocks, rows, _ = mixed_ref.shape
     depth = own_ref.shape[2]
-    first = place_ref[1] == 0
+    first = place()[1] == 0
     sides = [(own_ref[layer], other_ref[layer])]
     if layer == 0:
         sides.append((refs[0][pl.ds(0, LANES), :], refs[0][pl.ds(LANES, LANES), :]))
@@ -230,10 +229,10 @@
         )
 
 
-def settle_kernel(place_ref, summed_ref, tokens_ref, packed_ref, *refs):
+def settle_kernel(summed_ref, tokens_ref, packed_ref, *refs):
     rows_ref, spread_ref = refs[-2:]
     columns, rows, _ = summed_ref.shape
-    first = place_ref[0] == 0
+    first = place()[0] == 0
     for member in range(2):
         total = summed_ref[member].astype(jnp.float32)
         for column in range(member + 2, columns, 2):
@@ -248,9 +247,9 @@
             spread_ref[column] = total
 
 
-def finish_kernel(place_ref, summed_ref, rows_ref, back_ref, out_ref):
+def finish_kernel(summed_ref, rows_ref, back_ref, out_ref):
     columns, half, depth = summed_ref.shape
-    first = place_ref[0] == 0
+    first = place()[0] == 0
     for member in range(2):
         total = summed_ref[member].astype(jnp.float32)
         for column in range(member + 2, columns, 2):
@@ -274,8 +273,7 @@
     return pl.pallas_call(
         kernel,
         out_shape=outs,
-        in_specs=[SMEM]
-        + [VMEM] * (len(operands) - 1)
+        in_specs=[VMEM] * len(operands)
         + [pl.BlockSpec(memory_space=pl.ANY)] * len(awaited),
         out_specs=jax.tree.map(lambda _: VMEM, outs),
         **params(),
@@ -286,36 +284,19 @@
     return jax.ShapeDtypeStruct(shape, jnp.bfloat16)
 
 
-def advance(layer, width, shared, arrived, lengths, base, gain, states, held, awaited):
-    rows = lengths.shape[0] * NEW
-    state_rows = states.shape[1]
-    block = pl.BlockSpec((1, state_rows, LANES), lambda i: (layer, 0, 0))
-    in_block = pl.BlockSpec((None, state_rows, LANES), lambda i: (layer, 0, 0))
-    operands = [arrived, lengths, base, gain, states]
-    in_specs = [VMEM, SMEM, VMEM, VMEM, in_block]
-    aliases = {}
-    if held is not None:
-        aliases = {len(operands): 1}
-        operands.append(held)
-        in_specs.append(pl.BlockSpec(memory_space=pl.ANY))
-    operands.extend(awaited)
-    in_specs.extend([pl.BlockSpec(memory_space=pl.ANY)] * len(awaited))
+def advance(layer, width, shared, arrived, limits, base, gain, states, awaited):
+    rows = limits.shape[0]
     return pl.pallas_call(
         functools.partial(advance_kernel, layer, rows, width),
-        grid=(1,),
-        out_shape=(
-            jax.ShapeDtypeStruct(shared, jnp.bfloat16),
-            jax.ShapeDtypeStruct(states.shape, jnp.float32),
-        ),
-        in_specs=in_specs,
-        out_specs=(pl.BlockSpec(shared, lambda i: (0, 0, 0, 0)), block),
+        out_shape=(bf16(*shared), jax.ShapeDtypeStruct(states.shape[1:], jnp.float32)),
+        in_specs=[VMEM] * 5 + [pl.BlockSpec(memory_space=pl.ANY)] * len(awaited),
+        out_specs=(VMEM, VMEM),
         scratch_shapes=[
             pltpu.VMEM((11, rows, LANES), jnp.float32),
             pltpu.VMEM((rows, LANES), jnp.float32),
         ],
-        input_output_aliases=aliases,
         **params(),
-    )(*operands)
+    )(arrived, limits, base, gain, states, *awaited)
 
 
 def exchange(x, axis, groups=None):
@@ -348,14 +329,14 @@
     folded = states.reshape(blocks, seqs, heads, HEAD // 2, LANES)
     folded = jnp.swapaxes(folded, 2, 3).reshape(blocks, seqs * HEAD, LANES)
     columns, owners = lax.axis_size("tp"), lax.axis_size("dp")
-    place = jnp.stack([lax.axis_index("dp") % 2, lax.axis_index("tp") % 2])
     both = ("tp", "dp")
     pairs = [
         [column * owners + owner for column in (first, first + 1) for owner in range(owners)]
         for first in range(0, columns, 2)
     ]
     half, quarter = own_count // 2, own_count // 4
-    core = place[0]
+    core = place()[0]
+    limits = jnp.broadcast_to(jnp.repeat(lengths, NEW)[:, None], (own_count, LANES))
     gathered = exchange(jnp.broadcast_to(tokens, (columns, own_count, depth)), "tp")
     other_out = from_partner(w_out, "tp")
     own_weights = jnp.stack([weight[1] for weight in weights])
@@ -384,53 +365,54 @@
     far = call(
         functools.partial(project_kernel, True),
         bf16(columns, 3 * own_count + 8, LANES),
-        place, gathered, norm_gain, *weights,
+        gathered, norm_gain, *weights,
     )
     came = from_partner(far, "dp")
     near = call(
         functools.partial(project_kernel, False),
         bf16(columns, 3 * own_count + 8, LANES),
-        place, gathered, norm_gain, *weights, came,
+        gathered, norm_gain, *weights, came,
     )
     arrived = exchange(near, "dp")
-    shared, held = advance(
-        0, width, (2, owners, quarter, LANES), arrived, lengths, decay_base, group_gain,
-        folded, None, [other_out],
+    shared, first_states = advance(
+        0, width, (2, owners, quarter, LANES), arrived, limits, decay_base, group_gain,
+        folded, [other_out],
     )
     shared = exchange(shared.reshape(2 * owners, quarter, LANES), both, pairs)
     product = call(
         functools.partial(out_kernel, 0),
         bf16(columns, quarter, 2 * depth),
-        place, shared.reshape(2, owners, quarter, LANES), w_out, other_out, packed,
+        shared.reshape(2, owners, quarter, LANES), w_out, other_out, packed,
         awaited=[other_weights],
     )
     summed = exchange(product, "tp")
     rows, spread = call(
         settle_kernel,
         (bf16(2, quarter, 2 * depth), bf16(columns, quarter, 2 * depth)),
-        place, summed, tokens, packed,
+        summed, tokens, packed,
         awaited=[core_own, core_other],
     )
     gathered = exchange(spread, "tp")
     near = call(
         project_pair_kernel,
         bf16(2, columns, 6 * quarter + 8, LANES),
-        place, gathered, norm_gain, packed, *weights, other_weights, core_own, core_other,
+        gathered, norm_gain, packed, *weights, other_weights, core_own, core_other,
     )
     arrived = exchange(near.reshape(-1, *near.shape[2:]), both, pairs)
     back = from_partner(rows[:, :, depth:], "dp")
-    shared, held = advance(
-        1, width, (2, owners, half, LANES), arrived, lengths, decay_base, group_gain,
-        folded, held, [],
+    shared, last_states = advance(
+        1, width, (2, owners, half, LANES), arrived, limits, decay_base, group_gain,
+        folded, [],
     )
     shared = exchange(shared.reshape(2 * owners, half, LANES), both, pairs)
     product = call(
         functools.partial(out_kernel, 1),
         bf16(columns, half, depth),
-        place, shared.reshape(2, owners, half, LANES), w_out, other_out,
+        shared.reshape(2, owners, half, LANES), w_out, other_out,
     )
     summed = exchange(product, "tp")
-    own_rows = call(finish_kernel, bf16(own_count, depth), place, summed, rows, back)
+    own_rows = call(finish_kernel, bf16(own_count, depth), summed, rows, back)
+    held = jnp.stack([first_states, last_states])
     new_states = jnp.swapaxes(held.reshape(blocks, seqs, HEAD // 2, heads, LANES), 2, 3)
     return (own_rows, new_states.reshape(states.shape))
 

time: 207 us -> 203 us (0.981)
  Pallas kernels: 13 us -> 7.87 us
  waiting for transfers between devices: 52 us -> 47.4 us
  local copies, waits for them, and re-layouts: 2.61 us -> 6.95 us
    pallas_call x9, Pallas kernels: 13 us -> 7.87 us  [the longest x7 4.09 us: call(): pl.pallas_call(kernel, out_shape=outs, in_specs=[VMEM] * len(operands) +...]
    unnamed x31, local copies, waits for them, and re-layouts: 0.98 us -> 4.48 us
    all_to_all x5, waiting for transfers between devices: 46.5 us -> 44.2 us  [exchange(): return lax.all_to_all(x, axis, 0, 0, tiled=True, axis_index_groups=groups)]
    ppermute x7, waiting for transfers between devices: 5.5 us -> 3.26 us  [from_partner(): lax.ppermute(x, axis, [(i, i ^ 1) for i in range(lax.axis_size(axis))])]
  transfers between devices with their start and end apart: 12 -> 12, of which waited for: 9 -> 9; matrix products, arithmetic and copies ran while one was open for 0% -> 3% of each run, Pallas kernels for 2% -> 2%
where the time goes in v5:
time: 203 us; the launch traced here: 202 us
  starting transfers between devices  86.4 us (43%)
  blocking collectives  51.1 us (25%)
  waiting for transfers between devices  47.4 us (23%)
  Pallas kernels  7.87 us (4%)
  local copies, waits for them, and re-layouts  6.95 us (3%)
    all_to_all x5, starting transfers between devices, exchange(): return lax.all_to_all(x, axis, 0, 0, tiled=True, axis_index_groups=groups)  67.4 us
    all_to_all x3, blocking collectives, exchange(): return lax.all_to_all(x, axis, 0, 0, tiled=True, axis_index_groups=groups)  51.1 us
    all_to_all x5, waiting for transfers between devices, exchange(): return lax.all_to_all(x, axis, 0, 0, tiled=True, axis_index_groups=groups)  44.2 us
    ppermute x7, starting transfers between devices, from_partner(): lax.ppermute(x, axis, [(i, i ^ 1) for i in range(lax.axis_size(axis))])  19 us
    unnamed x31, local copies, waits for them, and re-layouts  4.48 us
    pallas_call x7, Pallas kernels, call(): pl.pallas_call(kernel, out_shape=outs, in_specs=[VMEM] * len(operands) +...  4.09 us
  transfers between devices with their start and end apart: 12, of which 9 were waited for; matrix products, arithmetic and copies ran while one was open for 3% of the time, Pallas kernels for 2%

profile of v5, /device:TPU:80, one launch (start us, length us, event | category | flops | bytes accessed | tf_op | source)
XLA Modules:
  0.0 201.8 jit_solution(4942816933293662228)
XLA Ops:
  0.6 1.5 broadcast_in_dim.16
  2.1 43.8 %all-to-all-start = ((bf16[16,32,256]{2,1,0:T(8,128)(2,1)}), bf16[16,32,256]{2,1,0:T(8,128)(2,1)S(1)}, u32[]{:S(2)}, u32[]{:S(2)}) async-start(bf16[16,32,256]{2,1,0:T(8,128)(2,1)} %broadcast_in_dim.16), calls=%async_computation | async-start | bytes 524288 | tf_op jit(solution)/shard_map/all_to_all | solution.py:303
  46.0 3.8 %collective-permute-start.1 = (bf16[2,128,256]{2,1,0:T(8,128)(2,1)S(1)}, bf16[2,128,256]{2,1,0:T(8,128)(2,1)S(1)}, u32[]{:S(2)}, u32[]{:S(2)}) collective-permute-start(bf16[2,128,256]{2,1,0:T(8,128)(2,1)S(1)} %copy-done.7), channel_id=1, source_target_pairs={{0,16},{16,0},{32,48},{48,32},{64,80},{80,64},{96,112},{112,96},{1... | collective-permute-start | bytes 393224 | tf_op jit(solution)/shard_map/ppermute | solution.py:307
  49.8 0.6 slice_dynamic-update-slice_fusion.5
  50.4 0.6 slice_dynamic-update-slice_fusion.4
  51.0 0.6 slice_dynamic-update-slice_fusion.3
  51.7 12.4 %all-to-all-done.x_ref = bf16[16,32,256]{2,1,0:T(8,128)(2,1)S(1)} async-done(((bf16[16,32,256]{2,1,0:T(8,128)(2,1)}), bf16[16,32,256]{2,1,0:T(8,128)(2,1)S(1)}, u32[]{:S(2)}, u32[]{:S(2)}) %all-to-all-start) | async-done | bytes 262176 | tf_op jit(solution)/shard_map/all_to_all | solution.py:303
  64.1 0.3 shard_map.140
  64.4 2.0 collective-permute-start
  66.3 0.6 slice_dynamic-update-slice_fusion.2
  66.9 0.6 slice_dynamic-update-slice_fusion.1
  67.6 0.5 collective-permute-done.refs_6_
  68.1 1.0 shard_map.141
  69.1 7.8 %all-to-all-start.1 = ((bf16[16,104,128]{2,1,0:T(8,128)(2,1)}), bf16[16,104,128]{2,1,0:T(8,128)(2,1)S(1)}, u32[]{:S(2)}, u32[]{:S(2)}) async-start(bf16[16,104,128]{2,1,0:T(8,128)(2,1)} %shard_map.141), calls=%async_computation.1 | async-start | bytes 851968 | tf_op jit(solution)/shard_map/all_to_all | solution.py:303
  76.9 0.6 slice_dynamic-update-slice_fusion
  77.5 5.0 %collective-permute-start.3 = (bf16[6,256,128]{2,1,0:T(8,128)(2,1)}, bf16[6,256,128]{2,1,0:T(8,128)(2,1)S(1)}, u32[]{:S(2)}, u32[]{:S(2)}) collective-permute-start(bf16[6,256,128]{2,1,0:T(8,128)(2,1)} %slice_dynamic-update-slice_fusion), channel_id=1, source_target_pairs={{0,16},{16,0},{32,48},{48,32},{64,80},{80,64},{96,112},{112,96},{1... | collective-permute-start | bytes 1179656 | tf_op jit(solution)/shard_map/ppermute | solution.py:307
  82.5 0.0 copy-start.11
  82.6 0.0 copy-start.12
  82.6 0.6 copy-done.12
  83.2 0.1 broadcast_in_dim.17
  83.3 0.1 broadcast_in_dim.18
  83.4 7.5 %all-to-all-done.1.arrived_ref = bf16[16,104,128]{2,1,0:T(8,128)(2,1)S(1)} async-done(((bf16[16,104,128]{2,1,0:T(8,128)(2,1)}), bf16[16,104,128]{2,1,0:T(8,128)(2,1)S(1)}, u32[]{:S(2)}, u32[]{:S(2)}) %all-to-all-start.1) | async-done | bytes 426016 | tf_op jit(solution)/shard_map/all_to_all | solution.py:303
  90.9 0.1 broadcast_in_dim.19.limits_ref
  90.9 0.7 copy-done.10
  91.6 2.2 %shard_map.142 = (bf16[2,16,8,128]{3,2,1,0:T(8,128)(2,1)}, f32[512,128]{1,0:T(8,128)S(1)}) custom-call(bf16[16,104,128]{2,1,0:T(8,128)(2,1)S(1)} %all-to-all-done.1.arrived_ref, s32[32,128]{1,0:T(8,128)S(1)} %broadcast_in_dim.19.limits_ref, f32[2,128]{1,0:T(2,128)S(1)} %copy-done.10, f32[2,128]{1,0:T(2,128)S(1)} %copy-done.11, f32[2,512,128]{2,1,0:T(8,128)S(1)} %bitcast.33, ...), custom_call_target="tpu_custom_call" | custom-call | flops 100000000 | bytes 2000000 | tf_op jit(solution)/shard_map/pallas_call | solution.py:289
  93.8 7.2 %all-to-all-start.2 = ((bf16[32,8,128]{2,1,0:T(8,128)(2,1)}), bf16[32,8,128]{2,1,0:T(8,128)(2,1)S(1)}, u32[]{:S(2)}, u32[]{:S(2)}) async-start(bf16[32,8,128]{2,1,0:T(8,128)(2,1)} %bitcast.3), calls=%async_computation.2 | async-start | bytes 131072 | tf_op jit(solution)/shard_map/all_to_all | solution.py:303
  101.1 0.2 concatenate.4
  101.3 2.0 collective-permute-start.2
  103.2 1.3 collective-permute-done.2.refs_0_.packed_ref
  104.6 4.5 %all-to-all-done.2 = bf16[32,8,128]{2,1,0:T(8,128)(2,1)S(1)} async-done(((bf16[32,8,128]{2,1,0:T(8,128)(2,1)}), bf16[32,8,128]{2,1,0:T(8,128)(2,1)S(1)}, u32[]{:S(2)}, u32[]{:S(2)}) %all-to-all-start.2) | async-done | bytes 65568 | tf_op jit(solution)/shard_map/all_to_all | solution.py:303
  109.1 0.9 shard_map.143
  110.0 4.6 %all-to-all-start.3 = ((bf16[16,8,512]{2,1,0:T(8,128)(2,1)}), bf16[16,8,512]{2,1,0:T(8,128)(2,1)S(1)}, u32[]{:S(2)}, u32[]{:S(2)}) async-start(bf16[16,8,512]{2,1,0:T(8,128)(2,1)} %shard_map.143), calls=%async_computation.3 | async-start | bytes 262144 | tf_op jit(solution)/shard_map/all_to_all | solution.py:303
  114.6 2.0 collective-permute-start.4
  116.5 2.4 %collective-permute-start.5 = (bf16[6,256,128]{2,1,0:T(8,128)(2,1)S(1)}, bf16[6,256,128]{2,1,0:T(8,128)(2,1)S(1)}, u32[]{:S(2)}, u32[]{:S(2)}) collective-permute-start(bf16[6,256,128]{2,1,0:T(8,128)(2,1)S(1)} %collective-permute-done.3.refs_1_.refs_6_), channel_id=1, source_target_pairs={{0,1},{1,0},{2,3},{3,2},{4,5},{5,4},{6,7},{7,6},{8,9},{9,8},{10,11... | collective-permute-start | bytes 1179656 | tf_op jit(solution)/shard_map/ppermute | solution.py:307
  119.0 1.3 collective-permute-done.5.refs_1_.refs_8_
  120.3 8.5 %all-to-all-done.3.summed_ref = bf16[16,8,512]{2,1,0:T(8,128)(2,1)S(1)} async-done(((bf16[16,8,512]{2,1,0:T(8,128)(2,1)}), bf16[16,8,512]{2,1,0:T(8,128)(2,1)S(1)}, u32[]{:S(2)}, u32[]{:S(2)}) %all-to-all-start.3) | async-done | bytes 131104 | tf_op jit(solution)/shard_map/all_to_all | solution.py:303
  128.8 18.4 %all_to_all.40.x_ref = bf16[16,8,512]{2,1,0:T(8,128)(2,1)S(1)} all-to-all(bf16[16,8,512]{2,1,0:T(8,128)(2,1)S(1)} %get-tuple-element.9), channel_id=1, replica_groups=mesh['grp'=2,'tp'=16,'dp'=16] {'tp'}, dimensions={0} | all-to-all | bytes 262144 | tf_op jit(solution)/shard_map/all_to_all | solution.py:303
  147.3 0.4 shard_map.145
  147.7 18.6 %all_to_all.41.arrived_ref = bf16[32,56,128]{2,1,0:T(8,128)(2,1)S(1)} all-to-all(bf16[32,56,128]{2,1,0:T(8,128)(2,1)S(1)} %bitcast.35), channel_id=1, replica_groups={{0,1,2,3,4,5,6,7,8,9,10,11,12,13,14,15,16,17,18,19,20,21,22,23,24,25,26..., dimensions={0} | all-to-all | bytes 917504 | tf_op jit(solution)/shard_map/all_to_all | solution.py:303
  166.2 1.6 shard_map.146
  167.8 14.1 %all_to_all.42 = bf16[32,16,128]{2,1,0:T(8,128)(2,1)S(1)} all-to-all(bf16[32,16,128]{2,1,0:T(8,128)(2,1)S(1)} %bitcast.41), channel_id=1, replica_groups={{0,1,2,3,4,5,6,7,8,9,10,11,12,13,14,15,16,17,18,19,20,21,22,23,24,25,26..., dimensions={0} | all-to-all | bytes 262144 | tf_op jit(solution)/shard_map/all_to_all | solution.py:303
  181.9 0.9 shard_map.147
  182.8 4.0 %all-to-all-start.7 = ((bf16[16,16,256]{2,1,0:T(8,128)(2,1)}), bf16[16,16,256]{2,1,0:T(8,128)(2,1)S(1)}, u32[]{:S(2)}, u32[]{:S(2)}) async-start(bf16[16,16,256]{2,1,0:T(8,128)(2,1)} %shard_map.147), calls=%async_computation.7 | async-start | bytes 262144 | tf_op jit(solution)/shard_map/all_to_all | solution.py:303
  186.7 2.0 collective-permute-start.6
  188.7 1.0 maximum_bitcast_fusion
  189.7 0.1 collective-permute-done.6.back_ref
  189.8 11.3 %all-to-all-done.7.summed_ref = bf16[16,16,256]{2,1,0:T(8,128)(2,1)S(1)} async-done(((bf16[16,16,256]{2,1,0:T(8,128)(2,1)}), bf16[16,16,256]{2,1,0:T(8,128)(2,1)S(1)}, u32[]{:S(2)}, u32[]{:S(2)}) %all-to-all-start.7) | async-done | bytes 131104 | tf_op jit(solution)/shard_map/all_to_all | solution.py:303
  201.1 0.6 shard_map.148
  (32 shorter events, 0.1 us)
Async XLA Ops:
  0.6 63.4 %copy-start.9 = (f32[2,256]{1,0:T(2,128)S(1)}, f32[2,256]{1,0:T(2,128)}, u32[]{:S(2)}) copy-start(f32[2,256]{1,0:T(2,128)} %gain_ref.8) | copy-start | bytes 6148
  2.1 43.8 %copy-start.7 = (bf16[2,128,256]{2,1,0:T(8,128)(2,1)S(1)}, bf16[2,128,256]{2,1,0:T(8,128)(2,1)}, u32[]{:S(2)}) copy-start(bf16[2,128,256]{2,1,0:T(8,128)(2,1)} %own_ref.3) | copy-start | bytes 393220
  2.1 47.7 %copy-start.1 = (bf16[2,256,128]{2,1,0:T(8,128)(2,1)S(1)}, bf16[2,256,128]{2,1,0:T(8,128)(2,1)}, u32[]{:S(2)}) copy-start(bf16[2,256,128]{2,1,0:T(8,128)(2,1)} %refs_0_.5) | copy-start | bytes 393220
  2.1 62.0 %copy-start.5 = (bf16[2,256,128]{2,1,0:T(8,128)(2,1)S(1)}, bf16[2,256,128]{2,1,0:T(8,128)(2,1)}, u32[]{:S(2)}) copy-start(bf16[2,256,128]{2,1,0:T(8,128)(2,1)} %refs_4_.5) | copy-start | bytes 393220
  2.1 62.0 %copy-start.6 = (bf16[2,256,128]{2,1,0:T(8,128)(2,1)S(1)}, bf16[2,256,128]{2,1,0:T(8,128)(2,1)}, u32[]{:S(2)}) copy-start(bf16[2,256,128]{2,1,0:T(8,128)(2,1)} %refs_5_.5) | copy-start | bytes 393220
  2.1 62.0 %all-to-all-start = ((bf16[16,32,256]{2,1,0:T(8,128)(2,1)}), bf16[16,32,256]{2,1,0:T(8,128)(2,1)S(1)}, u32[]{:S(2)}, u32[]{:S(2)}) async-start(bf16[16,32,256]{2,1,0:T(8,128)(2,1)} %broadcast_in_dim.16), calls=%async_computation | async-start | bytes 524288 | tf_op jit(solution)/shard_map/all_to_all | solution.py:303
  45.9 4.5 %copy-start.2 = (bf16[2,256,128]{2,1,0:T(8,128)(2,1)S(1)}, bf16[2,256,128]{2,1,0:T(8,128)(2,1)}, u32[]{:S(2)}) copy-start(bf16[2,256,128]{2,1,0:T(8,128)(2,1)} %refs_1_.5) | copy-start | bytes 393220
  46.0 5.1 %copy-start.3 = (bf16[2,256,128]{2,1,0:T(8,128)(2,1)S(1)}, bf16[2,256,128]{2,1,0:T(8,128)(2,1)}, u32[]{:S(2)}) copy-start(bf16[2,256,128]{2,1,0:T(8,128)(2,1)} %refs_2_.5) | copy-start | bytes 393220
  46.0 37.4 %collective-permute-start.1 = (bf16[2,128,256]{2,1,0:T(8,128)(2,1)S(1)}, bf16[2,128,256]{2,1,0:T(8,128)(2,1)S(1)}, u32[]{:S(2)}, u32[]{:S(2)}) collective-permute-start(bf16[2,128,256]{2,1,0:T(8,128)(2,1)S(1)} %copy-done.7), channel_id=1, source_target_pairs={{0,16},{16,0},{32,48},{48,32},{64,80},{80,64},{96,112},{112,96},{1... | collective-permute-start | bytes 393224 | tf_op jit(solution)/shard_map/ppermute | solution.py:307
  50.4 13.7 %copy-start.4 = (bf16[2,256,128]{2,1,0:T(8,128)(2,1)S(1)}, bf16[2,256,128]{2,1,0:T(8,128)(2,1)}, u32[]{:S(2)}) copy-start(bf16[2,256,128]{2,1,0:T(8,128)(2,1)} %refs_3_.5) | copy-start | bytes 393220
  64.4 3.7 %collective-permute-start = (bf16[16,104,128]{2,1,0:T(8,128)(2,1)S(1)}, bf16[16,104,128]{2,1,0:T(8,128)(2,1)S(1)}, u32[]{:S(2)}, u32[]{:S(2)}) collective-permute-start(bf16[16,104,128]{2,1,0:T(8,128)(2,1)S(1)} %shard_map.140), channel_id=1, source_target_pairs={{0,1},{1,0},{2,3},{3,2},{4,5},{5,4},{6,7},{7,6},{8,9},{9,8},{10,11... | collective-permute-start | bytes 1277960 | tf_op jit(solution)/shard_map/ppermute | solution.py:307
  69.1 21.8 %copy-start = (f32[2,8,2,4096]{3,2,1,0:T(2,128)S(1)}, f32[2,8,2,4096]{3,2,1,0:T(2,128)}, u32[]{:S(2)}) copy-start(f32[2,8,2,4096]{3,2,1,0:T(2,128)} %param.25) | copy-start | bytes 1572868
  69.1 21.8 %all-to-all-start.1 = ((bf16[16,104,128]{2,1,0:T(8,128)(2,1)}), bf16[16,104,128]{2,1,0:T(8,128)(2,1)S(1)}, u32[]{:S(2)}, u32[]{:S(2)}) async-start(bf16[16,104,128]{2,1,0:T(8,128)(2,1)} %shard_map.141), calls=%async_computation.1 | async-start | bytes 851968 | tf_op jit(solution)/shard_map/all_to_all | solution.py:303
  77.5 5.0 %copy-start.8 = (bf16[32,256]{1,0:T(8,128)(2,1)S(1)}, bf16[32,256]{1,0:T(8,128)(2,1)}, u32[]{:S(2)}) copy-start(bf16[32,256]{1,0:T(8,128)(2,1)} %tokens_ref.1) | copy-start | bytes 49156
  77.5 27.1 %collective-permute-start.3 = (bf16[6,256,128]{2,1,0:T(8,128)(2,1)}, bf16[6,256,128]{2,1,0:T(8,128)(2,1)S(1)}, u32[]{:S(2)}, u32[]{:S(2)}) collective-permute-start(bf16[6,256,128]{2,1,0:T(8,128)(2,1)} %slice_dynamic-update-slice_fusion), channel_id=1, source_target_pairs={{0,16},{16,0},{32,48},{48,32},{64,80},{80,64},{96,112},{112,96},{1... | collective-permute-start | bytes 1179656 | tf_op jit(solution)/shard_map/ppermute | solution.py:307
  82.5 8.4 %copy-start.11 = (f32[2,128]{1,0:T(2,128)S(1)}, f32[2,128]{1,0:T(2,128)}, u32[]{:S(2)}) copy-start(f32[2,128]{1,0:T(2,128)} %gain_ref.9) | copy-start | bytes 3076
  82.6 0.7 copy-start.12
  90.9 0.7 copy-start.10
  93.8 15.3 %all-to-all-start.2 = ((bf16[32,8,128]{2,1,0:T(8,128)(2,1)}), bf16[32,8,128]{2,1,0:T(8,128)(2,1)S(1)}, u32[]{:S(2)}, u32[]{:S(2)}) async-start(bf16[32,8,128]{2,1,0:T(8,128)(2,1)} %bitcast.3), calls=%async_computation.2 | async-start | bytes 131072 | tf_op jit(solution)/shard_map/all_to_all | solution.py:303
  101.3 3.3 %collective-permute-start.2 = (bf16[288,256]{1,0:T(8,128)(2,1)S(1)}, bf16[288,256]{1,0:T(8,128)(2,1)S(1)}, u32[]{:S(2)}, u32[]{:S(2)}) collective-permute-start(bf16[288,256]{1,0:T(8,128)(2,1)S(1)} %concatenate.4), channel_id=1, source_target_pairs={{0,1},{1,0},{2,3},{3,2},{4,5},{5,4},{6,7},{7,6},{8,9},{9,8},{10,11... | collective-permute-start | bytes 442376 | tf_op jit(solution)/shard_map/ppermute | solution.py:307
  110.0 18.8 %all-to-all-start.3 = ((bf16[16,8,512]{2,1,0:T(8,128)(2,1)}), bf16[16,8,512]{2,1,0:T(8,128)(2,1)S(1)}, u32[]{:S(2)}, u32[]{:S(2)}) async-start(bf16[16,8,512]{2,1,0:T(8,128)(2,1)} %shard_map.143), calls=%async_computation.3 | async-start | bytes 262144 | tf_op jit(solution)/shard_map/all_to_all | solution.py:303
  114.6 4.4 %collective-permute-start.4 = (bf16[6,256,128]{2,1,0:T(8,128)(2,1)}, bf16[6,256,128]{2,1,0:T(8,128)(2,1)S(1)}, u32[]{:S(2)}, u32[]{:S(2)}) collective-permute-start(bf16[6,256,128]{2,1,0:T(8,128)(2,1)} %slice_dynamic-update-slice_fusion), channel_id=1, source_target_pairs={{0,1},{1,0},{2,3},{3,2},{4,5},{5,4},{6,7},{7,6},{8,9},{9,8},{10,11... | collective-permute-start | bytes 1179656 | tf_op jit(solution)/shard_map/ppermute | solution.py:307
  116.5 3.8 %collective-permute-start.5 = (bf16[6,256,128]{2,1,0:T(8,128)(2,1)S(1)}, bf16[6,256,128]{2,1,0:T(8,128)(2,1)S(1)}, u32[]{:S(2)}, u32[]{:S(2)}) collective-permute-start(bf16[6,256,128]{2,1,0:T(8,128)(2,1)S(1)} %collective-permute-done.3.refs_1_.refs_6_), channel_id=1, source_target_pairs={{0,1},{1,0},{2,3},{3,2},{4,5},{5,4},{6,7},{7,6},{8,9},{9,8},{10,11... | collective-permute-start | bytes 1179656 | tf_op jit(solution)/shard_map/ppermute | solution.py:307
  182.8 18.4 %all-to-all-start.7 = ((bf16[16,16,256]{2,1,0:T(8,128)(2,1)}), bf16[16,16,256]{2,1,0:T(8,128)(2,1)S(1)}, u32[]{:S(2)}, u32[]{:S(2)}) async-start(bf16[16,16,256]{2,1,0:T(8,128)(2,1)} %shard_map.147), calls=%async_computation.7 | async-start | bytes 262144 | tf_op jit(solution)/shard_map/all_to_all | solution.py:303
  186.7 3.1 %collective-permute-start.6 = (bf16[2,8,256]{2,1,0:T(8,128)(2,1)S(1)}, bf16[2,8,256]{2,1,0:T(8,128)(2,1)S(1)}, u32[]{:S(2)}, u32[]{:S(2)}) collective-permute-start(bf16[2,8,256]{2,1,0:T(8,128)(2,1)S(1)} %slice.47), channel_id=1, source_target_pairs={{0,1},{1,0},{2,3},{3,2},{4,5},{5,4},{6,7},{7,6},{8,9},{9,8},{10,11... | collective-permute-start | bytes 24584 | tf_op jit(solution)/shard_map/ppermute | solution.py:307

commit v6 on v5

--- a/solution.py
+++ b/solution.py
@@ -135,7 +135,10 @@
     decays = jnp.exp(jax.nn.sigmoid(log_rate) * (-0.6065306597126334))
     rates = jax.nn.sigmoid(rate_pre)
     unit = keys * lax.rsqrt(split_dot(keys * keys, same_head) + unit_epsilon)
-    live = iota((rows, LANES), 0) % NEW < limits_ref[...]
+    seqs_row = limits_ref[...].astype(jnp.float32)
+    of_seq = iota((rows, seqs), 0) // NEW == iota((rows, seqs), 1)
+    limit = jnp.sum(jnp.where(of_seq, seqs_row, 0.0), 1, keepdims=True)
+    live = (iota((rows, LANES), 0) % NEW).astype(jnp.float32) < limit
     decays = jnp.where(live, decays, 1.0)
     unit = jnp.where(live, unit, 0.0)
     keys = jnp.where(live, keys, 0.0)
@@ -229,6 +232,43 @@
         )
 
 
+def out_quad_kernel(mixed_ref, pair_ref, far_ref, out_ref):
+    members, blocks, rows, _ = mixed_ref.shape
+    me = lax.rem(lax.axis_index("tp"), members)
+    total = 0.0
+    for member in range(members):
+        offset = jnp.bitwise_xor(me, member)
+        side = lax.rem(offset, 2)
+        matrix = jnp.where(offset < 2, pair_ref[side], far_ref[side])
+        lines = mixed_ref[member].astype(jnp.float32).reshape(blocks * rows, LANES)
+        total += jnp.dot(lines.astype(jnp.bfloat16), matrix, preferred_element_type=jnp.float32)
+    out_ref[...] = total.reshape(blocks, rows, total.shape[1]).astype(jnp.bfloat16)
+
+
+def stack_kernel(layer, *refs):
+    for index, ref in enumerate(refs[:-1]):
+        refs[-1][index] = ref[layer]
+
+
+def pack_kernel(own_ref, other_ref, tokens_ref, gain_ref, out_ref):
+    quarter = tokens_ref.shape[0] // 4
+    out_ref[pl.ds(0, LANES), :] = own_ref[0]
+    out_ref[pl.ds(LANES, LANES), :] = other_ref[0]
+    lines = []
+    for member in range(2):
+        near = tokens_ref[pl.ds(member * 2 * quarter, 2 * quarter), :].astype(jnp.float32)
+        lines.append(jnp.where(place()[0] == 0, near[quarter:], near[:quarter]))
+    out_ref[pl.ds(2 * LANES, 2 * quarter), :] = jnp.concatenate(lines, 0).astype(jnp.bfloat16)
+    rest = gain_ref[1:2, :]
+    pick = iota((16, rest.shape[1]), 0)
+    lines = jnp.zeros(pick.shape, jnp.float32)
+    for index in range(3):
+        term = rest.astype(jnp.bfloat16).astype(jnp.float32)
+        lines = jnp.where(pick == index, term, lines)
+        rest = rest - term
+    out_ref[pl.ds(2 * LANES + 2 * quarter, 16), :] = lines.astype(jnp.bfloat16)
+
+
 def settle_kernel(summed_ref, tokens_ref, packed_ref, *refs):
     rows_ref, spread_ref = refs[-2:]
     columns, rows, _ = summed_ref.shape
@@ -248,16 +288,18 @@
 
 
 def finish_kernel(summed_ref, rows_ref, back_ref, out_ref):
-    columns, half, depth = summed_ref.shape
+    columns, _, depth = summed_ref.shape
     first = place()[0] == 0
-    for member in range(2):
+    lines = []
+    for member in range(4):
         total = summed_ref[member].astype(jnp.float32)
-        for column in range(member + 2, columns, 2):
+        for column in range(member + 4, columns, 4):
             total += summed_ref[column].astype(jnp.float32)
-        near = rows_ref[member].astype(jnp.float32)[:, :depth]
-        core = back_ref[member].astype(jnp.float32)
-        held = jnp.concatenate([jnp.where(first, near, core), jnp.where(first, core, near)], 0)
-        out_ref[pl.ds(member * half, half), :] = (total + held).astype(jnp.bfloat16)
+        near = rows_ref[member // 2].astype(jnp.float32)[:, :depth]
+        core = back_ref[member // 2].astype(jnp.float32)
+        held = jnp.where(first, near, core) if member % 2 == 0 else jnp.where(first, core, near)
+        lines.append(total + held)
+    out_ref[...] = jnp.concatenate(lines, 0).astype(jnp.bfloat16)
 
 
 def params():
@@ -285,7 +327,7 @@
 
 
 def advance(layer, width, shared, arrived, limits, base, gain, states, awaited):
-    rows = limits.shape[0]
+    rows = limits.shape[1] * NEW
     return pl.pallas_call(
         functools.partial(advance_kernel, layer, rows, width),
         out_shape=(bf16(*shared), jax.ShapeDtypeStruct(states.shape[1:], jnp.float32)),
@@ -334,38 +376,32 @@
         [column * owners + owner for column in (first, first + 1) for owner in range(owners)]
         for first in range(0, columns, 2)
     ]
+    quads = [
+        [column * owners + owner for column in range(first, first + 4) for owner in range(owners)]
+        for first in range(0, columns, 4)
+    ]
     half, quarter = own_count // 2, own_count // 4
-    core = place()[0]
-    limits = jnp.broadcast_to(jnp.repeat(lengths, NEW)[:, None], (own_count, LANES))
+    limits = lengths.reshape(1, -1)
     gathered = exchange(jnp.broadcast_to(tokens, (columns, own_count, depth)), "tp")
     other_out = from_partner(w_out, "tp")
-    own_weights = jnp.stack([weight[1] for weight in weights])
+    own_weights = call(
+        functools.partial(stack_kernel, 1), bf16(6, depth, LANES), *weights
+    )
     other_weights = from_partner(own_weights, "tp")
-    quarters = tokens.reshape(2, 2, quarter, depth)
-    quarters = jnp.where(core == 0, quarters[:, 1], quarters[:, 0])
-    gain_line = norm_gain[1:2]
-    gain_lines = []
-    for _ in range(3):
-        term = lax.reduce_precision(gain_line, 8, 7)
-        gain_lines.append(term.astype(jnp.bfloat16))
-        gain_line = gain_line - term
-    packed = jnp.concatenate(
-        [
-            w_out[0],
-            other_out[0],
-            quarters.reshape(half, depth),
-            *gain_lines,
-            jnp.zeros((13, depth), jnp.bfloat16),
-        ],
-        0,
+    packed = call(
+        pack_kernel,
+        bf16(2 * LANES + half + 16, depth),
+        w_out, other_out, tokens, norm_gain,
     )
     packed = from_partner(packed, "dp")
+    out_pair = call(functools.partial(stack_kernel, 1), bf16(2, LANES, depth), w_out, other_out)
+    out_far = lax.ppermute(out_pair, "tp", [(i, i ^ 2) for i in range(columns)])
     core_own = from_partner(own_weights, "dp")
     core_other = from_partner(other_weights, "dp")
     far = call(
         functools.partial(project_kernel, True),
         bf16(columns, 3 * own_count + 8, LANES),
-        gathered, norm_gain, *weights,
+        gathered, norm_gain, *weights, limits, decay_base, group_gain,
     )
     came = from_partner(far, "dp")
     near = call(
@@ -383,7 +419,7 @@
         functools.partial(out_kernel, 0),
         bf16(columns, quarter, 2 * depth),
         shared.reshape(2, owners, quarter, LANES), w_out, other_out, packed,
-        awaited=[other_weights],
+        awaited=[other_weights, out_far],
     )
     summed = exchange(product, "tp")
     rows, spread = call(
@@ -401,14 +437,14 @@
     arrived = exchange(near.reshape(-1, *near.shape[2:]), both, pairs)
     back = from_partner(rows[:, :, depth:], "dp")
     shared, last_states = advance(
-        1, width, (2, owners, half, LANES), arrived, limits, decay_base, group_gain,
+        1, width, (4, owners, quarter, LANES), arrived, limits, decay_base, group_gain,
         folded, [],
     )
-    shared = exchange(shared.reshape(2 * owners, half, LANES), both, pairs)
+    shared = exchange(shared.reshape(4 * owners, quarter, LANES), both, quads)
     product = call(
-        functools.partial(out_kernel, 1),
-        bf16(columns, half, depth),
-        shared.reshape(2, owners, half, LANES), w_out, other_out,
+        out_quad_kernel,
+        bf16(columns, quarter, depth),
+        shared.reshape(4, owners, quarter, LANES), out_pair, out_far,
     )
     summed = exchange(product, "tp")
     own_rows = call(finish_kernel, bf16(own_count, depth), summed, rows, back)

time: 203 us -> 215 us (1.059)
  blocking collectives: 51.1 us -> 102 us
  starting transfers between devices: 86.4 us -> 53.4 us
  local copies, waits for them, and re-layouts: 6.95 us -> 1.47 us
    all_to_all x3, blocking collectives: 51.1 us -> 102 us  [exchange(): return lax.all_to_all(x, axis, 0, 0, tiled=True, axis_index_groups=groups)]
    all_to_all x5, starting transfers between devices: 67.4 us -> 33 us  [exchange(): return lax.all_to_all(x, axis, 0, 0, tiled=True, axis_index_groups=groups)]
    all_to_all x5, waiting for transfers between devices: 44.2 us -> 34 us  [exchange(): return lax.all_to_all(x, axis, 0, 0, tiled=True, axis_index_groups=groups)]
    ppermute x0 -> x1, waiting for transfers between devices: none -> 7.35 us  [per_device(): out_far = lax.ppermute(out_pair, 'tp', [(i, i ^ 2) for i in range(columns)])]
    ppermute x0 -> x1, starting transfers between devices: none -> 4.18 us  [per_device(): out_far = lax.ppermute(out_pair, 'tp', [(i, i ^ 2) for i in range(columns)])]
    unnamed x31 -> x30, local copies, waits for them, and re-layouts: 4.48 us -> 0.68 us
    ppermute x7, starting transfers between devices: 19 us -> 16.3 us  [from_partner(): lax.ppermute(x, axis, [(i, i ^ 1) for i in range(lax.axis_size(axis))])]
  transfers between devices with their start and end apart: 12 -> 13, of which waited for: 9 -> 8; matrix products, arithmetic and copies ran while one was open for 3% -> 0% of each run, Pallas kernels for 2% -> 1%
where the time goes in v6:
time: 215 us; the launch traced here: 214 us
  blocking collectives  102 us (47%)
  starting transfers between devices  53.4 us (25%)
  waiting for transfers between devices  46 us (21%)
  Pallas kernels  8.53 us (4%)
    all_to_all x3, blocking collectives, exchange(): return lax.all_to_all(x, axis, 0, 0, tiled=True, axis_index_groups=groups)  102 us
    all_to_all x5, waiting for transfers between devices, exchange(): return lax.all_to_all(x, axis, 0, 0, tiled=True, axis_index_groups=groups)  34 us
    all_to_all x5, starting transfers between devices, exchange(): return lax.all_to_all(x, axis, 0, 0, tiled=True, axis_index_groups=groups)  33 us
    ppermute x7, starting transfers between devices, from_partner(): lax.ppermute(x, axis, [(i, i ^ 1) for i in range(lax.axis_size(axis))])  16.3 us
    ppermute x1, waiting for transfers between devices, per_device(): out_far = lax.ppermute(out_pair, 'tp', [(i, i ^ 2) for i in range(columns)])  7.35 us
    ppermute x7, waiting for transfers between devices, from_partner(): lax.ppermute(x, axis, [(i, i ^ 1) for i in range(lax.axis_size(axis))])  4.63 us
    pallas_call x2, Pallas kernels, advance(): pl.pallas_call(functools.partial(advance_kernel, layer, rows, width), out...  4.4 us
  transfers between devices with their start and end apart: 13, of which 8 were waited for; matrix products, arithmetic and copies ran while one was open for 0% of the time, Pallas kernels for 1%

profile of v6, /device:TPU:80, one launch (start us, length us, event | category | flops | bytes accessed | tf_op | source)
XLA Modules:
  0.0 213.7 jit_solution(11868349843160449236)
XLA Ops:
  0.6 0.0 copy-start.5
  0.7 0.8 broadcast_in_dim.3
  1.5 0.0 copy-start.1
  1.5 0.0 copy-start.2
  1.5 0.0 copy-start.3
  1.5 0.0 copy-start.4
  1.5 61.7 %all_to_all.40.x_ref = bf16[16,32,256]{2,1,0:T(8,128)(2,1)S(1)} all-to-all(bf16[16,32,256]{2,1,0:T(8,128)(2,1)S(1)} %broadcast_in_dim.3), channel_id=1, replica_groups=mesh['grp'=2,'tp'=16,'dp'=16] {'tp'}, dimensions={0} | all-to-all | bytes 524288 | tf_op jit(solution)/shard_map/all_to_all | solution.py:345
  63.3 0.6 copy-done.12
  63.9 0.3 shard_map.140
  64.2 2.0 collective-permute-start
  66.2 1.7 collective-permute-done.refs_6_
  67.9 1.0 shard_map.141
  69.0 7.8 %all-to-all-start.1 = ((bf16[16,104,128]{2,1,0:T(8,128)(2,1)}), bf16[16,104,128]{2,1,0:T(8,128)(2,1)S(1)}, u32[]{:S(2)}, u32[]{:S(2)}) async-start(bf16[16,104,128]{2,1,0:T(8,128)(2,1)} %shard_map.141), calls=%async_computation.1 | async-start | bytes 851968 | tf_op jit(solution)/shard_map/all_to_all | solution.py:345
  76.7 0.0 copy-done.7
  76.7 0.0 copy-start
  76.8 3.7 %collective-permute-start.1 = (bf16[2,128,256]{2,1,0:T(8,128)(2,1)S(1)}, bf16[2,128,256]{2,1,0:T(8,128)(2,1)S(1)}, u32[]{:S(2)}, u32[]{:S(2)}) collective-permute-start(bf16[2,128,256]{2,1,0:T(8,128)(2,1)S(1)} %copy-done.7), channel_id=1, source_target_pairs={{0,16},{16,0},{32,48},{48,32},{64,80},{80,64},{96,112},{112,96},{1... | collective-permute-start | bytes 393224 | tf_op jit(solution)/shard_map/ppermute | solution.py:349
  80.5 2.3 %collective-permute-start.3 = (bf16[6,256,128]{2,1,0:T(8,128)(2,1)S(1)}, bf16[6,256,128]{2,1,0:T(8,128)(2,1)S(1)}, u32[]{:S(2)}, u32[]{:S(2)}) collective-permute-start(bf16[6,256,128]{2,1,0:T(8,128)(2,1)S(1)} %shard_map.144), channel_id=1, source_target_pairs={{0,16},{16,0},{32,48},{48,32},{64,80},{80,64},{96,112},{112,96},{1... | collective-permute-start | bytes 1179656 | tf_op jit(solution)/shard_map/ppermute | solution.py:349
  82.8 1.6 collective-permute-done.1.refs_0_.other_ref.refs_1_
  84.4 6.3 %all-to-all-done.1.arrived_ref = bf16[16,104,128]{2,1,0:T(8,128)(2,1)S(1)} async-done(((bf16[16,104,128]{2,1,0:T(8,128)(2,1)}), bf16[16,104,128]{2,1,0:T(8,128)(2,1)S(1)}, u32[]{:S(2)}, u32[]{:S(2)}) %all-to-all-start.1) | async-done | bytes 426016 | tf_op jit(solution)/shard_map/all_to_all | solution.py:345
  90.7 2.2 %shard_map.142 = (bf16[2,16,8,128]{3,2,1,0:T(8,128)(2,1)}, f32[512,128]{1,0:T(8,128)S(1)}) custom-call(bf16[16,104,128]{2,1,0:T(8,128)(2,1)S(1)} %all-to-all-done.1.arrived_ref, s32[1,8]{1,0:T(1,128)S(1)} %bitcast.25, f32[2,128]{1,0:T(2,128)S(1)} %copy-done.12, f32[2,128]{1,0:T(2,128)S(1)} %copy-done.13, f32[2,512,128]{2,1,0:T(8,128)S(1)} %bitcast.17, ...), custom_call_target="tpu_custom_call" | custom-call | flops 100000000 | bytes 2000000 | tf_op jit(solution)/shard_map/pallas_call | solution.py:331
  92.9 6.1 %all-to-all-start.2 = ((bf16[32,8,128]{2,1,0:T(8,128)(2,1)}), bf16[32,8,128]{2,1,0:T(8,128)(2,1)S(1)}, u32[]{:S(2)}, u32[]{:S(2)}) async-start(bf16[32,8,128]{2,1,0:T(8,128)(2,1)} %bitcast.4), calls=%async_computation.2 | async-start | bytes 131072 | tf_op jit(solution)/shard_map/all_to_all | solution.py:345
  99.1 2.0 collective-permute-start.2
  101.0 4.2 %collective-permute-start.4 = (bf16[2,128,256]{2,1,0:T(8,128)(2,1)S(1)}, bf16[2,128,256]{2,1,0:T(8,128)(2,1)S(1)}, u32[]{:S(2)}, u32[]{:S(2)}) collective-permute-start(bf16[2,128,256]{2,1,0:T(8,128)(2,1)S(1)} %shard_map.145.pair_ref), channel_id=1, source_target_pairs={{0,32},{16,48},{32,0},{48,16},{64,96},{80,112},{96,64},{112,80},{1... | collective-permute-start | bytes 393224 | tf_op jit(solution)/shard_map/ppermute | solution.py:398
  105.2 7.3 %collective-permute-done.4.refs_2_.far_ref = bf16[2,128,256]{2,1,0:T(8,128)(2,1)S(1)} collective-permute-done((bf16[2,128,256]{2,1,0:T(8,128)(2,1)S(1)}, bf16[2,128,256]{2,1,0:T(8,128)(2,1)S(1)}, u32[]{:S(2)}, u32[]{:S(2)}) %collective-permute-start.4) | collective-permute-done | bytes 131104 | tf_op jit(solution)/shard_map/ppermute | solution.py:398
  112.6 0.0 collective-permute-done.2.refs_0_.packed_ref
  112.6 0.0 collective-permute-done.3.refs_1_.refs_6_
  112.6 0.0 all-to-all-done.2
  112.6 0.9 shard_map.146
  113.5 5.8 %all-to-all-start.3 = ((bf16[16,8,512]{2,1,0:T(8,128)(2,1)}), bf16[16,8,512]{2,1,0:T(8,128)(2,1)S(1)}, u32[]{:S(2)}, u32[]{:S(2)}) async-start(bf16[16,8,512]{2,1,0:T(8,128)(2,1)} %shard_map.146), calls=%async_computation.3 | async-start | bytes 262144 | tf_op jit(solution)/shard_map/all_to_all | solution.py:345
  119.3 2.0 collective-permute-start.5
  121.2 2.4 %collective-permute-start.6 = (bf16[6,256,128]{2,1,0:T(8,128)(2,1)S(1)}, bf16[6,256,128]{2,1,0:T(8,128)(2,1)S(1)}, u32[]{:S(2)}, u32[]{:S(2)}) collective-permute-start(bf16[6,256,128]{2,1,0:T(8,128)(2,1)S(1)} %collective-permute-done.3.refs_1_.refs_6_), channel_id=1, source_target_pairs={{0,1},{1,0},{2,3},{3,2},{4,5},{5,4},{6,7},{7,6},{8,9},{9,8},{10,11... | collective-permute-start | bytes 1179656 | tf_op jit(solution)/shard_map/ppermute | solution.py:349
  123.7 0.0 collective-permute-done.5.refs_0_.refs_7_
  123.7 1.3 collective-permute-done.6.refs_1_.refs_8_
  125.0 8.9 %all-to-all-done.3.summed_ref = bf16[16,8,512]{2,1,0:T(8,128)(2,1)S(1)} async-done(((bf16[16,8,512]{2,1,0:T(8,128)(2,1)}), bf16[16,8,512]{2,1,0:T(8,128)(2,1)S(1)}, u32[]{:S(2)}, u32[]{:S(2)}) %all-to-all-start.3) | async-done | bytes 131104 | tf_op jit(solution)/shard_map/all_to_all | solution.py:345
  133.9 18.0 %all_to_all.41.x_ref = bf16[16,8,512]{2,1,0:T(8,128)(2,1)S(1)} all-to-all(bf16[16,8,512]{2,1,0:T(8,128)(2,1)S(1)} %get-tuple-element.9), channel_id=1, replica_groups=mesh['grp'=2,'tp'=16,'dp'=16] {'tp'}, dimensions={0} | all-to-all | bytes 262144 | tf_op jit(solution)/shard_map/all_to_all | solution.py:345
  151.9 0.4 shard_map.148
  152.3 22.5 %all_to_all.42.arrived_ref = bf16[32,56,128]{2,1,0:T(8,128)(2,1)S(1)} all-to-all(bf16[32,56,128]{2,1,0:T(8,128)(2,1)S(1)} %bitcast.19), channel_id=1, replica_groups={{0,1,2,3,4,5,6,7,8,9,10,11,12,13,14,15,16,17,18,19,20,21,22,23,24,25,26..., dimensions={0} | all-to-all | bytes 917504 | tf_op jit(solution)/shard_map/all_to_all | solution.py:345
  174.8 2.2 %shard_map.149 = (bf16[4,16,8,128]{3,2,1,0:T(8,128)(2,1)}, f32[512,128]{1,0:T(8,128)S(1)}) custom-call(bf16[32,56,128]{2,1,0:T(8,128)(2,1)S(1)} %all_to_all.42.arrived_ref, s32[1,8]{1,0:T(1,128)S(1)} %bitcast.26, f32[2,128]{1,0:T(2,128)S(1)} %copy-done.12, f32[2,128]{1,0:T(2,128)S(1)} %copy-done.13, f32[2,512,128]{2,1,0:T(8,128)S(1)} %bitcast.18), custom_call_target="tpu_custom_call" | custom-call | flops 100000000 | bytes 2000000 | tf_op jit(solution)/shard_map/pallas_call | solution.py:331
  177.0 8.1 %all-to-all-start.6 = ((bf16[64,8,128]{2,1,0:T(8,128)(2,1)}), bf16[64,8,128]{2,1,0:T(8,128)(2,1)S(1)}, u32[]{:S(2)}, u32[]{:S(2)}) async-start(bf16[64,8,128]{2,1,0:T(8,128)(2,1)} %bitcast.7), calls=%async_computation.6 | async-start | bytes 262144 | tf_op jit(solution)/shard_map/all_to_all | solution.py:345
  185.2 2.0 collective-permute-start.7
  187.1 7.4 %all-to-all-done.6 = bf16[64,8,128]{2,1,0:T(8,128)(2,1)S(1)} async-done(((bf16[64,8,128]{2,1,0:T(8,128)(2,1)}), bf16[64,8,128]{2,1,0:T(8,128)(2,1)S(1)}, u32[]{:S(2)}, u32[]{:S(2)}) %all-to-all-start.6) | async-done | bytes 131104 | tf_op jit(solution)/shard_map/all_to_all | solution.py:345
  194.5 0.8 shard_map.150
  195.3 5.2 %all-to-all-start.7 = ((bf16[16,8,256]{2,1,0:T(8,128)(2,1)}), bf16[16,8,256]{2,1,0:T(8,128)(2,1)S(1)}, u32[]{:S(2)}, u32[]{:S(2)}) async-start(bf16[16,8,256]{2,1,0:T(8,128)(2,1)} %shard_map.150), calls=%async_computation.7 | async-start | bytes 131072 | tf_op jit(solution)/shard_map/all_to_all | solution.py:345
  200.5 0.0 copy-done.9
  200.5 1.0 maximum_bitcast_fusion
  201.6 0.0 collective-permute-done.7.back_ref
  201.6 11.5 %all-to-all-done.7.summed_ref = bf16[16,8,256]{2,1,0:T(8,128)(2,1)S(1)} async-done(((bf16[16,8,256]{2,1,0:T(8,128)(2,1)}), bf16[16,8,256]{2,1,0:T(8,128)(2,1)S(1)}, u32[]{:S(2)}, u32[]{:S(2)}) %all-to-all-start.7) | async-done | bytes 65568 | tf_op jit(solution)/shard_map/all_to_all | solution.py:345
  213.1 0.6 shard_map.151
  (26 shorter events, 0.1 us)
Async XLA Ops:
  0.6 62.6 %copy-start.5 = (bf16[2,256,128]{2,1,0:T(8,128)(2,1)S(1)}, bf16[2,256,128]{2,1,0:T(8,128)(2,1)}, u32[]{:S(2)}) copy-start(bf16[2,256,128]{2,1,0:T(8,128)(2,1)} %refs_4_.7) | copy-start | bytes 393220
  0.6 62.6 %copy-start.6 = (bf16[2,256,128]{2,1,0:T(8,128)(2,1)S(1)}, bf16[2,256,128]{2,1,0:T(8,128)(2,1)}, u32[]{:S(2)}) copy-start(bf16[2,256,128]{2,1,0:T(8,128)(2,1)} %refs_5_.7) | copy-start | bytes 393220
  0.7 62.6 %copy-start.11 = (f32[2,256]{1,0:T(2,128)S(1)}, f32[2,256]{1,0:T(2,128)}, u32[]{:S(2)}) copy-start(f32[2,256]{1,0:T(2,128)} %gain_ref.10) | copy-start | bytes 6148
  0.7 62.6 %copy-start.13 = (f32[2,128]{1,0:T(2,128)S(1)}, f32[2,128]{1,0:T(2,128)}, u32[]{:S(2)}) copy-start(f32[2,128]{1,0:T(2,128)} %gain_ref.11) | copy-start | bytes 3076
  1.5 61.8 %copy-start.1 = (bf16[2,256,128]{2,1,0:T(8,128)(2,1)S(1)}, bf16[2,256,128]{2,1,0:T(8,128)(2,1)}, u32[]{:S(2)}) copy-start(bf16[2,256,128]{2,1,0:T(8,128)(2,1)} %refs_0_.9) | copy-start | bytes 393220
  1.5 61.8 %copy-start.2 = (bf16[2,256,128]{2,1,0:T(8,128)(2,1)S(1)}, bf16[2,256,128]{2,1,0:T(8,128)(2,1)}, u32[]{:S(2)}) copy-start(bf16[2,256,128]{2,1,0:T(8,128)(2,1)} %refs_1_.7) | copy-start | bytes 393220
  1.5 61.8 %copy-start.3 = (bf16[2,256,128]{2,1,0:T(8,128)(2,1)S(1)}, bf16[2,256,128]{2,1,0:T(8,128)(2,1)}, u32[]{:S(2)}) copy-start(bf16[2,256,128]{2,1,0:T(8,128)(2,1)} %refs_2_.7) | copy-start | bytes 393220
  1.5 61.8 %copy-start.4 = (bf16[2,256,128]{2,1,0:T(8,128)(2,1)S(1)}, bf16[2,256,128]{2,1,0:T(8,128)(2,1)}, u32[]{:S(2)}) copy-start(bf16[2,256,128]{2,1,0:T(8,128)(2,1)} %refs_3_.7) | copy-start | bytes 393220
  63.3 0.7 copy-start.12
  63.3 0.7 copy-start.14
  64.2 3.7 %collective-permute-start = (bf16[16,104,128]{2,1,0:T(8,128)(2,1)S(1)}, bf16[16,104,128]{2,1,0:T(8,128)(2,1)S(1)}, u32[]{:S(2)}, u32[]{:S(2)}) collective-permute-start(bf16[16,104,128]{2,1,0:T(8,128)(2,1)S(1)} %shard_map.140), channel_id=1, source_target_pairs={{0,1},{1,0},{2,3},{3,2},{4,5},{5,4},{6,7},{7,6},{8,9},{9,8},{10,11... | collective-permute-start | bytes 1277960 | tf_op jit(solution)/shard_map/ppermute | solution.py:349
  69.0 7.8 %copy-start.7 = (bf16[2,128,256]{2,1,0:T(8,128)(2,1)S(1)}, bf16[2,128,256]{2,1,0:T(8,128)(2,1)}, u32[]{:S(2)}) copy-start(bf16[2,128,256]{2,1,0:T(8,128)(2,1)} %own_ref.3) | copy-start | bytes 393220
  69.0 21.8 %all-to-all-start.1 = ((bf16[16,104,128]{2,1,0:T(8,128)(2,1)}), bf16[16,104,128]{2,1,0:T(8,128)(2,1)S(1)}, u32[]{:S(2)}, u32[]{:S(2)}) async-start(bf16[16,104,128]{2,1,0:T(8,128)(2,1)} %shard_map.141), calls=%async_computation.1 | async-start | bytes 851968 | tf_op jit(solution)/shard_map/all_to_all | solution.py:345
  76.7 14.0 %copy-start = (f32[2,8,2,4096]{3,2,1,0:T(2,128)S(1)}, f32[2,8,2,4096]{3,2,1,0:T(2,128)}, u32[]{:S(2)}) copy-start(f32[2,8,2,4096]{3,2,1,0:T(2,128)} %param.25) | copy-start | bytes 1572868
  76.8 7.7 %collective-permute-start.1 = (bf16[2,128,256]{2,1,0:T(8,128)(2,1)S(1)}, bf16[2,128,256]{2,1,0:T(8,128)(2,1)S(1)}, u32[]{:S(2)}, u32[]{:S(2)}) collective-permute-start(bf16[2,128,256]{2,1,0:T(8,128)(2,1)S(1)} %copy-done.7), channel_id=1, source_target_pairs={{0,16},{16,0},{32,48},{48,32},{64,80},{80,64},{96,112},{112,96},{1... | collective-permute-start | bytes 393224 | tf_op jit(solution)/shard_map/ppermute | solution.py:349
  80.5 32.1 %collective-permute-start.3 = (bf16[6,256,128]{2,1,0:T(8,128)(2,1)S(1)}, bf16[6,256,128]{2,1,0:T(8,128)(2,1)S(1)}, u32[]{:S(2)}, u32[]{:S(2)}) collective-permute-start(bf16[6,256,128]{2,1,0:T(8,128)(2,1)S(1)} %shard_map.144), channel_id=1, source_target_pairs={{0,16},{16,0},{32,48},{48,32},{64,80},{80,64},{96,112},{112,96},{1... | collective-permute-start | bytes 1179656 | tf_op jit(solution)/shard_map/ppermute | solution.py:349
  92.9 6.1 %copy-start.8 = (f32[512,128]{1,0:T(8,128)}, f32[512,128]{1,0:T(8,128)S(1)}, u32[]{:S(2)}) copy-start(f32[512,128]{1,0:T(8,128)S(1)} %get-tuple-element.12) | copy-start | bytes 786436
  92.9 6.1 %copy-start.10 = (bf16[32,256]{1,0:T(8,128)(2,1)S(1)}, bf16[32,256]{1,0:T(8,128)(2,1)}, u32[]{:S(2)}) copy-start(bf16[32,256]{1,0:T(8,128)(2,1)} %tokens_ref.3) | copy-start | bytes 49156
  92.9 19.6 %all-to-all-start.2 = ((bf16[32,8,128]{2,1,0:T(8,128)(2,1)}), bf16[32,8,128]{2,1,0:T(8,128)(2,1)S(1)}, u32[]{:S(2)}, u32[]{:S(2)}) async-start(bf16[32,8,128]{2,1,0:T(8,128)(2,1)} %bitcast.4), calls=%async_computation.2 | async-start | bytes 131072 | tf_op jit(solution)/shard_map/all_to_all | solution.py:345
  99.1 13.5 %collective-permute-start.2 = (bf16[288,256]{1,0:T(8,128)(2,1)S(1)}, bf16[288,256]{1,0:T(8,128)(2,1)S(1)}, u32[]{:S(2)}, u32[]{:S(2)}) collective-permute-start(bf16[288,256]{1,0:T(8,128)(2,1)S(1)} %shard_map.143), channel_id=1, source_target_pairs={{0,1},{1,0},{2,3},{3,2},{4,5},{5,4},{6,7},{7,6},{8,9},{9,8},{10,11... | collective-permute-start | bytes 442376 | tf_op jit(solution)/shard_map/ppermute | solution.py:349
  101.0 11.5 %collective-permute-start.4 = (bf16[2,128,256]{2,1,0:T(8,128)(2,1)S(1)}, bf16[2,128,256]{2,1,0:T(8,128)(2,1)S(1)}, u32[]{:S(2)}, u32[]{:S(2)}) collective-permute-start(bf16[2,128,256]{2,1,0:T(8,128)(2,1)S(1)} %shard_map.145.pair_ref), channel_id=1, source_target_pairs={{0,32},{16,48},{32,0},{48,16},{64,96},{80,112},{96,64},{112,80},{1... | collective-permute-start | bytes 393224 | tf_op jit(solution)/shard_map/ppermute | solution.py:398
  113.5 20.4 %all-to-all-start.3 = ((bf16[16,8,512]{2,1,0:T(8,128)(2,1)}), bf16[16,8,512]{2,1,0:T(8,128)(2,1)S(1)}, u32[]{:S(2)}, u32[]{:S(2)}) async-start(bf16[16,8,512]{2,1,0:T(8,128)(2,1)} %shard_map.146), calls=%async_computation.3 | async-start | bytes 262144 | tf_op jit(solution)/shard_map/all_to_all | solution.py:345
  119.3 4.4 %collective-permute-start.5 = (bf16[6,256,128]{2,1,0:T(8,128)(2,1)S(1)}, bf16[6,256,128]{2,1,0:T(8,128)(2,1)S(1)}, u32[]{:S(2)}, u32[]{:S(2)}) collective-permute-start(bf16[6,256,128]{2,1,0:T(8,128)(2,1)S(1)} %shard_map.144), channel_id=1, source_target_pairs={{0,1},{1,0},{2,3},{3,2},{4,5},{5,4},{6,7},{7,6},{8,9},{9,8},{10,11... | collective-permute-start | bytes 1179656 | tf_op jit(solution)/shard_map/ppermute | solution.py:349
  121.2 3.8 %collective-permute-start.6 = (bf16[6,256,128]{2,1,0:T(8,128)(2,1)S(1)}, bf16[6,256,128]{2,1,0:T(8,128)(2,1)S(1)}, u32[]{:S(2)}, u32[]{:S(2)}) collective-permute-start(bf16[6,256,128]{2,1,0:T(8,128)(2,1)S(1)} %collective-permute-done.3.refs_1_.refs_6_), channel_id=1, source_target_pairs={{0,1},{1,0},{2,3},{3,2},{4,5},{5,4},{6,7},{7,6},{8,9},{9,8},{10,11... | collective-permute-start | bytes 1179656 | tf_op jit(solution)/shard_map/ppermute | solution.py:349
  177.0 17.5 %all-to-all-start.6 = ((bf16[64,8,128]{2,1,0:T(8,128)(2,1)}), bf16[64,8,128]{2,1,0:T(8,128)(2,1)S(1)}, u32[]{:S(2)}, u32[]{:S(2)}) async-start(bf16[64,8,128]{2,1,0:T(8,128)(2,1)} %bitcast.7), calls=%async_computation.6 | async-start | bytes 262144 | tf_op jit(solution)/shard_map/all_to_all | solution.py:345
  185.2 16.4 %collective-permute-start.7 = (bf16[2,8,256]{2,1,0:T(8,128)(2,1)S(1)}, bf16[2,8,256]{2,1,0:T(8,128)(2,1)S(1)}, u32[]{:S(2)}, u32[]{:S(2)}) collective-permute-start(bf16[2,8,256]{2,1,0:T(8,128)(2,1)S(1)} %slice.3), channel_id=1, source_target_pairs={{0,1},{1,0},{2,3},{3,2},{4,5},{5,4},{6,7},{7,6},{8,9},{9,8},{10,11... | collective-permute-start | bytes 24584 | tf_op jit(solution)/shard_map/ppermute | solution.py:349
  194.5 6.1 %copy-start.9 = (f32[512,128]{1,0:T(8,128)S(1)}, f32[512,128]{1,0:T(8,128)}, u32[]{:S(2)}) copy-start(f32[512,128]{1,0:T(8,128)} %copy-done.8) | copy-start | bytes 786436
  195.3 17.8 %all-to-all-start.7 = ((bf16[16,8,256]{2,1,0:T(8,128)(2,1)}), bf16[16,8,256]{2,1,0:T(8,128)(2,1)S(1)}, u32[]{:S(2)}, u32[]{:S(2)}) async-start(bf16[16,8,256]{2,1,0:T(8,128)(2,1)} %shard_map.150), calls=%async_computation.7 | async-start | bytes 131072 | tf_op jit(solution)/shard_map/all_to_all | solution.py:345

commit v7 on v6

--- a/solution.py
+++ b/solution.py
@@ -106,7 +106,7 @@
             out_ref[member, block, pl.ds(6 * rows, 8), :] = squares_tail(row)
 
 
-def advance_kernel(layer, rows, width, arrived_ref, limits_ref, base_ref, gain_ref, state_ref, *refs):
+def advance_kernel(layer, rows, width, arrived_ref, limits_ref, lines_ref, state_ref, *refs):
     mixed_ref, new_ref, line_ref, read_ref = refs[-4:]
     seqs = rows // NEW
     parts, part_rows = arrived_ref.shape[0], (arrived_ref.shape[1] - 8) // 6
@@ -131,7 +131,7 @@
     same_head = (iota((LANES, LANES), 0) // HEAD == iota((LANES, LANES), 1) // HEAD).astype(
         jnp.float32
     ).astype(jnp.bfloat16)
-    log_rate = base_ref[layer : layer + 1, :] + decay_pre
+    log_rate = lines_ref[layer : layer + 1, :] + decay_pre
     decays = jnp.exp(jax.nn.sigmoid(log_rate) * (-0.6065306597126334))
     rates = jax.nn.sigmoid(rate_pre)
     unit = keys * lax.rsqrt(split_dot(keys * keys, same_head) + unit_epsilon)
@@ -201,7 +201,7 @@
     read = read_ref[...]
     centred = read - split_dot(read, same_head) / HEAD
     variance = split_dot(centred * centred, same_head) / HEAD
-    normed = centred * lax.rsqrt(variance + group_epsilon) * gain_ref[layer : layer + 1, :]
+    normed = centred * lax.rsqrt(variance + group_epsilon) * lines_ref[2 + layer : 3 + layer, :]
     mixed = jnp.where(live, normed * jax.nn.sigmoid(gate_pre), 0.0)
     members, owners, share, _ = mixed_ref.shape
     for member in range(members):
@@ -232,17 +232,8 @@
         )
 
 
-def out_quad_kernel(mixed_ref, pair_ref, far_ref, out_ref):
-    members, blocks, rows, _ = mixed_ref.shape
-    me = lax.rem(lax.axis_index("tp"), members)
-    total = 0.0
-    for member in range(members):
-        offset = jnp.bitwise_xor(me, member)
-        side = lax.rem(offset, 2)
-        matrix = jnp.where(offset < 2, pair_ref[side], far_ref[side])
-        lines = mixed_ref[member].astype(jnp.float32).reshape(blocks * rows, LANES)
-        total += jnp.dot(lines.astype(jnp.bfloat16), matrix, preferred_element_type=jnp.float32)
-    out_ref[...] = total.reshape(blocks, rows, total.shape[1]).astype(jnp.bfloat16)
+def join_kernel(first_ref, second_ref, out_ref):
+    out_ref[...] = jnp.concatenate([first_ref[...], second_ref[...]], 0)
 
 
 def stack_kernel(layer, *refs):
@@ -288,18 +279,16 @@
 
 
 def finish_kernel(summed_ref, rows_ref, back_ref, out_ref):
-    columns, _, depth = summed_ref.shape
+    columns, half, depth = summed_ref.shape
     first = place()[0] == 0
-    lines = []
-    for member in range(4):
+    for member in range(2):
         total = summed_ref[member].astype(jnp.float32)
-        for column in range(member + 4, columns, 4):
+        for column in range(member + 2, columns, 2):
             total += summed_ref[column].astype(jnp.float32)
-        near = rows_ref[member // 2].astype(jnp.float32)[:, :depth]
-        core = back_ref[member // 2].astype(jnp.float32)
-        held = jnp.where(first, near, core) if member % 2 == 0 else jnp.where(first, core, near)
-        lines.append(total + held)
-    out_ref[...] = jnp.concatenate(lines, 0).astype(jnp.bfloat16)
+        near = rows_ref[member].astype(jnp.float32)[:, :depth]
+        core = back_ref[member].astype(jnp.float32)
+        held = jnp.concatenate([jnp.where(first, near, core), jnp.where(first, core, near)], 0)
+        out_ref[pl.ds(member * half, half), :] = (total + held).astype(jnp.bfloat16)
 
 
 def params():
@@ -326,19 +315,19 @@
     return jax.ShapeDtypeStruct(shape, jnp.bfloat16)
 
 
-def advance(layer, width, shared, arrived, limits, base, gain, states, awaited):
+def advance(layer, width, shared, arrived, limits, lines, states, awaited):
     rows = limits.shape[1] * NEW
     return pl.pallas_call(
         functools.partial(advance_kernel, layer, rows, width),
         out_shape=(bf16(*shared), jax.ShapeDtypeStruct(states.shape[1:], jnp.float32)),
-        in_specs=[VMEM] * 5 + [pl.BlockSpec(memory_space=pl.ANY)] * len(awaited),
+        in_specs=[VMEM] * 4 + [pl.BlockSpec(memory_space=pl.ANY)] * len(awaited),
         out_specs=(VMEM, VMEM),
         scratch_shapes=[
             pltpu.VMEM((11, rows, LANES), jnp.float32),
             pltpu.VMEM((rows, LANES), jnp.float32),
         ],
         **params(),
-    )(arrived, limits, base, gain, states, *awaited)
+    )(arrived, limits, lines, states, *awaited)
 
 
 def exchange(x, axis, groups=None):
@@ -376,10 +365,6 @@
         [column * owners + owner for column in (first, first + 1) for owner in range(owners)]
         for first in range(0, columns, 2)
     ]
-    quads = [
-        [column * owners + owner for column in range(first, first + 4) for owner in range(owners)]
-        for first in range(0, columns, 4)
-    ]
     half, quarter = own_count // 2, own_count // 4
     limits = lengths.reshape(1, -1)
     gathered = exchange(jnp.broadcast_to(tokens, (columns, own_count, depth)), "tp")
@@ -388,20 +373,24 @@
         functools.partial(stack_kernel, 1), bf16(6, depth, LANES), *weights
     )
     other_weights = from_partner(own_weights, "tp")
+    lines = call(
+        join_kernel,
+        jax.ShapeDtypeStruct((4, decay_base.shape[1]), jnp.float32),
+        decay_base, group_gain,
+    )
     packed = call(
         pack_kernel,
         bf16(2 * LANES + half + 16, depth),
         w_out, other_out, tokens, norm_gain,
     )
     packed = from_partner(packed, "dp")
-    out_pair = call(functools.partial(stack_kernel, 1), bf16(2, LANES, depth), w_out, other_out)
-    out_far = lax.ppermute(out_pair, "tp", [(i, i ^ 2) for i in range(columns)])
     core_own = from_partner(own_weights, "dp")
     core_other = from_partner(other_weights, "dp")
     far = call(
         functools.partial(project_kernel, True),
         bf16(columns, 3 * own_count + 8, LANES),
-        gathered, norm_gain, *weights, limits, decay_base, group_gain,
+        gathered, norm_gain, *weights,
+        awaited=[core_own],
     )
     came = from_partner(far, "dp")
     near = call(
@@ -411,22 +400,20 @@
     )
     arrived = exchange(near, "dp")
     shared, first_states = advance(
-        0, width, (2, owners, quarter, LANES), arrived, limits, decay_base, group_gain,
-        folded, [other_out],
+        0, width, (2, owners, quarter, LANES), arrived, limits, lines, folded, [packed],
     )
     shared = exchange(shared.reshape(2 * owners, quarter, LANES), both, pairs)
     product = call(
         functools.partial(out_kernel, 0),
         bf16(columns, quarter, 2 * depth),
         shared.reshape(2, owners, quarter, LANES), w_out, other_out, packed,
-        awaited=[other_weights, out_far],
+        awaited=[core_other],
     )
     summed = exchange(product, "tp")
     rows, spread = call(
         settle_kernel,
         (bf16(2, quarter, 2 * depth), bf16(columns, quarter, 2 * depth)),
         summed, tokens, packed,
-        awaited=[core_own, core_other],
     )
     gathered = exchange(spread, "tp")
     near = call(
@@ -437,14 +424,13 @@
     arrived = exchange(near.reshape(-1, *near.shape[2:]), both, pairs)
     back = from_partner(rows[:, :, depth:], "dp")
     shared, last_states = advance(
-        1, width, (4, owners, quarter, LANES), arrived, limits, decay_base, group_gain,
-        folded, [],
-    )
-    shared = exchange(shared.reshape(4 * owners, quarter, LANES), both, quads)
+        1, width, (2, owners, half, LANES), arrived, limits, lines, folded, [],
+    )
+    shared = exchange(shared.reshape(2 * owners, half, LANES), both, pairs)
     product = call(
-        out_quad_kernel,
-        bf16(columns, quarter, depth),
-        shared.reshape(4, owners, quarter, LANES), out_pair, out_far,
+        functools.partial(out_kernel, 1),
+        bf16(columns, half, depth),
+        shared.reshape(2, owners, half, LANES), w_out, other_out,
     )
     summed = exchange(product, "tp")
     own_rows = call(finish_kernel, bf16(own_count, depth), summed, rows, back)

time: 215 us -> 212 us (0.986)
  blocking collectives: 102 us -> 70.6 us
  starting transfers between devices: 53.4 us -> 80.9 us
    all_to_all x5 -> x4, starting transfers between devices: 33 us -> 64.7 us  [exchange(): return lax.all_to_all(x, axis, 0, 0, tiled=True, axis_index_groups=groups)]
    all_to_all x3 -> x4, blocking collectives: 102 us -> 70.6 us  [exchange(): return lax.all_to_all(x, axis, 0, 0, tiled=True, axis_index_groups=groups)]
    ppermute x7, waiting for transfers between devices: 4.63 us -> 13.5 us  [from_partner(): lax.ppermute(x, axis, [(i, i ^ 1) for i in range(lax.axis_size(axis))])]
    ppermute x1 -> x0, waiting for transfers between devices: 7.35 us -> none  [per_device(): out_far = lax.ppermute(out_pair, 'tp', [(i, i ^ 2) for i in range(columns)])]
    ppermute x1 -> x0, starting transfers between devices: 4.18 us -> none  [per_device(): out_far = lax.ppermute(out_pair, 'tp', [(i, i ^ 2) for i in range(columns)])]
    all_to_all x5 -> x4, waiting for transfers between devices: 34 us -> 33.4 us  [exchange(): return lax.all_to_all(x, axis, 0, 0, tiled=True, axis_index_groups=groups)]
  transfers between devices with their start and end apart: 13 -> 11, of which waited for: 8 -> 7; matrix products, arithmetic and copies ran while one was open for 0% -> 0% of each run, Pallas kernels for 1% -> 1%
where the time goes in v7:
time: 212 us; the launch traced here: 211 us
  starting transfers between devices  80.9 us (38%)
  blocking collectives  70.6 us (33%)
  waiting for transfers between devices  47 us (22%)
  Pallas kernels  7.27 us (3%)
  local copies, waits for them, and re-layouts  2.89 us (1%)
    all_to_all x4, blocking collectives, exchange(): return lax.all_to_all(x, axis, 0, 0, tiled=True, axis_index_groups=groups)  70.6 us
    all_to_all x4, starting transfers between devices, exchange(): return lax.all_to_all(x, axis, 0, 0, tiled=True, axis_index_groups=groups)  64.7 us
    all_to_all x4, waiting for transfers between devices, exchange(): return lax.all_to_all(x, axis, 0, 0, tiled=True, axis_index_groups=groups)  33.4 us
    ppermute x7, starting transfers between devices, from_partner(): lax.ppermute(x, axis, [(i, i ^ 1) for i in range(lax.axis_size(axis))])  16.3 us
    ppermute x7, waiting for transfers between devices, from_partner(): lax.ppermute(x, axis, [(i, i ^ 1) for i in range(lax.axis_size(axis))])  13.5 us
  transfers between devices with their start and end apart: 11, of which 7 were waited for; matrix products, arithmetic and copies ran while one was open for 0% of the time, Pallas kernels for 1%

profile of v7, /device:TPU:80, one launch (start us, length us, event | category | flops | bytes accessed | tf_op | source)
XLA Modules:
  0.0 210.7 jit_solution(2625040607414910602)
XLA Ops:
  0.6 0.0 copy-start.4
  0.6 0.0 copy-start.5
  0.6 1.5 broadcast_in_dim.3
  2.1 43.8 %all-to-all-start = ((bf16[16,32,256]{2,1,0:T(8,128)(2,1)}), bf16[16,32,256]{2,1,0:T(8,128)(2,1)S(1)}, u32[]{:S(2)}, u32[]{:S(2)}) async-start(bf16[16,32,256]{2,1,0:T(8,128)(2,1)} %broadcast_in_dim.3), calls=%async_computation | async-start | bytes 524288 | tf_op jit(solution)/shard_map/all_to_all | solution.py:334
  46.0 0.0 copy-done.4
  46.0 0.0 copy-done.5
  46.0 0.0 copy-done
  46.0 0.0 copy-done.1
  46.0 0.0 copy-done.2
  46.0 0.0 copy-start.11
  46.1 2.0 collective-permute-start
  48.1 1.7 collective-permute-done.refs_6_.refs_7_
  49.7 14.4 %all-to-all-done.x_ref = bf16[16,32,256]{2,1,0:T(8,128)(2,1)S(1)} async-done(((bf16[16,32,256]{2,1,0:T(8,128)(2,1)}), bf16[16,32,256]{2,1,0:T(8,128)(2,1)S(1)}, u32[]{:S(2)}, u32[]{:S(2)}) %all-to-all-start) | async-done | bytes 262176 | tf_op jit(solution)/shard_map/all_to_all | solution.py:334
  64.1 0.3 shard_map.141
  64.4 2.0 collective-permute-start.1
  66.3 1.7 collective-permute-done.1.refs_6_
  68.1 1.0 shard_map.142
  69.1 7.8 %all-to-all-start.1 = ((bf16[16,104,128]{2,1,0:T(8,128)(2,1)}), bf16[16,104,128]{2,1,0:T(8,128)(2,1)S(1)}, u32[]{:S(2)}, u32[]{:S(2)}) async-start(bf16[16,104,128]{2,1,0:T(8,128)(2,1)} %shard_map.142), calls=%async_computation.1 | async-start | bytes 851968 | tf_op jit(solution)/shard_map/all_to_all | solution.py:334
  76.9 0.0 copy-start.6
  76.9 3.7 %collective-permute-start.4 = (bf16[6,256,128]{2,1,0:T(8,128)(2,1)S(1)}, bf16[6,256,128]{2,1,0:T(8,128)(2,1)S(1)}, u32[]{:S(2)}, u32[]{:S(2)}) collective-permute-start(bf16[6,256,128]{2,1,0:T(8,128)(2,1)S(1)} %shard_map.140), channel_id=1, source_target_pairs={{0,16},{16,0},{32,48},{48,32},{64,80},{80,64},{96,112},{112,96},{1... | collective-permute-start | bytes 1179656 | tf_op jit(solution)/shard_map/ppermute | solution.py:338
  80.7 2.3 %collective-permute-start.2 = (bf16[2,128,256]{2,1,0:T(8,128)(2,1)S(1)}, bf16[2,128,256]{2,1,0:T(8,128)(2,1)S(1)}, u32[]{:S(2)}, u32[]{:S(2)}) collective-permute-start(bf16[2,128,256]{2,1,0:T(8,128)(2,1)S(1)} %copy-done.7), channel_id=1, source_target_pairs={{0,16},{16,0},{32,48},{48,32},{64,80},{80,64},{96,112},{112,96},{1... | collective-permute-start | bytes 393224 | tf_op jit(solution)/shard_map/ppermute | solution.py:338
  83.0 10.0 %collective-permute-done.2.other_ref = bf16[2,128,256]{2,1,0:T(8,128)(2,1)S(1)} collective-permute-done((bf16[2,128,256]{2,1,0:T(8,128)(2,1)S(1)}, bf16[2,128,256]{2,1,0:T(8,128)(2,1)S(1)}, u32[]{:S(2)}, u32[]{:S(2)}) %collective-permute-start.2) | collective-permute-done | bytes 131104 | tf_op jit(solution)/shard_map/ppermute | solution.py:338
  93.0 1.9 collective-permute-start.3
  95.0 0.0 collective-permute-done.4.refs_6_
  95.0 2.4 %collective-permute-start.5 = (bf16[6,256,128]{2,1,0:T(8,128)(2,1)S(1)}, bf16[6,256,128]{2,1,0:T(8,128)(2,1)S(1)}, u32[]{:S(2)}, u32[]{:S(2)}) collective-permute-start(bf16[6,256,128]{2,1,0:T(8,128)(2,1)S(1)} %collective-permute-done.4.refs_6_), channel_id=1, source_target_pairs={{0,1},{1,0},{2,3},{3,2},{4,5},{5,4},{6,7},{7,6},{8,9},{9,8},{10,11... | collective-permute-start | bytes 1179656 | tf_op jit(solution)/shard_map/ppermute | solution.py:338
  97.5 0.0 collective-permute-done.3.refs_0_.packed_ref
  97.5 0.0 all-to-all-done.1.arrived_ref
  97.5 0.0 copy-start.12
  97.5 0.6 copy-done.12
  98.2 2.2 %shard_map.145 = (bf16[2,16,8,128]{3,2,1,0:T(8,128)(2,1)}, f32[512,128]{1,0:T(8,128)S(1)}) custom-call(bf16[16,104,128]{2,1,0:T(8,128)(2,1)S(1)} %all-to-all-done.1.arrived_ref, s32[1,8]{1,0:T(1,128)S(1)} %bitcast.25, f32[4,128]{1,0:T(4,128)S(1)} %shard_map.143.lines_ref, f32[2,512,128]{2,1,0:T(8,128)S(1)} %bitcast.17, ...), custom_call_target="tpu_custom_call" | custom-call | flops 100000000 | bytes 2000000 | tf_op jit(solution)/shard_map/pallas_call | solution.py:320
  100.4 0.7 copy-done.8
  101.1 9.0 %all-to-all-start.2 = ((bf16[32,8,128]{2,1,0:T(8,128)(2,1)}), bf16[32,8,128]{2,1,0:T(8,128)(2,1)S(1)}, u32[]{:S(2)}, u32[]{:S(2)}) async-start(bf16[32,8,128]{2,1,0:T(8,128)(2,1)} %bitcast.4), calls=%async_computation.2 | async-start | bytes 131072 | tf_op jit(solution)/shard_map/all_to_all | solution.py:334
  110.1 0.0 collective-permute-done.5.refs_1_.refs_8_
  110.1 8.0 %all-to-all-done.2 = bf16[32,8,128]{2,1,0:T(8,128)(2,1)S(1)} async-done(((bf16[32,8,128]{2,1,0:T(8,128)(2,1)}), bf16[32,8,128]{2,1,0:T(8,128)(2,1)S(1)}, u32[]{:S(2)}, u32[]{:S(2)}) %all-to-all-start.2) | async-done | bytes 65568 | tf_op jit(solution)/shard_map/all_to_all | solution.py:334
  118.1 0.2 shard_map.146
  118.3 19.9 %all_to_all.40.summed_ref = bf16[16,8,512]{2,1,0:T(8,128)(2,1)S(1)} all-to-all(bf16[16,8,512]{2,1,0:T(8,128)(2,1)S(1)} %shard_map.146), channel_id=1, replica_groups=mesh['grp'=2,'tp'=16,'dp'=16] {'tp'}, dimensions={0} | all-to-all | bytes 262144 | tf_op jit(solution)/shard_map/all_to_all | solution.py:334
  138.2 17.7 %all_to_all.41.x_ref = bf16[16,8,512]{2,1,0:T(8,128)(2,1)S(1)} all-to-all(bf16[16,8,512]{2,1,0:T(8,128)(2,1)S(1)} %get-tuple-element.9), channel_id=1, replica_groups=mesh['grp'=2,'tp'=16,'dp'=16] {'tp'}, dimensions={0} | all-to-all | bytes 262144 | tf_op jit(solution)/shard_map/all_to_all | solution.py:334
  155.9 0.4 shard_map.148
  156.3 19.0 %all_to_all.42.arrived_ref = bf16[32,56,128]{2,1,0:T(8,128)(2,1)S(1)} all-to-all(bf16[32,56,128]{2,1,0:T(8,128)(2,1)S(1)} %bitcast.19), channel_id=1, replica_groups={{0,1,2,3,4,5,6,7,8,9,10,11,12,13,14,15,16,17,18,19,20,21,22,23,24,25,26..., dimensions={0} | all-to-all | bytes 917504 | tf_op jit(solution)/shard_map/all_to_all | solution.py:334
  175.2 1.6 shard_map.149
  176.8 14.1 %all_to_all.43 = bf16[32,16,128]{2,1,0:T(8,128)(2,1)S(1)} all-to-all(bf16[32,16,128]{2,1,0:T(8,128)(2,1)S(1)} %bitcast.24), channel_id=1, replica_groups={{0,1,2,3,4,5,6,7,8,9,10,11,12,13,14,15,16,17,18,19,20,21,22,23,24,25,26..., dimensions={0} | all-to-all | bytes 262144 | tf_op jit(solution)/shard_map/all_to_all | solution.py:334
  190.9 0.9 shard_map.150
  191.8 4.1 %all-to-all-start.7 = ((bf16[16,16,256]{2,1,0:T(8,128)(2,1)}), bf16[16,16,256]{2,1,0:T(8,128)(2,1)S(1)}, u32[]{:S(2)}, u32[]{:S(2)}) async-start(bf16[16,16,256]{2,1,0:T(8,128)(2,1)} %shard_map.150), calls=%async_computation.7 | async-start | bytes 262144 | tf_op jit(solution)/shard_map/all_to_all | solution.py:334
  195.9 2.0 collective-permute-start.6
  197.9 1.0 maximum_bitcast_fusion
  198.9 0.1 collective-permute-done.6.back_ref
  199.0 11.0 %all-to-all-done.7.summed_ref = bf16[16,16,256]{2,1,0:T(8,128)(2,1)S(1)} async-done(((bf16[16,16,256]{2,1,0:T(8,128)(2,1)}), bf16[16,16,256]{2,1,0:T(8,128)(2,1)S(1)}, u32[]{:S(2)}, u32[]{:S(2)}) %all-to-all-start.7) | async-done | bytes 131104 | tf_op jit(solution)/shard_map/all_to_all | solution.py:334
  210.0 0.6 shard_map.151
  (23 shorter events, 0.1 us)
Async XLA Ops:
  0.6 45.4 %copy-start.4 = (bf16[2,256,128]{2,1,0:T(8,128)(2,1)S(1)}, bf16[2,256,128]{2,1,0:T(8,128)(2,1)}, u32[]{:S(2)}) copy-start(bf16[2,256,128]{2,1,0:T(8,128)(2,1)} %refs_4_.7) | copy-start | bytes 393220
  0.6 45.4 %copy-start.5 = (bf16[2,256,128]{2,1,0:T(8,128)(2,1)S(1)}, bf16[2,256,128]{2,1,0:T(8,128)(2,1)}, u32[]{:S(2)}) copy-start(bf16[2,256,128]{2,1,0:T(8,128)(2,1)} %refs_5_.7) | copy-start | bytes 393220
  2.1 43.9 %copy-start = (bf16[2,256,128]{2,1,0:T(8,128)(2,1)S(1)}, bf16[2,256,128]{2,1,0:T(8,128)(2,1)}, u32[]{:S(2)}) copy-start(bf16[2,256,128]{2,1,0:T(8,128)(2,1)} %refs_0_.7) | copy-start | bytes 393220
  2.1 43.9 %copy-start.1 = (bf16[2,256,128]{2,1,0:T(8,128)(2,1)S(1)}, bf16[2,256,128]{2,1,0:T(8,128)(2,1)}, u32[]{:S(2)}) copy-start(bf16[2,256,128]{2,1,0:T(8,128)(2,1)} %refs_1_.7) | copy-start | bytes 393220
  2.1 43.9 %copy-start.2 = (bf16[2,256,128]{2,1,0:T(8,128)(2,1)S(1)}, bf16[2,256,128]{2,1,0:T(8,128)(2,1)}, u32[]{:S(2)}) copy-start(bf16[2,256,128]{2,1,0:T(8,128)(2,1)} %refs_2_.7) | copy-start | bytes 393220
  2.1 43.9 %copy-start.3 = (bf16[2,256,128]{2,1,0:T(8,128)(2,1)S(1)}, bf16[2,256,128]{2,1,0:T(8,128)(2,1)}, u32[]{:S(2)}) copy-start(bf16[2,256,128]{2,1,0:T(8,128)(2,1)} %refs_3_.7) | copy-start | bytes 393220
  2.1 62.0 %all-to-all-start = ((bf16[16,32,256]{2,1,0:T(8,128)(2,1)}), bf16[16,32,256]{2,1,0:T(8,128)(2,1)S(1)}, u32[]{:S(2)}, u32[]{:S(2)}) async-start(bf16[16,32,256]{2,1,0:T(8,128)(2,1)} %broadcast_in_dim.3), calls=%async_computation | async-start | bytes 524288 | tf_op jit(solution)/shard_map/all_to_all | solution.py:334
  46.0 18.1 %copy-start.11 = (f32[2,256]{1,0:T(2,128)S(1)}, f32[2,256]{1,0:T(2,128)}, u32[]{:S(2)}) copy-start(f32[2,256]{1,0:T(2,128)} %gain_ref.7) | copy-start | bytes 6148
  46.1 3.6 %collective-permute-start = (bf16[6,256,128]{2,1,0:T(8,128)(2,1)S(1)}, bf16[6,256,128]{2,1,0:T(8,128)(2,1)S(1)}, u32[]{:S(2)}, u32[]{:S(2)}) collective-permute-start(bf16[6,256,128]{2,1,0:T(8,128)(2,1)S(1)} %shard_map.140), channel_id=1, source_target_pairs={{0,1},{1,0},{2,3},{3,2},{4,5},{5,4},{6,7},{7,6},{8,9},{9,8},{10,11... | collective-permute-start | bytes 1179656 | tf_op jit(solution)/shard_map/ppermute | solution.py:338
  64.4 3.7 %collective-permute-start.1 = (bf16[16,104,128]{2,1,0:T(8,128)(2,1)S(1)}, bf16[16,104,128]{2,1,0:T(8,128)(2,1)S(1)}, u32[]{:S(2)}, u32[]{:S(2)}) collective-permute-start(bf16[16,104,128]{2,1,0:T(8,128)(2,1)S(1)} %shard_map.141), channel_id=1, source_target_pairs={{0,1},{1,0},{2,3},{3,2},{4,5},{5,4},{6,7},{7,6},{8,9},{9,8},{10,11... | collective-permute-start | bytes 1277960 | tf_op jit(solution)/shard_map/ppermute | solution.py:338
  69.1 11.5 %copy-start.7 = (bf16[2,128,256]{2,1,0:T(8,128)(2,1)S(1)}, bf16[2,128,256]{2,1,0:T(8,128)(2,1)}, u32[]{:S(2)}) copy-start(bf16[2,128,256]{2,1,0:T(8,128)(2,1)} %own_ref.5) | copy-start | bytes 393220
  69.1 23.9 %copy-start.10 = (bf16[32,256]{1,0:T(8,128)(2,1)S(1)}, bf16[32,256]{1,0:T(8,128)(2,1)}, u32[]{:S(2)}) copy-start(bf16[32,256]{1,0:T(8,128)(2,1)} %tokens_ref.3) | copy-start | bytes 49156
  69.1 28.3 %copy-start.13 = (f32[2,128]{1,0:T(2,128)S(1)}, f32[2,128]{1,0:T(2,128)}, u32[]{:S(2)}) copy-start(f32[2,128]{1,0:T(2,128)} %first_ref.1) | copy-start | bytes 3076
  69.1 28.3 %copy-start.14 = (f32[2,128]{1,0:T(2,128)S(1)}, f32[2,128]{1,0:T(2,128)}, u32[]{:S(2)}) copy-start(f32[2,128]{1,0:T(2,128)} %second_ref.1) | copy-start | bytes 3076
  69.1 28.4 %all-to-all-start.1 = ((bf16[16,104,128]{2,1,0:T(8,128)(2,1)}), bf16[16,104,128]{2,1,0:T(8,128)(2,1)S(1)}, u32[]{:S(2)}, u32[]{:S(2)}) async-start(bf16[16,104,128]{2,1,0:T(8,128)(2,1)} %shard_map.142), calls=%async_computation.1 | async-start | bytes 851968 | tf_op jit(solution)/shard_map/all_to_all | solution.py:334
  76.9 20.6 %copy-start.6 = (f32[2,8,2,4096]{3,2,1,0:T(2,128)S(1)}, f32[2,8,2,4096]{3,2,1,0:T(2,128)}, u32[]{:S(2)}) copy-start(f32[2,8,2,4096]{3,2,1,0:T(2,128)} %param.25) | copy-start | bytes 1572868
  76.9 18.1 %collective-permute-start.4 = (bf16[6,256,128]{2,1,0:T(8,128)(2,1)S(1)}, bf16[6,256,128]{2,1,0:T(8,128)(2,1)S(1)}, u32[]{:S(2)}, u32[]{:S(2)}) collective-permute-start(bf16[6,256,128]{2,1,0:T(8,128)(2,1)S(1)} %shard_map.140), channel_id=1, source_target_pairs={{0,16},{16,0},{32,48},{48,32},{64,80},{80,64},{96,112},{112,96},{1... | collective-permute-start | bytes 1179656 | tf_op jit(solution)/shard_map/ppermute | solution.py:338
  80.7 12.4 %collective-permute-start.2 = (bf16[2,128,256]{2,1,0:T(8,128)(2,1)S(1)}, bf16[2,128,256]{2,1,0:T(8,128)(2,1)S(1)}, u32[]{:S(2)}, u32[]{:S(2)}) collective-permute-start(bf16[2,128,256]{2,1,0:T(8,128)(2,1)S(1)} %copy-done.7), channel_id=1, source_target_pairs={{0,16},{16,0},{32,48},{48,32},{64,80},{80,64},{96,112},{112,96},{1... | collective-permute-start | bytes 393224 | tf_op jit(solution)/shard_map/ppermute | solution.py:338
  93.0 4.4 %collective-permute-start.3 = (bf16[288,256]{1,0:T(8,128)(2,1)S(1)}, bf16[288,256]{1,0:T(8,128)(2,1)S(1)}, u32[]{:S(2)}, u32[]{:S(2)}) collective-permute-start(bf16[288,256]{1,0:T(8,128)(2,1)S(1)} %shard_map.144), channel_id=1, source_target_pairs={{0,1},{1,0},{2,3},{3,2},{4,5},{5,4},{6,7},{7,6},{8,9},{9,8},{10,11... | collective-permute-start | bytes 442376 | tf_op jit(solution)/shard_map/ppermute | solution.py:338
  95.0 15.1 %collective-permute-start.5 = (bf16[6,256,128]{2,1,0:T(8,128)(2,1)S(1)}, bf16[6,256,128]{2,1,0:T(8,128)(2,1)S(1)}, u32[]{:S(2)}, u32[]{:S(2)}) collective-permute-start(bf16[6,256,128]{2,1,0:T(8,128)(2,1)S(1)} %collective-permute-done.4.refs_6_), channel_id=1, source_target_pairs={{0,1},{1,0},{2,3},{3,2},{4,5},{5,4},{6,7},{7,6},{8,9},{9,8},{10,11... | collective-permute-start | bytes 1179656 | tf_op jit(solution)/shard_map/ppermute | solution.py:338
  97.5 0.7 copy-start.12
  100.4 0.7 copy-start.8
  101.1 17.0 %all-to-all-start.2 = ((bf16[32,8,128]{2,1,0:T(8,128)(2,1)}), bf16[32,8,128]{2,1,0:T(8,128)(2,1)S(1)}, u32[]{:S(2)}, u32[]{:S(2)}) async-start(bf16[32,8,128]{2,1,0:T(8,128)(2,1)} %bitcast.4), calls=%async_computation.2 | async-start | bytes 131072 | tf_op jit(solution)/shard_map/all_to_all | solution.py:334
  191.8 6.1 %copy-start.9 = (f32[512,128]{1,0:T(8,128)S(1)}, f32[512,128]{1,0:T(8,128)}, u32[]{:S(2)}) copy-start(f32[512,128]{1,0:T(8,128)} %copy-done.8) | copy-start | bytes 786436
  191.8 18.2 %all-to-all-start.7 = ((bf16[16,16,256]{2,1,0:T(8,128)(2,1)}), bf16[16,16,256]{2,1,0:T(8,128)(2,1)S(1)}, u32[]{:S(2)}, u32[]{:S(2)}) async-start(bf16[16,16,256]{2,1,0:T(8,128)(2,1)} %shard_map.150), calls=%async_computation.7 | async-start | bytes 262144 | tf_op jit(solution)/shard_map/all_to_all | solution.py:334
  195.9 3.1 %collective-permute-start.6 = (bf16[2,8,256]{2,1,0:T(8,128)(2,1)S(1)}, bf16[2,8,256]{2,1,0:T(8,128)(2,1)S(1)}, u32[]{:S(2)}, u32[]{:S(2)}) collective-permute-start(bf16[2,8,256]{2,1,0:T(8,128)(2,1)S(1)} %slice.3), channel_id=1, source_target_pairs={{0,1},{1,0},{2,3},{3,2},{4,5},{5,4},{6,7},{7,6},{8,9},{9,8},{10,11... | collective-permute-start | bytes 24584 | tf_op jit(solution)/shard_map/ppermute | solution.py:338

commit v8 on v7

--- a/solution.py
+++ b/solution.py
@@ -135,10 +135,7 @@
     decays = jnp.exp(jax.nn.sigmoid(log_rate) * (-0.6065306597126334))
     rates = jax.nn.sigmoid(rate_pre)
     unit = keys * lax.rsqrt(split_dot(keys * keys, same_head) + unit_epsilon)
-    seqs_row = limits_ref[...].astype(jnp.float32)
-    of_seq = iota((rows, seqs), 0) // NEW == iota((rows, seqs), 1)
-    limit = jnp.sum(jnp.where(of_seq, seqs_row, 0.0), 1, keepdims=True)
-    live = (iota((rows, LANES), 0) % NEW).astype(jnp.float32) < limit
+    live = (iota((rows, LANES), 0) % NEW).astype(jnp.float32) < limits_ref[...]
     decays = jnp.where(live, decays, 1.0)
     unit = jnp.where(live, unit, 0.0)
     keys = jnp.where(live, keys, 0.0)
@@ -232,8 +229,28 @@
         )
 
 
-def join_kernel(first_ref, second_ref, out_ref):
-    out_ref[...] = jnp.concatenate([first_ref[...], second_ref[...]], 0)
+def join_kernel(first_ref, second_ref, lengths_ref, lines_ref, limits_ref):
+    lines_ref[...] = jnp.concatenate([first_ref[...], second_ref[...]], 0)
+    rows = limits_ref.shape[0]
+    of_seq = iota((rows, rows // NEW), 0) // NEW == iota((rows, rows // NEW), 1)
+    limit = jnp.where(of_seq, lengths_ref[...].astype(jnp.float32), 0.0)
+    limits_ref[...] = jnp.broadcast_to(jnp.sum(limit, 1, keepdims=True), limits_ref.shape)
+
+
+def store_kernel(states_ref, *refs):
+    refs[-1][0] = states_ref[...]
+
+
+def store(layer, states, held):
+    return pl.pallas_call(
+        store_kernel,
+        grid=(1,),
+        out_shape=jax.ShapeDtypeStruct((2, *states.shape), states.dtype),
+        in_specs=[VMEM] + [pl.BlockSpec(memory_space=pl.ANY)] * (layer > 0),
+        out_specs=pl.BlockSpec((1, *states.shape), lambda i: (layer, 0, 0)),
+        input_output_aliases={1: 0} if layer else {},
+        **params(),
+    )(states, *([held] if layer else []))
 
 
 def stack_kernel(layer, *refs):
@@ -316,7 +333,7 @@
 
 
 def advance(layer, width, shared, arrived, limits, lines, states, awaited):
-    rows = limits.shape[1] * NEW
+    rows = limits.shape[0]
     return pl.pallas_call(
         functools.partial(advance_kernel, layer, rows, width),
         out_shape=(bf16(*shared), jax.ShapeDtypeStruct(states.shape[1:], jnp.float32)),
@@ -366,17 +383,19 @@
         for first in range(0, columns, 2)
     ]
     half, quarter = own_count // 2, own_count // 4
-    limits = lengths.reshape(1, -1)
     gathered = exchange(jnp.broadcast_to(tokens, (columns, own_count, depth)), "tp")
     other_out = from_partner(w_out, "tp")
     own_weights = call(
         functools.partial(stack_kernel, 1), bf16(6, depth, LANES), *weights
     )
     other_weights = from_partner(own_weights, "tp")
-    lines = call(
+    lines, limits = call(
         join_kernel,
-        jax.ShapeDtypeStruct((4, decay_base.shape[1]), jnp.float32),
-        decay_base, group_gain,
+        (
+            jax.ShapeDtypeStruct((4, LANES), jnp.float32),
+            jax.ShapeDtypeStruct((own_count, LANES), jnp.float32),
+        ),
+        decay_base, group_gain, lengths.reshape(1, -1),
     )
     packed = call(
         pack_kernel,
@@ -390,7 +409,6 @@
         functools.partial(project_kernel, True),
         bf16(columns, 3 * own_count + 8, LANES),
         gathered, norm_gain, *weights,
-        awaited=[core_own],
     )
     came = from_partner(far, "dp")
     near = call(
@@ -407,13 +425,14 @@
         functools.partial(out_kernel, 0),
         bf16(columns, quarter, 2 * depth),
         shared.reshape(2, owners, quarter, LANES), w_out, other_out, packed,
-        awaited=[core_other],
     )
     summed = exchange(product, "tp")
+    held = store(0, first_states, None)
     rows, spread = call(
         settle_kernel,
         (bf16(2, quarter, 2 * depth), bf16(columns, quarter, 2 * depth)),
         summed, tokens, packed,
+        awaited=[core_own, core_other],
     )
     gathered = exchange(spread, "tp")
     near = call(
@@ -434,7 +453,7 @@
     )
     summed = exchange(product, "tp")
     own_rows = call(finish_kernel, bf16(own_count, depth), summed, rows, back)
-    held = jnp.stack([first_states, last_states])
+    held = store(1, last_states, held)
     new_states = jnp.swapaxes(held.reshape(blocks, seqs, HEAD // 2, heads, LANES), 2, 3)
     return (own_rows, new_states.reshape(states.shape))
 

time: 212 us -> 202 us (0.953)
  blocking collectives: 70.6 us -> 128 us
  starting transfers between devices: 80.9 us -> 35.3 us
  waiting for transfers between devices: 47 us -> 27.4 us
    all_to_all x4 -> x5, blocking collectives: 70.6 us -> 128 us  [exchange(): return lax.all_to_all(x, axis, 0, 0, tiled=True, axis_index_groups=groups)]
    all_to_all x4 -> x3, starting transfers between devices: 64.7 us -> 17.8 us  [exchange(): return lax.all_to_all(x, axis, 0, 0, tiled=True, axis_index_groups=groups)]
    all_to_all x4 -> x3, waiting for transfers between devices: 33.4 us -> 20 us  [exchange(): return lax.all_to_all(x, axis, 0, 0, tiled=True, axis_index_groups=groups)]
    ppermute x7, waiting for transfers between devices: 13.5 us -> 7.41 us  [from_partner(): lax.ppermute(x, axis, [(i, i ^ 1) for i in range(lax.axis_size(axis))])]
  transfers between devices with their start and end apart: 11 -> 10, of which waited for: 7 -> 7; matrix products, arithmetic and copies ran while one was open for 0% -> 0% of each run, Pallas kernels for 1% -> 2%
where the time goes in v8:
time: 202 us; the launch traced here: 201 us
  blocking collectives  128 us (63%)
  starting transfers between devices  35.3 us (17%)
  waiting for transfers between devices  27.4 us (14%)
  Pallas kernels  8.84 us (4%)
    all_to_all x5, blocking collectives, exchange(): return lax.all_to_all(x, axis, 0, 0, tiled=True, axis_index_groups=groups)  128 us
    all_to_all x3, waiting for transfers between devices, exchange(): return lax.all_to_all(x, axis, 0, 0, tiled=True, axis_index_groups=groups)  20 us
    all_to_all x3, starting transfers between devices, exchange(): return lax.all_to_all(x, axis, 0, 0, tiled=True, axis_index_groups=groups)  17.8 us
    ppermute x7, starting transfers between devices, from_partner(): lax.ppermute(x, axis, [(i, i ^ 1) for i in range(lax.axis_size(axis))])  17.5 us
    ppermute x7, waiting for transfers between devices, from_partner(): lax.ppermute(x, axis, [(i, i ^ 1) for i in range(lax.axis_size(axis))])  7.41 us
    pallas_call x10, Pallas kernels, call(): pl.pallas_call(kernel, out_shape=outs, in_specs=[VMEM] * len(operands) +...  4.25 us
  transfers between devices with their start and end apart: 10, of which 7 were waited for; matrix products, arithmetic and copies ran while one was open for 0% of the time, Pallas kernels for 2%

profile of v8, /device:TPU:80, one launch (start us, length us, event | category | flops | bytes accessed | tf_op | source)
XLA Modules:
  0.0 200.9 jit_solution(17073552628471537996)
XLA Ops:
  0.7 0.8 broadcast_in_dim.3
  1.4 0.0 copy-start
  1.5 0.0 copy-start.1
  1.5 0.0 copy-start.2
  1.5 0.0 copy-start.3
  1.5 61.7 %all_to_all.40.x_ref = bf16[16,32,256]{2,1,0:T(8,128)(2,1)S(1)} all-to-all(bf16[16,32,256]{2,1,0:T(8,128)(2,1)S(1)} %broadcast_in_dim.3), channel_id=1, replica_groups=mesh['grp'=2,'tp'=16,'dp'=16] {'tp'}, dimensions={0} | all-to-all | bytes 524288 | tf_op jit(solution)/shard_map/all_to_all | solution.py:351
  63.2 0.0 copy-done.11
  63.2 0.0 copy-done
  63.3 0.0 copy-done.1
  63.3 0.3 shard_map.140
  63.6 2.0 collective-permute-start
  65.5 1.7 collective-permute-done.refs_6_
  67.3 1.0 shard_map.141
  68.3 7.8 %all-to-all-start.1 = ((bf16[16,104,128]{2,1,0:T(8,128)(2,1)}), bf16[16,104,128]{2,1,0:T(8,128)(2,1)S(1)}, u32[]{:S(2)}, u32[]{:S(2)}) async-start(bf16[16,104,128]{2,1,0:T(8,128)(2,1)} %shard_map.141), calls=%async_computation.1 | async-start | bytes 851968 | tf_op jit(solution)/shard_map/all_to_all | solution.py:351
  76.1 3.6 %collective-permute-start.1 = (bf16[2,128,256]{2,1,0:T(8,128)(2,1)S(1)}, bf16[2,128,256]{2,1,0:T(8,128)(2,1)S(1)}, u32[]{:S(2)}, u32[]{:S(2)}) collective-permute-start(bf16[2,128,256]{2,1,0:T(8,128)(2,1)S(1)} %copy-done.7), channel_id=1, source_target_pairs={{0,16},{16,0},{32,48},{48,32},{64,80},{80,64},{96,112},{112,96},{1... | collective-permute-start | bytes 393224 | tf_op jit(solution)/shard_map/ppermute | solution.py:355
  79.7 3.9 %collective-permute-done.1.other_ref = bf16[2,128,256]{2,1,0:T(8,128)(2,1)S(1)} collective-permute-done((bf16[2,128,256]{2,1,0:T(8,128)(2,1)S(1)}, bf16[2,128,256]{2,1,0:T(8,128)(2,1)S(1)}, u32[]{:S(2)}, u32[]{:S(2)}) %collective-permute-start.1) | collective-permute-done | bytes 131104 | tf_op jit(solution)/shard_map/ppermute | solution.py:355
  83.7 2.1 %collective-permute-start.2 = (bf16[288,256]{1,0:T(8,128)(2,1)S(1)}, bf16[288,256]{1,0:T(8,128)(2,1)S(1)}, u32[]{:S(2)}, u32[]{:S(2)}) collective-permute-start(bf16[288,256]{1,0:T(8,128)(2,1)S(1)} %shard_map.143), channel_id=1, source_target_pairs={{0,1},{1,0},{2,3},{3,2},{4,5},{5,4},{6,7},{7,6},{8,9},{9,8},{10,11... | collective-permute-start | bytes 442376 | tf_op jit(solution)/shard_map/ppermute | solution.py:355
  85.8 0.0 copy-start.13
  85.8 0.0 copy-start.12
  85.8 0.0 copy-start.14
  85.8 3.6 %collective-permute-start.4 = (bf16[6,256,128]{2,1,0:T(8,128)(2,1)S(1)}, bf16[6,256,128]{2,1,0:T(8,128)(2,1)S(1)}, u32[]{:S(2)}, u32[]{:S(2)}) collective-permute-start(bf16[6,256,128]{2,1,0:T(8,128)(2,1)S(1)} %shard_map.146), channel_id=1, source_target_pairs={{0,16},{16,0},{32,48},{48,32},{64,80},{80,64},{96,112},{112,96},{1... | collective-permute-start | bytes 1179656 | tf_op jit(solution)/shard_map/ppermute | solution.py:355
  89.4 0.1 shard_map.142
  89.5 0.0 collective-permute-done.2.refs_0_.packed_ref
  89.5 0.6 all-to-all-done.1.arrived_ref
  90.1 1.6 shard_map.144
  91.7 0.0 copy-start.8
  91.7 15.2 %all_to_all.41 = bf16[32,8,128]{2,1,0:T(8,128)(2,1)S(1)} all-to-all(bf16[32,8,128]{2,1,0:T(8,128)(2,1)S(1)} %bitcast.22), channel_id=1, replica_groups={{0,1,2,3,4,5,6,7,8,9,10,11,12,13,14,15,16,17,18,19,20,21,22,23,24,25,26..., dimensions={0} | all-to-all | bytes 131072 | tf_op jit(solution)/shard_map/all_to_all | solution.py:351
  106.8 0.9 shard_map.145
  107.7 5.9 %all-to-all-start.3 = ((bf16[16,8,512]{2,1,0:T(8,128)(2,1)}), bf16[16,8,512]{2,1,0:T(8,128)(2,1)S(1)}, u32[]{:S(2)}, u32[]{:S(2)}) async-start(bf16[16,8,512]{2,1,0:T(8,128)(2,1)} %shard_map.145), calls=%async_computation.3 | async-start | bytes 262144 | tf_op jit(solution)/shard_map/all_to_all | solution.py:351
  113.7 2.0 collective-permute-start.3
  115.6 0.0 collective-permute-done.4.refs_6_
  115.6 2.4 %collective-permute-start.5 = (bf16[6,256,128]{2,1,0:T(8,128)(2,1)S(1)}, bf16[6,256,128]{2,1,0:T(8,128)(2,1)S(1)}, u32[]{:S(2)}, u32[]{:S(2)}) collective-permute-start(bf16[6,256,128]{2,1,0:T(8,128)(2,1)S(1)} %collective-permute-done.4.refs_6_), channel_id=1, source_target_pairs={{0,1},{1,0},{2,3},{3,2},{4,5},{5,4},{6,7},{7,6},{8,9},{9,8},{10,11... | collective-permute-start | bytes 1179656 | tf_op jit(solution)/shard_map/ppermute | solution.py:355
  118.1 0.0 collective-permute-done.3.refs_0_.refs_7_
  118.1 1.3 collective-permute-done.5.refs_1_.refs_8_
  119.4 8.8 %all-to-all-done.3.summed_ref = bf16[16,8,512]{2,1,0:T(8,128)(2,1)S(1)} async-done(((bf16[16,8,512]{2,1,0:T(8,128)(2,1)}), bf16[16,8,512]{2,1,0:T(8,128)(2,1)S(1)}, u32[]{:S(2)}, u32[]{:S(2)}) %all-to-all-start.3) | async-done | bytes 131104 | tf_op jit(solution)/shard_map/all_to_all | solution.py:351
  128.2 18.0 %all_to_all.42.x_ref = bf16[16,8,512]{2,1,0:T(8,128)(2,1)S(1)} all-to-all(bf16[16,8,512]{2,1,0:T(8,128)(2,1)S(1)} %get-tuple-element.13), channel_id=1, replica_groups=mesh['grp'=2,'tp'=16,'dp'=16] {'tp'}, dimensions={0} | all-to-all | bytes 262144 | tf_op jit(solution)/shard_map/all_to_all | solution.py:351
  146.3 0.4 shard_map.148
  146.7 18.5 %all_to_all.43.arrived_ref = bf16[32,56,128]{2,1,0:T(8,128)(2,1)S(1)} all-to-all(bf16[32,56,128]{2,1,0:T(8,128)(2,1)S(1)} %bitcast.18), channel_id=1, replica_groups={{0,1,2,3,4,5,6,7,8,9,10,11,12,13,14,15,16,17,18,19,20,21,22,23,24,25,26..., dimensions={0} | all-to-all | bytes 917504 | tf_op jit(solution)/shard_map/all_to_all | solution.py:351
  165.2 1.6 shard_map.149
  166.8 14.1 %all_to_all.44 = bf16[32,16,128]{2,1,0:T(8,128)(2,1)S(1)} all-to-all(bf16[32,16,128]{2,1,0:T(8,128)(2,1)S(1)} %bitcast.21), channel_id=1, replica_groups={{0,1,2,3,4,5,6,7,8,9,10,11,12,13,14,15,16,17,18,19,20,21,22,23,24,25,26..., dimensions={0} | all-to-all | bytes 262144 | tf_op jit(solution)/shard_map/all_to_all | solution.py:351
  180.9 0.9 shard_map.150
  181.7 4.1 %all-to-all-start.7 = ((bf16[16,16,256]{2,1,0:T(8,128)(2,1)}), bf16[16,16,256]{2,1,0:T(8,128)(2,1)S(1)}, u32[]{:S(2)}, u32[]{:S(2)}) async-start(bf16[16,16,256]{2,1,0:T(8,128)(2,1)} %shard_map.150), calls=%async_computation.7 | async-start | bytes 262144 | tf_op jit(solution)/shard_map/all_to_all | solution.py:351
  185.8 0.7 shard_map.152.refs_0_
  186.6 1.9 collective-permute-start.6
  188.5 0.7 shard_map.153
  189.2 0.4 collective-permute-done.6.back_ref
  189.6 10.6 %all-to-all-done.7.summed_ref = bf16[16,16,256]{2,1,0:T(8,128)(2,1)S(1)} async-done(((bf16[16,16,256]{2,1,0:T(8,128)(2,1)}), bf16[16,16,256]{2,1,0:T(8,128)(2,1)S(1)}, u32[]{:S(2)}, u32[]{:S(2)}) %all-to-all-start.7) | async-done | bytes 131104 | tf_op jit(solution)/shard_map/all_to_all | solution.py:351
  200.3 0.6 shard_map.151
  (23 shorter events, 0.1 us)
Async XLA Ops:
  0.6 62.6 %copy-start.4 = (bf16[2,256,128]{2,1,0:T(8,128)(2,1)S(1)}, bf16[2,256,128]{2,1,0:T(8,128)(2,1)}, u32[]{:S(2)}) copy-start(bf16[2,256,128]{2,1,0:T(8,128)(2,1)} %refs_4_.7) | copy-start | bytes 393220
  0.6 62.6 %copy-start.5 = (bf16[2,256,128]{2,1,0:T(8,128)(2,1)S(1)}, bf16[2,256,128]{2,1,0:T(8,128)(2,1)}, u32[]{:S(2)}) copy-start(bf16[2,256,128]{2,1,0:T(8,128)(2,1)} %refs_5_.7) | copy-start | bytes 393220
  0.7 62.6 %copy-start.11 = (f32[2,256]{1,0:T(2,128)S(1)}, f32[2,256]{1,0:T(2,128)}, u32[]{:S(2)}) copy-start(f32[2,256]{1,0:T(2,128)} %gain_ref.7) | copy-start | bytes 6148
  1.4 61.8 %copy-start = (bf16[2,256,128]{2,1,0:T(8,128)(2,1)S(1)}, bf16[2,256,128]{2,1,0:T(8,128)(2,1)}, u32[]{:S(2)}) copy-start(bf16[2,256,128]{2,1,0:T(8,128)(2,1)} %refs_0_.7) | copy-start | bytes 393220
  1.5 61.8 %copy-start.1 = (bf16[2,256,128]{2,1,0:T(8,128)(2,1)S(1)}, bf16[2,256,128]{2,1,0:T(8,128)(2,1)}, u32[]{:S(2)}) copy-start(bf16[2,256,128]{2,1,0:T(8,128)(2,1)} %refs_1_.7) | copy-start | bytes 393220
  1.5 61.8 %copy-start.2 = (bf16[2,256,128]{2,1,0:T(8,128)(2,1)S(1)}, bf16[2,256,128]{2,1,0:T(8,128)(2,1)}, u32[]{:S(2)}) copy-start(bf16[2,256,128]{2,1,0:T(8,128)(2,1)} %refs_2_.7) | copy-start | bytes 393220
  1.5 61.8 %copy-start.3 = (bf16[2,256,128]{2,1,0:T(8,128)(2,1)S(1)}, bf16[2,256,128]{2,1,0:T(8,128)(2,1)}, u32[]{:S(2)}) copy-start(bf16[2,256,128]{2,1,0:T(8,128)(2,1)} %refs_3_.7) | copy-start | bytes 393220
  63.6 3.7 %collective-permute-start = (bf16[16,104,128]{2,1,0:T(8,128)(2,1)S(1)}, bf16[16,104,128]{2,1,0:T(8,128)(2,1)S(1)}, u32[]{:S(2)}, u32[]{:S(2)}) collective-permute-start(bf16[16,104,128]{2,1,0:T(8,128)(2,1)S(1)} %shard_map.140), channel_id=1, source_target_pairs={{0,1},{1,0},{2,3},{3,2},{4,5},{5,4},{6,7},{7,6},{8,9},{9,8},{10,11... | collective-permute-start | bytes 1277960 | tf_op jit(solution)/shard_map/ppermute | solution.py:355
  68.3 7.8 %copy-start.7 = (bf16[2,128,256]{2,1,0:T(8,128)(2,1)S(1)}, bf16[2,128,256]{2,1,0:T(8,128)(2,1)}, u32[]{:S(2)}) copy-start(bf16[2,128,256]{2,1,0:T(8,128)(2,1)} %own_ref.5) | copy-start | bytes 393220
  68.3 15.3 %copy-start.10 = (bf16[32,256]{1,0:T(8,128)(2,1)S(1)}, bf16[32,256]{1,0:T(8,128)(2,1)}, u32[]{:S(2)}) copy-start(bf16[32,256]{1,0:T(8,128)(2,1)} %tokens_ref.3) | copy-start | bytes 49156
  68.3 21.8 %all-to-all-start.1 = ((bf16[16,104,128]{2,1,0:T(8,128)(2,1)}), bf16[16,104,128]{2,1,0:T(8,128)(2,1)S(1)}, u32[]{:S(2)}, u32[]{:S(2)}) async-start(bf16[16,104,128]{2,1,0:T(8,128)(2,1)} %shard_map.141), calls=%async_computation.1 | async-start | bytes 851968 | tf_op jit(solution)/shard_map/all_to_all | solution.py:351
  76.1 7.5 %collective-permute-start.1 = (bf16[2,128,256]{2,1,0:T(8,128)(2,1)S(1)}, bf16[2,128,256]{2,1,0:T(8,128)(2,1)S(1)}, u32[]{:S(2)}, u32[]{:S(2)}) collective-permute-start(bf16[2,128,256]{2,1,0:T(8,128)(2,1)S(1)} %copy-done.7), channel_id=1, source_target_pairs={{0,16},{16,0},{32,48},{48,32},{64,80},{80,64},{96,112},{112,96},{1... | collective-permute-start | bytes 393224 | tf_op jit(solution)/shard_map/ppermute | solution.py:355
  83.7 6.4 %copy-start.6 = (f32[2,8,2,4096]{3,2,1,0:T(2,128)S(1)}, f32[2,8,2,4096]{3,2,1,0:T(2,128)}, u32[]{:S(2)}) copy-start(f32[2,8,2,4096]{3,2,1,0:T(2,128)} %param.25) | copy-start | bytes 1572868
  83.7 5.9 %collective-permute-start.2 = (bf16[288,256]{1,0:T(8,128)(2,1)S(1)}, bf16[288,256]{1,0:T(8,128)(2,1)S(1)}, u32[]{:S(2)}, u32[]{:S(2)}) collective-permute-start(bf16[288,256]{1,0:T(8,128)(2,1)S(1)} %shard_map.143), channel_id=1, source_target_pairs={{0,1},{1,0},{2,3},{3,2},{4,5},{5,4},{6,7},{7,6},{8,9},{9,8},{10,11... | collective-permute-start | bytes 442376 | tf_op jit(solution)/shard_map/ppermute | solution.py:355
  85.8 3.7 %copy-start.13 = (f32[2,128]{1,0:T(2,128)S(1)}, f32[2,128]{1,0:T(2,128)}, u32[]{:S(2)}) copy-start(f32[2,128]{1,0:T(2,128)} %second_ref.1) | copy-start | bytes 3076
  85.8 3.6 %copy-start.12 = (f32[2,128]{1,0:T(2,128)S(1)}, f32[2,128]{1,0:T(2,128)}, u32[]{:S(2)}) copy-start(f32[2,128]{1,0:T(2,128)} %first_ref.1) | copy-start | bytes 3076
  85.8 3.6 %copy-start.14 = (s32[8]{0:T(128)S(1)}, s32[8]{0:T(128)}, u32[]{:S(2)}) copy-start(s32[8]{0:T(128)} %param.14) | copy-start | bytes 100
  85.8 29.8 %collective-permute-start.4 = (bf16[6,256,128]{2,1,0:T(8,128)(2,1)S(1)}, bf16[6,256,128]{2,1,0:T(8,128)(2,1)S(1)}, u32[]{:S(2)}, u32[]{:S(2)}) collective-permute-start(bf16[6,256,128]{2,1,0:T(8,128)(2,1)S(1)} %shard_map.146), channel_id=1, source_target_pairs={{0,16},{16,0},{32,48},{48,32},{64,80},{80,64},{96,112},{112,96},{1... | collective-permute-start | bytes 1179656 | tf_op jit(solution)/shard_map/ppermute | solution.py:355
  91.7 16.1 %copy-start.8 = (f32[512,128]{1,0:T(8,128)}, f32[512,128]{1,0:T(8,128)S(1)}, u32[]{:S(2)}) copy-start(f32[512,128]{1,0:T(8,128)S(1)} %get-tuple-element.17.states_ref) | copy-start | bytes 786436
  107.7 20.5 %all-to-all-start.3 = ((bf16[16,8,512]{2,1,0:T(8,128)(2,1)}), bf16[16,8,512]{2,1,0:T(8,128)(2,1)S(1)}, u32[]{:S(2)}, u32[]{:S(2)}) async-start(bf16[16,8,512]{2,1,0:T(8,128)(2,1)} %shard_map.145), calls=%async_computation.3 | async-start | bytes 262144 | tf_op jit(solution)/shard_map/all_to_all | solution.py:351
  113.7 4.4 %collective-permute-start.3 = (bf16[6,256,128]{2,1,0:T(8,128)(2,1)S(1)}, bf16[6,256,128]{2,1,0:T(8,128)(2,1)S(1)}, u32[]{:S(2)}, u32[]{:S(2)}) collective-permute-start(bf16[6,256,128]{2,1,0:T(8,128)(2,1)S(1)} %shard_map.146), channel_id=1, source_target_pairs={{0,1},{1,0},{2,3},{3,2},{4,5},{5,4},{6,7},{7,6},{8,9},{9,8},{10,11... | collective-permute-start | bytes 1179656 | tf_op jit(solution)/shard_map/ppermute | solution.py:355
  115.6 3.8 %collective-permute-start.5 = (bf16[6,256,128]{2,1,0:T(8,128)(2,1)S(1)}, bf16[6,256,128]{2,1,0:T(8,128)(2,1)S(1)}, u32[]{:S(2)}, u32[]{:S(2)}) collective-permute-start(bf16[6,256,128]{2,1,0:T(8,128)(2,1)S(1)} %collective-permute-done.4.refs_6_), channel_id=1, source_target_pairs={{0,1},{1,0},{2,3},{3,2},{4,5},{5,4},{6,7},{7,6},{8,9},{9,8},{10,11... | collective-permute-start | bytes 1179656 | tf_op jit(solution)/shard_map/ppermute | solution.py:355
  181.7 4.1 %copy-start.9 = (f32[512,128]{1,0:T(8,128)S(1)}, f32[512,128]{1,0:T(8,128)}, u32[]{:S(2)}) copy-start(f32[512,128]{1,0:T(8,128)} %copy-done.8) | copy-start | bytes 786436
  181.7 18.6 %all-to-all-start.7 = ((bf16[16,16,256]{2,1,0:T(8,128)(2,1)}), bf16[16,16,256]{2,1,0:T(8,128)(2,1)S(1)}, u32[]{:S(2)}, u32[]{:S(2)}) async-start(bf16[16,16,256]{2,1,0:T(8,128)(2,1)} %shard_map.150), calls=%async_computation.7 | async-start | bytes 262144 | tf_op jit(solution)/shard_map/all_to_all | solution.py:351
  186.6 3.1 %collective-permute-start.6 = (bf16[2,8,256]{2,1,0:T(8,128)(2,1)S(1)}, bf16[2,8,256]{2,1,0:T(8,128)(2,1)S(1)}, u32[]{:S(2)}, u32[]{:S(2)}) collective-permute-start(bf16[2,8,256]{2,1,0:T(8,128)(2,1)S(1)} %slice.3), channel_id=1, source_target_pairs={{0,1},{1,0},{2,3},{3,2},{4,5},{5,4},{6,7},{7,6},{8,9},{9,8},{10,11... | collective-permute-start | bytes 24584 | tf_op jit(solution)/shard_map/ppermute | solution.py:355
